TPU v7x, 512 devices: a whole 4x8x8 slice. The times are simulated.
512 devices in a mesh: kv: 64 (over z, y), tp: 8 (over x, core).
Axes of the slice: x: 4, y: 8, z: 8, core: 2. Of those that a mesh axis runs over, the one named last changes fastest.
Arguments:
- normed: bfloat16 [32768, 4096], P('kv'), may hold values from -16 to 16
- queries: bfloat16 [32768, 1024], P('kv', 'tp'), may hold values from -6 to 6
- keys: bfloat16 [32768, 64], P('kv'), may hold values from -6 to 6
- values: bfloat16 [32768, 64], P('kv'), may hold values from -6 to 6
- attended: bfloat16 [32768, 1024], P('kv', 'tp'), may hold values from -6 to 6
- cotangent: bfloat16 [32768, 1024], P('kv', 'tp'), may hold values from -24 to 24
- log_sum: float32 [32768, 16], P('kv', 'tp'), may hold values from 6 to 8
- chosen: int32 [512, 16], P('kv'), may hold values from -1 to 511, as said below
Outputs:
- grad_queries: bfloat16 [32768, 1024], P('kv', 'tp')
- grad_keys: float32 [32768, 64], P('kv')
- grad_values: float32 [32768, 64], P('kv')
- weight_grad: float32 [4096, 1024], P('kv', 'tp')
Inputs may be any that keep to these rules, and one draw needn't show every extreme that they name: `chosen`: each row lists distinct key blocks, none after its own block, and always its own block; the listed entries come first and -1 fills the rest. A row lists from 8 to 16 blocks, fewer only where fewer blocks are open to it; on every index of kv some row lists 16 blocks where that many are open. The rows of one index of kv together list at most one block of each other index of kv's positions; every index of kv from 1 on lists a block of index 0 and a block of the index before it, and every index from half the axis on a block of the index half the axis before it.
All inputs are finite; a program needn't handle non-finite values.
Results may differ from a plain program's by a relative error of at most 0.007.
Values may be sent and summed in bfloat16 or wider, within the bound.
No kernel may reach another device: no remote copies, remote signals or barrier semaphores. Data moves between devices by JAX's collectives and lax.ppermute only.
A program may use at most 64 MiB of HBM per device.

v0:
```python
import jax
import jax.numpy as jnp
from jax import lax
from jax.sharding import Mesh
from jax.sharding import PartitionSpec as P

BLOCK = 64
KV = ("kv_0", "kv_1")


def from_everyone(shard, axis):
    copies = jnp.broadcast_to(shard, (lax.axis_size(axis), *shard.shape))
    return lax.all_to_all(copies, axis, split_axis=0, concat_axis=0, tiled=True)


def of_everyone(shard, axis):
    return from_everyone(shard, axis).sum(axis=0)


def summed_rows(running, axes):
    for axis in axes:
        running = lax.psum_scatter(running, axis, scatter_dimension=0, tiled=True)
    return running


def shards(normed, queries, keys, values, attended, cotangent, log_sum, chosen):
    my_rank = lax.axis_index(KV)
    peer_count = lax.axis_size(KV)
    tok_rows, model_width = normed.shape
    slot_count = chosen.shape[1]
    local_blocks = tok_rows // BLOCK
    head_dim = keys.shape[1]
    heads_here = log_sum.shape[1]
    score_scale = head_dim ** (-0.5)
    pairs_local = jnp.concatenate([keys, values], axis=1).reshape(local_blocks, BLOCK, 2 * head_dim)
    owners = chosen // local_blocks
    within = chosen % local_blocks
    listed = chosen >= 0
    remote = listed & (owners != my_rank)
    peer_ids = jnp.arange(peer_count, dtype=jnp.int32)
    matched = remote[:, :, None] & (owners[:, :, None] == peer_ids[None, None, :])
    wanted = jnp.max(jnp.where(matched, within[:, :, None] + 1, 0), axis=(0, 1))
    asked_for = (
        lax.all_to_all(wanted.reshape(peer_count, 1), KV, split_axis=0, concat_axis=0, tiled=True)[
            :, 0
        ]
        - 1
    )
    picked = jnp.maximum(asked_for, 0)
    outgoing = jnp.take(pairs_local, picked, axis=0)
    fetched = lax.all_to_all(outgoing, KV, split_axis=0, concat_axis=0, tiled=True)
    block_table = jnp.concatenate([pairs_local, fetched], axis=0)
    slot_index = jnp.where(owners == my_rank, within, local_blocks + owners)
    slot_index = jnp.where(listed, slot_index, 0)
    gathered = jnp.take(block_table, slot_index.reshape(-1), axis=0)
    gathered = gathered.reshape(local_blocks, slot_count * BLOCK, 2 * head_dim)
    selected_keys = gathered[:, :, :head_dim]
    selected_values = gathered[:, :, head_dim:]
    query_matrix = queries.reshape(local_blocks, BLOCK, heads_here, head_dim)
    gradient_rows = cotangent.reshape(local_blocks, BLOCK, heads_here, head_dim)
    out_rows = attended.reshape(local_blocks, BLOCK, heads_here, head_dim)
    log_rows = log_sum.reshape(local_blocks, BLOCK, heads_here).transpose(0, 2, 1)
    offsets = jnp.arange(BLOCK, dtype=jnp.int32)
    query_pos = (my_rank * tok_rows + jnp.arange(tok_rows, dtype=jnp.int32)).reshape(
        local_blocks, BLOCK
    )
    key_pos = (jnp.where(listed, chosen, 0)[:, :, None] * BLOCK + offsets).reshape(
        local_blocks, slot_count * BLOCK
    )
    listed_keys = jnp.repeat(listed, BLOCK, axis=1)
    allowed = listed_keys[:, None, :] & (key_pos[:, None, :] <= query_pos[:, :, None])
    scores = (
        jnp.einsum(
            "gfvo,geo->gvfe", query_matrix, selected_keys, preferred_element_type=jnp.float32
        )
        * score_scale
    )
    probs = jnp.where(allowed[:, None], jnp.exp(scores - log_rows[:, :, :, None]), 0.0)
    reduced_probabilities = probs.astype(jnp.bfloat16)
    grad_value = jnp.einsum(
        "jpqx,jqpe->jxe", reduced_probabilities, gradient_rows, preferred_element_type=jnp.float32
    )
    probability_gradient = jnp.einsum(
        "gfvo,geo->gvfe", gradient_rows, selected_values, preferred_element_type=jnp.float32
    )
    deltas = jnp.sum(
        gradient_rows.astype(jnp.float32) * out_rows.astype(jnp.float32), axis=-1
    ).transpose(0, 2, 1)
    score_gradient = (probs * (probability_gradient - deltas[:, :, :, None]) * score_scale).astype(
        jnp.bfloat16
    )
    query_gradient = jnp.einsum(
        "xwqi,xiu->xqwu", score_gradient, selected_keys, preferred_element_type=jnp.float32
    )
    query_gradient = query_gradient.astype(jnp.bfloat16).reshape(tok_rows, heads_here * head_dim)
    key_gradient = jnp.einsum(
        "jpqx,jqpe->jxe", score_gradient, query_matrix, preferred_element_type=jnp.float32
    )
    slot_grads = jnp.concatenate([key_gradient, grad_value], axis=2).reshape(
        local_blocks * slot_count, BLOCK * 2 * head_dim
    )
    table_ids = jnp.arange(local_blocks + peer_count, dtype=jnp.int32)
    one_hot = (
        (slot_index.reshape(-1)[:, None] == table_ids[None, :]) & listed.reshape(-1)[:, None]
    ).astype(jnp.float32)
    block_sums = jnp.dot(one_hot.T, slot_grads)
    block_sums = block_sums.reshape(local_blocks + peer_count, BLOCK, 2 * head_dim)
    own_part = block_sums[:local_blocks]
    sent_back = block_sums[local_blocks:]
    taken_by = (asked_for[:, None] == jnp.arange(local_blocks, dtype=jnp.int32)[None, :]).astype(
        jnp.float32
    )
    returned = lax.all_to_all(sent_back, KV, split_axis=0, concat_axis=0, tiled=True)
    totals = own_part + jnp.einsum("sb,skc->bkc", taken_by, returned)
    totals = of_everyone(totals, "tp")
    grad_keys = totals[:, :, :head_dim].reshape(tok_rows, head_dim)
    grad_values = totals[:, :, head_dim:].reshape(tok_rows, head_dim)
    weight_grad = summed_rows(
        lax.dot_general(
            normed, query_gradient, (((0,), (0,)), ((), ())), preferred_element_type=jnp.float32
        ),
        KV,
    )
    return (query_gradient, grad_keys, grad_values, weight_grad)


def solution(mesh):
    torus = Mesh(mesh.devices.reshape(8, 8, mesh.shape["tp"]), ("kv_0", "kv_1", "tp"))
    in_specs = (
        P(KV, None),
        P(KV, "tp"),
        P(KV, None),
        P(KV, None),
        P(KV, "tp"),
        P(KV, "tp"),
        P(KV, "tp"),
        P(KV, None),
    )
    out_specs = (P(KV, "tp"), P(KV, None), P(KV, None), P(KV, "tp"))
    return jax.shard_map(
        shards, mesh=torus, in_specs=in_specs, out_specs=out_specs, check_vma=False
    )
```

profile of v0, /device:TPU:2, one launch (start us, length us, event | category | flops | bytes accessed | tf_op | source)
XLA Modules:
  0.0 207.3 jit_solution(2065064810087217444)
XLA Ops:
  9.4 16.6 %all-to-all-start = ((s32[64,1,1]{2,1,0:T(1,128)}), s32[64,1,1]{2,1,0:T(1,128)S(1)}, u32[]{:S(2)}, u32[]{:S(2)}) async-start(s32[64,1,1]{2,1,0:T(1,128)} %copy.68), calls=%async_computation | async-start | bytes 65536 | tf_op jit(solution)/shard_map/all_to_all | solution.py:44
  26.0 1.0 copy.67
  27.0 1.0 copy.66
  28.1 9.9 %all-to-all-done = s32[64,1,1]{2,1,0:T(1,128)S(1)} async-done(((s32[64,1,1]{2,1,0:T(1,128)}), s32[64,1,1]{2,1,0:T(1,128)S(1)}, u32[]{:S(2)}, u32[]{:S(2)}) %all-to-all-start) | async-done | bytes 288 | tf_op jit(solution)/shard_map/all_to_all | solution.py:44
  38.0 2.4 %add_reduce_fusion = (s32[64]{0:T(128)S(1)}, s32[64]{0:T(128)S(1)}) fusion(s32[64,1,1]{2,1,0:T(1,128)S(1)} %all-to-all-done), kind=kLoop, calls=%fused_computation.44 | loop fusion | flops 128 | bytes 768 | tf_op jit(solution)/shard_map/sub | solution.py:44
  40.4 0.7 gather_fusion
  41.1 1.1 broadcast_select_fusion.1
  42.3 4.8 %all-to-all-start.1 = ((bf16[64,64,128]{2,1,0:T(8,128)(2,1)}), bf16[64,64,128]{2,1,0:T(8,128)(2,1)S(1)}, u32[]{:S(2)}, u32[]{:S(2)}) async-start(bf16[64,64,128]{2,1,0:T(8,128)(2,1)} %broadcast_select_fusion.1), calls=%async_computation.1 | async-start | bytes 2097152 | tf_op jit(solution)/shard_map/all_to_all | solution.py:51
  49.3 0.9 copy.76
  52.9 1.3 compare_and_fusion
  54.2 21.6 %all-to-all-done.1 = bf16[64,64,128]{2,1,0:T(8,128)(2,1)S(1)} async-done(((bf16[64,64,128]{2,1,0:T(8,128)(2,1)}), bf16[64,64,128]{2,1,0:T(8,128)(2,1)S(1)}, u32[]{:S(2)}, u32[]{:S(2)}) %all-to-all-start.1) | async-done | bytes 1048608 | tf_op jit(solution)/shard_map/all_to_all | solution.py:51
  75.9 1.1 gather_fusion.1
  77.0 2.6 %copy.69 = bf16[8,1024,128]{1,2,0:T(8,128)(2,1)} copy(bf16[8,1024,128]{2,1,0:T(8,128)(2,1)S(1)} %bitcast.81) | data formatting | bytes 4194304 | tf_op jit(solution)/shard_map/jit(_take)/gather | solution.py:55
  79.6 1.8 broadcast_select_fusion
  81.5 0.8 fusion.21
  82.5 2.4 %fusion.14 = bf16[8,1024,64]{1,2,0:T(8,128)(2,1)} fusion(bf16[8,64,2,64]{1,3,2,0:T(8,128)(2,1)S(1)} %copy-done.1, f32[8,1024,64,2]{1,2,3,0:T(8,128)S(1)} %fusion.21, f32[8,2,64]{2,1,0:T(2,128)S(1)} %bitcast.86, pred[8,64,1024]{2,1,0:T(8,128)(4,1)S(1)} %copy-done), kind=kOutput, calls=%fused_computation.22 | convolution fusion | flops 138412032 | bytes 5902336 | tf_op jit(solution)/shard_map/jpqx,jqpe->jxe/dot_general | solution.py:80
  84.9 2.0 fusion.2
  86.9 1.1 fusion.20
  88.9 1.5 pad_maximum_fusion
  90.4 2.4 %copy.77 = bf16[8,1024,128]{2,1,0:T(8,128)(2,1)} copy(bf16[8,1024,128]{1,2,0:T(8,128)(2,1)S(1)} %pad_maximum_fusion) | data formatting | bytes 4194304 | tf_op jit(solution)/shard_map/concatenate | solution.py:99
  92.8 2.8 %reshape.153 = bf16[128,8192]{1,0:T(8,128)(2,1)S(1)} reshape(bf16[8,1024,128]{2,1,0:T(8,128)(2,1)} %copy.77) | data formatting | bytes 4194304 | tf_op jit(solution)/shard_map/reshape | solution.py:99
  95.6 4.2 %convolution_bitcast_fusion = f32[4096,128]{0,1:T(8,128)} fusion(bf16[512,128]{0,1:T(8,128)(2,1)S(1)} %reshape.151, bf16[512,4096]{1,0:T(8,128)(2,1)} %param.8), kind=kOutput, calls=%fused_computation.2 | convolution fusion | flops 536870912 | bytes 6422528 | tf_op jit(solution)/shard_map/dot_general | solution.py:119
  101.6 34.3 %all_to_all.24 = bf16[64,64,128]{2,1,0:T(8,128)(2,1)S(1)} all-to-all(bf16[64,64,128]{2,1,0:T(8,128)(2,1)S(1)} %bitcast.82), channel_id=1, replica_groups=mesh['kv_0'=8,'kv_1'=8,'tp'=8] {'kv_0','kv_1'}, dimensions={0} | all-to-all | bytes 2097152 | tf_op jit(solution)/shard_map/all_to_all | solution.py:113
  136.6 1.6 broadcast_in_dim.80
  138.2 4.8 %all-to-all-start.3 = ((f32[8,8,64,128]{3,2,1,0:T(8,128)}), f32[8,8,64,128]{3,2,1,0:T(8,128)S(1)}, u32[]{:S(2)}, u32[]{:S(2)}) async-start(f32[8,8,64,128]{3,2,1,0:T(8,128)} %broadcast_in_dim.80), calls=%async_computation.3 | async-start | bytes 4194304 | tf_op jit(solution)/shard_map/all_to_all | solution.py:13
  143.0 17.2 %reduce-scatter.5.cloned.1.call-done = f32[512,128]{0,1:T(8,128)} async-done(((f32[4096,128]{0,1:T(8,128)}), f32[512,128]{0,1:T(8,128)}) %reduce-scatter.5.cloned.1.call-update) | async-done | bytes 262160 | tf_op jit(solution)/shard_map/reduce_scatter | solution.py:22
  160.2 1.8 copy.88
  162.0 0.8 copy.80
  162.8 6.0 %all-to-all-done.3 = f32[8,8,64,128]{3,2,1,0:T(8,128)S(1)} async-done(((f32[8,8,64,128]{3,2,1,0:T(8,128)}), f32[8,8,64,128]{3,2,1,0:T(8,128)S(1)}, u32[]{:S(2)}, u32[]{:S(2)}) %all-to-all-start.3) | async-done | bytes 2097184 | tf_op jit(solution)/shard_map/all_to_all | solution.py:13
  169.0 0.8 copy.81
  169.8 0.8 copy.82
  170.6 29.9 %reduce-scatter.7.cloned.1.call-done = f32[64,128]{1,0:T(8,128)} async-done(((f32[512,128]{1,0:T(8,128)}), f32[64,128]{1,0:T(8,128)}) %reduce-scatter.7.cloned.1.call-update) | async-done | bytes 32784
  (68 shorter events, 11.3 us)
Async XLA Ops:
  9.4 28.5 %all-to-all-start = ((s32[64,1,1]{2,1,0:T(1,128)}), s32[64,1,1]{2,1,0:T(1,128)S(1)}, u32[]{:S(2)}, u32[]{:S(2)}) async-start(s32[64,1,1]{2,1,0:T(1,128)} %copy.68), calls=%async_computation | async-start | bytes 65536 | tf_op jit(solution)/shard_map/all_to_all | solution.py:44
  40.3 2.0 copy-start.7
  41.1 7.5 %copy-start.2 = (bf16[512,128]{1,0:T(8,128)(2,1)S(1)}, bf16[512,128]{1,0:T(8,128)(2,1)}, u32[]{:S(2)}) copy-start(bf16[512,128]{1,0:T(8,128)(2,1)} %param.9) | copy-start | bytes 393220
  41.1 8.0 %copy-start.3 = (bf16[512,128]{1,0:T(8,128)(2,1)S(1)}, bf16[512,128]{1,0:T(8,128)(2,1)}, u32[]{:S(2)}) copy-start(bf16[512,128]{1,0:T(8,128)(2,1)} %param.13) | copy-start | bytes 393220
  42.3 7.8 %copy-start.4 = (bf16[512,128]{1,0:T(8,128)(2,1)S(1)}, bf16[512,128]{1,0:T(8,128)(2,1)}, u32[]{:S(2)}) copy-start(bf16[512,128]{1,0:T(8,128)(2,1)} %param.12) | copy-start | bytes 393220
  42.3 33.5 %all-to-all-start.1 = ((bf16[64,64,128]{2,1,0:T(8,128)(2,1)}), bf16[64,64,128]{2,1,0:T(8,128)(2,1)S(1)}, u32[]{:S(2)}, u32[]{:S(2)}) async-start(bf16[64,64,128]{2,1,0:T(8,128)(2,1)} %broadcast_select_fusion.1), calls=%async_computation.1 | async-start | bytes 2097152 | tf_op jit(solution)/shard_map/all_to_all | solution.py:51
  47.1 4.1 %copy-start.6 = (f32[512,2]{0,1:T(2,128)S(1)}, f32[512,2]{0,1:T(2,128)}, u32[]{:S(2)}) copy-start(f32[512,2]{0,1:T(2,128)} %param.14) | copy-start | bytes 12292
  47.1 113.1 %reduce-scatter.5.cloned.1.call-start = ((), (), s32[]{:S(2)}) async-start(), calls=%async_computation.6 | async-start | bytes 2359296 | tf_op jit(solution)/shard_map/reduce_scatter | solution.py:22
  81.4 1.0 copy-start
  81.4 1.1 copy-start.1
  81.4 1.1 copy-start.5
  99.8 0.7 copy-start.9
  99.8 0.7 copy-start.10
  101.3 34.6 %copy-start.8 = (s32[64]{0:T(128)S(1)}, s32[64]{0:T(128)}, u32[]{:S(2)}) copy-start(s32[64]{0:T(128)} %copy-done.7) | copy-start | bytes 772
  138.2 30.5 %all-to-all-start.3 = ((f32[8,8,64,128]{3,2,1,0:T(8,128)}), f32[8,8,64,128]{3,2,1,0:T(8,128)S(1)}, u32[]{:S(2)}, u32[]{:S(2)}) async-start(f32[8,8,64,128]{3,2,1,0:T(8,128)} %broadcast_in_dim.80), calls=%async_computation.3 | async-start | bytes 4194304 | tf_op jit(solution)/shard_map/all_to_all | solution.py:13
  143.0 57.5 %reduce-scatter.7.cloned.1.call-start = ((), (), s32[]{:S(2)}) async-start(), calls=%async_computation.7 | async-start | bytes 294912
Sparse Core Ops, SparseCore 0:
  100.0 60.1 reduce-scatter.4
  163.6 36.8 reduce-scatter.6
where the time goes:
time: 208 us; the launch traced here: 207 us
  waiting for transfers between devices  84.6 us (41%)
  blocking collectives  34.3 us (16%)
  starting transfers between devices  26.4 us (13%)
  local copies, waits for them, and re-layouts  24.3 us (12%)
  between operations  14.3 us (7%)
  matrix products  12.2 us (6%)
  other arithmetic  11.2 us (5%)
    all_to_all x1, blocking collectives, shards(): lax.all_to_all(sent_back, KV, split_axis=0, concat_axis=0, tiled=True)  34.3 us
    unnamed x3, waiting for transfers between devices  29.9 us
    all_to_all x1, waiting for transfers between devices, shards(): lax.all_to_all(outgoing, KV, split_axis=0, concat_axis=0, tiled=True)  21.6 us
    reduce_scatter x1, waiting for transfers between devices, summed_rows(): running = lax.psum_scatter(running, axis, scatter_dimension=0, tiled=True)  17.2 us
    all_to_all x1, starting transfers between devices, shards(): lax.all_to_all(wanted.reshape(peer_count, 1), KV, split_axis=0, concat_ax...  16.6 us
    all_to_all x1, waiting for transfers between devices, shards(): lax.all_to_all(wanted.reshape(peer_count, 1), KV, split_axis=0, concat_ax...  9.9 us
    unnamed x30, local copies, waits for them, and re-layouts  7.44 us
    all_to_all x1, waiting for transfers between devices, from_everyone(): return lax.all_to_all(copies, axis, split_axis=0, concat_axis=0, tiled=True)  5.97 us
  transfers between devices with their start and end apart: 5, of which 5 were waited for; matrix products, arithmetic and copies ran while one was open for 8% of the time, Pallas kernels for 0%

commit v1 on v0

v1 whole, which is shorter than its diff:
```python
import jax
import jax.numpy as jnp
from jax import lax
from jax.experimental import pallas as pl
from jax.experimental.pallas import tpu as pltpu
from jax.sharding import Mesh
from jax.sharding import PartitionSpec as P


BLOCK = 64
BLOCKS = 8
SLOTS = 16
PEERS = 64
ROWS = 8
TOK = 512
LANES = 128
SCALE = 0.125
KV = ("z", "y")
FAR = 1 << 20
F32 = jnp.float32
BF16 = jnp.bfloat16
VMEM = pl.BlockSpec(memory_space=pltpu.VMEM)
SMEM = pl.BlockSpec(memory_space=pltpu.SMEM)


def low_lanes(shape):
    return lax.broadcasted_iota(jnp.int32, shape, len(shape) - 1) < LANES // 2


def wanted_kernel(rank_ref, chosen_ref, out_ref):
    rank = rank_ref[0]
    peer = lax.broadcasted_iota(jnp.int32, (PEERS, SLOTS), 0)
    best = jnp.zeros((PEERS, SLOTS), jnp.int32)
    for j in range(BLOCKS):
        c = chosen_ref[j : j + 1, :]
        hit = ((c >> 3) == peer) & (c >= 0) & (peer != rank)
        best = jnp.maximum(best, jnp.where(hit, (c & 7) + 1, 0))
    best = jnp.max(best, axis=1, keepdims=True)
    out_ref[...] = jnp.broadcast_to(best, (PEERS, LANES))


def pick_kernel(asked_ref, piece_ref, out_ref):
    pieces = [piece_ref[b].astype(F32) for b in range(BLOCKS)]
    for s in range(PEERS):
        want = jnp.broadcast_to(asked_ref[s : s + 1, :], (ROWS, LANES))
        got = jnp.zeros((ROWS, LANES), F32)
        for b in range(BLOCKS):
            got = jnp.where(want == b + 1, pieces[b], got)
        out_ref[s] = got.astype(BF16)


def attend_kernel(
    slot_ref,
    rel_ref,
    fetched_ref,
    piece_ref,
    q0,
    q1,
    q2,
    q3,
    qp_ref,
    stats_ref,
    away_ref,
    own_ref,
    gq_own_ref,
    gq_far_ref,
    keys_tab,
    vals_tab,
    acc,
):
    def fill(src, at, count):
        kv = src[...].astype(F32)
        turned = pltpu.roll(kv, LANES // 2, 2)
        low = low_lanes(kv.shape)
        keys_tab[at : at + count] = jnp.where(low, kv, turned)
        vals_tab[at : at + count] = jnp.where(low, turned, kv)

    fill(fetched_ref, 0, PEERS)
    fill(piece_ref, PEERS, BLOCKS)
    acc[...] = jnp.zeros(acc.shape, F32)
    near = (q0, q1, q2, q3)
    low = low_lanes((LANES, LANES))
    row8 = lax.broadcasted_iota(jnp.int32, (ROWS, LANES), 0)
    query_t = lax.broadcasted_iota(jnp.int32, (LANES, LANES), 1) & (BLOCK - 1)

    def one_block(j, carry):
        slots = [slot_ref[j, s] for s in range(SLOTS)]
        kk = jnp.concatenate([keys_tab[i] for i in slots], axis=0)
        vv = jnp.concatenate([vals_tab[i] for i in slots], axis=0)
        k2 = jnp.concatenate([jnp.where(low, kk, 0.0), jnp.where(low, 0.0, kk)], axis=0).astype(BF16)
        v2 = jnp.concatenate([jnp.where(low, vv, 0.0), jnp.where(low, 0.0, vv)], axis=0).astype(BF16)
        at = pl.multiple_of(j * BLOCK, BLOCK)
        q = jnp.concatenate(
            [r[pl.ds(at, BLOCK), :] for r in near]
            + [qp_ref[k, pl.ds(at, BLOCK), :] for k in range(4)],
            axis=0,
        )
        g = jnp.concatenate(
            [r[pl.ds(TOK + at, BLOCK), :] for r in near]
            + [qp_ref[k, pl.ds(TOK + at, BLOCK), :] for k in range(4)],
            axis=0,
        )
        last = (((1,), (1,)), ((), ()))
        scores = lax.dot_general(k2, q, last, preferred_element_type=F32)
        dprobs = lax.dot_general(v2, g, last, preferred_element_type=F32)
        rel = jnp.concatenate([row8 + rel_ref[j, s] for s in range(SLOTS)], axis=0)
        seen = (rel <= query_t).astype(F32)
        seen = jnp.concatenate([seen] * 4, axis=1) > 0.0
        stat = stats_ref[j]
        probs = []
        dscores = []
        for h in range(2):
            s = scores[h * LANES : (h + 1) * LANES]
            d = dprobs[h * LANES : (h + 1) * LANES]
            p = jnp.where(seen, jnp.exp(s * SCALE - stat[h : h + 1, :]), 0.0)
            probs.append(p.astype(BF16))
            dscores.append((p * (d - stat[2 + h : 3 + h, :]) * SCALE).astype(BF16))
        probs = jnp.concatenate(probs, axis=0)
        dscores = jnp.concatenate(dscores, axis=0)
        plain = (((1,), (0,)), ((), ()))
        dv = lax.dot_general(probs, g, plain, preferred_element_type=F32)
        dk = lax.dot_general(dscores, q, plain, preferred_element_type=F32)
        gq = lax.dot_general(dscores, k2, (((0,), (0,)), ((), ())), preferred_element_type=F32)
        for k in range(4):
            gq_own_ref[k, pl.ds(at, BLOCK), :] = gq[k * BLOCK : (k + 1) * BLOCK]
            gq_far_ref[k, pl.ds(at, BLOCK), :] = gq[(4 + k) * BLOCK : (5 + k) * BLOCK].astype(BF16)
        both = jnp.where(low, dk[:LANES], dv[LANES:]) + pltpu.roll(
            jnp.where(low, dv[:LANES], dk[LANES:]), LANES // 2, 1
        )
        for s in range(SLOTS):
            acc[slots[s]] += both[s * ROWS : (s + 1) * ROWS]
        return carry

    lax.fori_loop(0, BLOCKS, one_block, 0)
    away_ref[...] = acc[:PEERS].astype(BF16)
    own_ref[...] = acc[PEERS:]


def settle_kernel(asked_ref, returned_ref, own_ref, out_ref):
    totals = [own_ref[b] for b in range(BLOCKS)]
    for s in range(PEERS):
        want = jnp.broadcast_to(asked_ref[s : s + 1, :], (ROWS, LANES))
        got = returned_ref[s].astype(F32)
        for b in range(BLOCKS):
            totals[b] = totals[b] + jnp.where(want == b + 1, got, 0.0)
    for b in range(BLOCKS):
        out_ref[b] = totals[b]


def place_kernel(at_ref, near_ref, far_ref, keys_ref, vals_ref):
    x = at_ref[0]
    c = at_ref[1]
    for xa in range(4):
        k = (x + 4 - xa) & 3
        for ca in range(2):
            mine = (c == ca).astype(F32)
            for b in range(BLOCKS):
                piece = near_ref[k, b] * mine + far_ref[k, b] * (1.0 - mine)
                at = b * BLOCK + (xa * 2 + ca) * ROWS
                keys_ref[at : at + ROWS, :] = piece[:, : LANES // 2]
                vals_ref[at : at + ROWS, :] = piece[:, LANES // 2 :]


def call(kernel, ins, out_shape, args, flops, **kw):
    many = isinstance(out_shape, (list, tuple))
    return pl.pallas_call(
        kernel,
        in_specs=ins,
        out_specs=[VMEM] * len(out_shape) if many else VMEM,
        out_shape=out_shape,
        cost_estimate=pl.CostEstimate(flops=flops, bytes_accessed=1 << 20, transcendentals=0),
        **kw,
    )(*args)


def sds(shape, dtype):
    return jax.ShapeDtypeStruct(shape, dtype)


def x_from(arr, k):
    return lax.ppermute(arr, "x", [(i, (i + k) % 4) for i in range(4)])


def x_back(arr, k):
    return lax.ppermute(arr, "x", [((i + k) % 4, i) for i in range(4)])


def swap(arr):
    return lax.ppermute(arr, "c", [(0, 1), (1, 0)])


def exchange(arr):
    return lax.all_to_all(arr, KV, split_axis=0, concat_axis=0, tiled=True)


def step(normed, queries, keys, values, attended, cotangent, log_sum, chosen):
    rank = lax.axis_index(KV).astype(jnp.int32)
    x = lax.axis_index("x").astype(jnp.int32)
    c = lax.axis_index("c").astype(jnp.int32)
    tp = x * 2 + c
    wanted = call(
        wanted_kernel,
        [SMEM, VMEM],
        sds((PEERS, LANES), jnp.int32),
        (rank.reshape(1), chosen),
        1 << 18,
        name="wanted",
    )
    asked = exchange(wanted)
    pairs = jnp.concatenate([keys, values], axis=1).reshape(BLOCKS, 8, ROWS, 2 * 64)
    piece = lax.dynamic_index_in_dim(pairs, tp, axis=1, keepdims=False)
    picked = call(
        pick_kernel,
        [VMEM, VMEM],
        sds((PEERS, ROWS, LANES), BF16),
        (asked, piece),
        1 << 20,
        name="pick",
    )
    fetched = exchange(picked)

    qd = jnp.concatenate([queries, cotangent], axis=0)
    deltas = jnp.sum(
        (cotangent.astype(F32) * attended.astype(F32)).reshape(TOK, 2, 64), axis=-1
    )
    stats = jnp.concatenate([log_sum.T, deltas.T], axis=0)
    qds = [qd] + [x_from(qd, k) for k in (1, 2, 3)]
    sts = [stats] + [x_from(stats, k) for k in (1, 2, 3)]
    st4 = jnp.stack(sts)
    qd_far = swap(jnp.stack(qds))
    st_far = swap(st4)
    all_stats = jnp.concatenate([st4, st_far], axis=0)
    all_stats = all_stats.reshape(8, 4, BLOCKS, BLOCK).transpose(2, 1, 0, 3).reshape(BLOCKS, 4, TOK)

    owner = chosen >> 3
    slot = jnp.where(chosen < 0, 0, jnp.where(owner == rank, PEERS + (chosen & 7), owner))
    starts = rank * TOK + jnp.arange(BLOCKS, dtype=jnp.int32)[:, None] * BLOCK
    rel = jnp.where(chosen < 0, FAR, chosen * BLOCK + ROWS * tp - starts)

    away, own, gq_own, gq_far = call(
        attend_kernel,
        [SMEM, SMEM] + [VMEM] * 8,
        [
            sds((PEERS, ROWS, LANES), BF16),
            sds((BLOCKS, ROWS, LANES), F32),
            sds((4, TOK, LANES), F32),
            sds((4, TOK, LANES), BF16),
        ],
        (slot, rel, fetched, piece, *qds, qd_far, all_stats),
        1 << 30,
        scratch_shapes=[pltpu.VMEM((PEERS + BLOCKS, ROWS, LANES), F32)] * 3,
        name="attend",
    )
    returned = exchange(away)
    gq4 = gq_own + swap(gq_far).astype(F32)
    gq = gq4[0]
    for k in (1, 2, 3):
        gq = gq + x_back(gq4[k].astype(BF16), k).astype(F32)
    grad_queries = gq.astype(BF16)
    part = lax.dot_general(
        normed, grad_queries, (((0,), (0,)), ((), ())), preferred_element_type=F32
    ).astype(BF16)
    parts = exchange(part.reshape(PEERS, 64, LANES))
    weight_grad = jnp.sum(parts.astype(F32), axis=0)

    total = call(
        settle_kernel,
        [VMEM] * 3,
        sds((BLOCKS, ROWS, LANES), F32),
        (asked, returned, own),
        1 << 20,
        name="settle",
    )
    near = jnp.stack([total] + [x_from(total, k) for k in (1, 2, 3)])
    far = swap(near)
    grad_keys, grad_values = call(
        place_kernel,
        [SMEM, VMEM, VMEM],
        [sds((TOK, 64), F32), sds((TOK, 64), F32)],
        (jnp.stack([x, c]), near, far),
        1 << 20,
        name="place",
    )
    return grad_queries, grad_keys, grad_values, weight_grad


def solution(mesh):
    torus = Mesh(mesh.devices.reshape(8, 8, 4, 2), ("z", "y", "x", "c"))
    heads = ("x", "c")
    in_specs = (
        P(KV, None),
        P(KV, heads),
        P(KV, None),
        P(KV, None),
        P(KV, heads),
        P(KV, heads),
        P(KV, heads),
        P(KV, None),
    )
    out_specs = (P(KV, heads), P(KV, None), P(KV, None), P(KV, heads))
    return jax.shard_map(step, mesh=torus, in_specs=in_specs, out_specs=out_specs, check_vma=False)
```

time: 208 us -> 165 us (0.79)
  the two profiles are of different devices: /device:TPU:2 before, /device:TPU:8 now
where the time goes in v1:
time: 165 us; the launch traced here: 164 us
  starting transfers between devices  78.7 us (48%)
  waiting for transfers between devices  46.3 us (28%)
  local copies, waits for them, and re-layouts  14.9 us (9%)
  Pallas kernels  14.8 us (9%)
  other arithmetic  5.25 us (3%)
  matrix products  2.98 us (2%)
    all_to_all x4, starting transfers between devices, exchange(): return lax.all_to_all(arr, KV, split_axis=0, concat_axis=0, tiled=True)  32.9 us
    all_to_all x4, waiting for transfers between devices, exchange(): return lax.all_to_all(arr, KV, split_axis=0, concat_axis=0, tiled=True)  26.9 us
    ppermute x9, starting transfers between devices, x_from(): return lax.ppermute(arr, 'x', [(i, (i + k) % 4) for i in range(4)])  26.5 us
    ppermute x9, waiting for transfers between devices, x_from(): return lax.ppermute(arr, 'x', [(i, (i + k) % 4) for i in range(4)])  16.6 us
    pallas_call x5, Pallas kernels, call(): pl.pallas_call(kernel, in_specs=ins, out_specs=[VMEM] * len(out_shape) if...  14.8 us
    ppermute x3, starting transfers between devices, x_back(): return lax.ppermute(arr, 'x', [((i + k) % 4, i) for i in range(4)])  11.6 us
    unnamed x31, local copies, waits for them, and re-layouts  10.6 us
    ppermute x4, starting transfers between devices, swap(): return lax.ppermute(arr, 'c', [(0, 1), (1, 0)])  7.67 us
  transfers between devices with their start and end apart: 20, of which 12 were waited for; matrix products, arithmetic and copies ran while one was open for 10% of the time, Pallas kernels for 4%

profile of v1, /device:TPU:8, one launch (start us, length us, event | category | flops | bytes accessed | tf_op | source)
XLA Modules:
  0.0 163.9 jit_solution(13571428095848846791)
XLA Ops:
  2.5 4.7 %collective-permute-start.2 = (bf16[1024,128]{1,0:T(8,128)(2,1)S(1)}, bf16[1024,128]{1,0:T(8,128)(2,1)S(1)}, u32[]{:S(2)}, u32[]{:S(2)}) collective-permute-start(bf16[1024,128]{1,0:T(8,128)(2,1)S(1)} %constant_dynamic-update-slice_fusion.q0), channel_id=1, source_target_pairs={{0,6},{2,0},{4,2},{6,4},{1,7},{3,1},{5,3},{7,5},{8,14},{10,8},{12,... | collective-permute-start | bytes 786440 | tf_op jit(solution)/shard_map/ppermute | solution.py:181
  7.2 2.7 %collective-permute-start.1 = (bf16[1024,128]{1,0:T(8,128)(2,1)S(1)}, bf16[1024,128]{1,0:T(8,128)(2,1)S(1)}, u32[]{:S(2)}, u32[]{:S(2)}) collective-permute-start(bf16[1024,128]{1,0:T(8,128)(2,1)S(1)} %constant_dynamic-update-slice_fusion.q0), channel_id=1, source_target_pairs={{0,4},{2,6},{4,0},{6,2},{1,5},{3,7},{5,1},{7,3},{8,12},{10,14},{12... | collective-permute-start | bytes 786440 | tf_op jit(solution)/shard_map/ppermute | solution.py:181
  9.9 2.8 %collective-permute-start = (bf16[1024,128]{1,0:T(8,128)(2,1)S(1)}, bf16[1024,128]{1,0:T(8,128)(2,1)S(1)}, u32[]{:S(2)}, u32[]{:S(2)}) collective-permute-start(bf16[1024,128]{1,0:T(8,128)(2,1)S(1)} %constant_dynamic-update-slice_fusion.q0), channel_id=1, source_target_pairs={{0,2},{2,4},{4,6},{6,0},{1,3},{3,5},{5,7},{7,1},{8,10},{10,12},{12... | collective-permute-start | bytes 786440 | tf_op jit(solution)/shard_map/ppermute | solution.py:181
  12.7 5.7 %collective-permute-done.2.q3 = bf16[1024,128]{1,0:T(8,128)(2,1)S(1)} collective-permute-done((bf16[1024,128]{1,0:T(8,128)(2,1)S(1)}, bf16[1024,128]{1,0:T(8,128)(2,1)S(1)}, u32[]{:S(2)}, u32[]{:S(2)}) %collective-permute-start.2) | collective-permute-done | bytes 262176 | tf_op jit(solution)/shard_map/ppermute | solution.py:181
  19.8 4.2 %collective-permute-done.q1 = bf16[1024,128]{1,0:T(8,128)(2,1)S(1)} collective-permute-done((bf16[1024,128]{1,0:T(8,128)(2,1)S(1)}, bf16[1024,128]{1,0:T(8,128)(2,1)S(1)}, u32[]{:S(2)}, u32[]{:S(2)}) %collective-permute-start) | collective-permute-done | bytes 262176 | tf_op jit(solution)/shard_map/ppermute | solution.py:181
  24.1 1.9 %collective-permute-start.3 = (bf16[4,1024,128]{2,1,0:T(8,128)(2,1)S(1)}, bf16[4,1024,128]{2,1,0:T(8,128)(2,1)S(1)}, u32[]{:S(2)}, u32[]{:S(2)}) collective-permute-start(bf16[4,1024,128]{2,1,0:T(8,128)(2,1)S(1)} %pad_maximum_fusion), channel_id=1, source_target_pairs={{0,1},{1,0},{2,3},{3,2},{4,5},{5,4},{6,7},{7,6},{8,9},{9,8},{10,11... | collective-permute-start | bytes 3145736 | tf_op jit(solution)/shard_map/ppermute | solution.py:189
  28.8 2.5 %collective-permute-start.6 = (f32[4,512]{1,0:T(4,128)S(1)}, f32[4,512]{1,0:T(4,128)S(1)}, u32[]{:S(2)}, u32[]{:S(2)}) collective-permute-start(f32[4,512]{1,0:T(4,128)S(1)} %get-tuple-element.34), channel_id=1, source_target_pairs={{0,6},{2,0},{4,2},{6,4},{1,7},{3,1},{5,3},{7,5},{8,14},{10,8},{12,... | collective-permute-start | bytes 24584 | tf_op jit(solution)/shard_map/ppermute | solution.py:181
  31.3 2.7 %collective-permute-start.5 = (f32[4,512]{1,0:T(4,128)S(1)}, f32[4,512]{1,0:T(4,128)S(1)}, u32[]{:S(2)}, u32[]{:S(2)}) collective-permute-start(f32[4,512]{1,0:T(4,128)S(1)} %get-tuple-element.34), channel_id=1, source_target_pairs={{0,4},{2,6},{4,0},{6,2},{1,5},{3,7},{5,1},{7,3},{8,12},{10,14},{12... | collective-permute-start | bytes 24584 | tf_op jit(solution)/shard_map/ppermute | solution.py:181
  34.0 2.8 %collective-permute-start.4 = (f32[4,512]{1,0:T(4,128)S(1)}, f32[4,512]{1,0:T(4,128)S(1)}, u32[]{:S(2)}, u32[]{:S(2)}) collective-permute-start(f32[4,512]{1,0:T(4,128)S(1)} %get-tuple-element.34), channel_id=1, source_target_pairs={{0,2},{2,4},{4,6},{6,0},{1,3},{3,5},{5,7},{7,1},{8,10},{10,12},{12... | collective-permute-start | bytes 24584 | tf_op jit(solution)/shard_map/ppermute | solution.py:181
  38.3 16.6 %all-to-all-start = ((s32[64,1,128]{2,1,0:T(1,128)}), s32[64,1,128]{2,1,0:T(1,128)S(1)}, u32[]{:S(2)}, u32[]{:S(2)}) async-start(s32[64,1,128]{2,1,0:T(1,128)} %bitcast.59), calls=%async_computation | async-start | bytes 65536 | tf_op jit(solution)/shard_map/all_to_all | solution.py:193
  57.6 8.3 %all-to-all-done = s32[64,1,128]{2,1,0:T(1,128)S(1)} async-done(((s32[64,1,128]{2,1,0:T(1,128)}), s32[64,1,128]{2,1,0:T(1,128)S(1)}, u32[]{:S(2)}, u32[]{:S(2)}) %all-to-all-start) | async-done | bytes 32800 | tf_op jit(solution)/shard_map/all_to_all | solution.py:193
  68.0 5.5 %all-to-all-start.1 = ((bf16[64,8,128]{2,1,0:T(8,128)(2,1)}), bf16[64,8,128]{2,1,0:T(8,128)(2,1)S(1)}, u32[]{:S(2)}, u32[]{:S(2)}) async-start(bf16[64,8,128]{2,1,0:T(8,128)(2,1)} %pick.1), calls=%async_computation.1 | async-start | bytes 262144 | tf_op jit(solution)/shard_map/all_to_all | solution.py:193
  73.6 1.9 %collective-permute-start.7 = (f32[4,4,512]{2,1,0:T(4,128)S(1)}, f32[4,4,512]{2,1,0:T(4,128)S(1)}, u32[]{:S(2)}, u32[]{:S(2)}) collective-permute-start(f32[4,4,512]{2,1,0:T(4,128)S(1)} %pad_maximum_fusion.3), channel_id=1, source_target_pairs={{0,1},{1,0},{2,3},{3,2},{4,5},{5,4},{6,7},{7,6},{8,9},{9,8},{10,11... | collective-permute-start | bytes 98312 | tf_op jit(solution)/shard_map/ppermute | solution.py:189
  77.7 7.9 %all-to-all-done.1.fetched_ref = bf16[64,8,128]{2,1,0:T(8,128)(2,1)S(1)} async-done(((bf16[64,8,128]{2,1,0:T(8,128)(2,1)}), bf16[64,8,128]{2,1,0:T(8,128)(2,1)S(1)}, u32[]{:S(2)}, u32[]{:S(2)}) %all-to-all-start.1) | async-done | bytes 131104 | tf_op jit(solution)/shard_map/all_to_all | solution.py:193
  86.6 8.1 %attend.1 = (bf16[64,8,128]{2,1,0:T(8,128)(2,1)}, f32[8,8,128]{2,1,0:T(8,128)}, f32[4,512,128]{2,1,0:T(8,128)}, bf16[4,512,128]{2,1,0:T(8,128)(2,1)}) custom-call(s32[8,16]{1,0:T(8,128)} %get-tuple-element.36.slot_ref, s32[8,16]{1,0:T(8,128)} %get-tuple-element.35.rel_ref, bf16[64,8,128]{2,1,0:T(8,128)(2,1)} %copy-done.8, ...), custom_call_target="tpu_custom_call" | custom-call | flops 1073741824 | bytes 1048576 | tf_op jit(solution)/shard_map/attend/pallas_call | solution.py:166
  94.7 1.9 %collective-permute-start.8 = (bf16[4,512,128]{2,1,0:T(8,128)(2,1)}, bf16[4,512,128]{2,1,0:T(8,128)(2,1)S(1)}, u32[]{:S(2)}, u32[]{:S(2)}) collective-permute-start(bf16[4,512,128]{2,1,0:T(8,128)(2,1)} %get-tuple-element.11), channel_id=1, source_target_pairs={{0,1},{1,0},{2,3},{3,2},{4,5},{5,4},{6,7},{7,6},{8,9},{9,8},{10,11... | collective-permute-start | bytes 1572872 | tf_op jit(solution)/shard_map/ppermute | solution.py:189
  96.6 2.1 %collective-permute-done.8 = bf16[4,512,128]{2,1,0:T(8,128)(2,1)S(1)} collective-permute-done((bf16[4,512,128]{2,1,0:T(8,128)(2,1)}, bf16[4,512,128]{2,1,0:T(8,128)(2,1)S(1)}, u32[]{:S(2)}, u32[]{:S(2)}) %collective-permute-start.8) | collective-permute-done | bytes 524320 | tf_op jit(solution)/shard_map/ppermute | solution.py:189
  100.1 4.4 %collective-permute-start.9 = (bf16[512,128]{1,0:T(8,128)(2,1)S(1)}, bf16[512,128]{1,0:T(8,128)(2,1)S(1)}, u32[]{:S(2)}, u32[]{:S(2)}) collective-permute-start(bf16[512,128]{1,0:T(8,128)(2,1)S(1)} %get-tuple-element.30), channel_id=1, source_target_pairs={{2,0},{4,2},{6,4},{0,6},{3,1},{5,3},{7,5},{1,7},{10,8},{12,10},{14... | collective-permute-start | bytes 393224 | tf_op jit(solution)/shard_map/ppermute | solution.py:185
  104.5 1.9 %collective-permute-start.11 = (bf16[512,128]{1,0:T(8,128)(2,1)S(1)}, bf16[512,128]{1,0:T(8,128)(2,1)S(1)}, u32[]{:S(2)}, u32[]{:S(2)}) collective-permute-start(bf16[512,128]{1,0:T(8,128)(2,1)S(1)} %get-tuple-element.31), channel_id=1, source_target_pairs={{6,0},{0,2},{2,4},{4,6},{7,1},{1,3},{3,5},{5,7},{14,8},{8,10},{10,... | collective-permute-start | bytes 393224 | tf_op jit(solution)/shard_map/ppermute | solution.py:185
  106.4 5.3 %collective-permute-start.10 = (bf16[512,128]{1,0:T(8,128)(2,1)S(1)}, bf16[512,128]{1,0:T(8,128)(2,1)S(1)}, u32[]{:S(2)}, u32[]{:S(2)}) collective-permute-start(bf16[512,128]{1,0:T(8,128)(2,1)S(1)} %get-tuple-element.32), channel_id=1, source_target_pairs={{4,0},{6,2},{0,4},{2,6},{5,1},{7,3},{1,5},{3,7},{12,8},{14,10},{8,... | collective-permute-start | bytes 393224 | tf_op jit(solution)/shard_map/ppermute | solution.py:185
  111.7 5.4 %all-to-all-start.2 = ((bf16[64,8,128]{2,1,0:T(8,128)(2,1)}), bf16[64,8,128]{2,1,0:T(8,128)(2,1)S(1)}, u32[]{:S(2)}, u32[]{:S(2)}) async-start(bf16[64,8,128]{2,1,0:T(8,128)(2,1)} %get-tuple-element.12), calls=%async_computation.2 | async-start | bytes 262144 | tf_op jit(solution)/shard_map/all_to_all | solution.py:193
  117.3 3.0 %fusion = bf16[4096,128]{0,1:T(8,128)(2,1)S(1)} fusion(bf16[512,128]{1,0:T(8,128)(2,1)S(1)} %fusion.4, bf16[512,4096]{1,0:T(8,128)(2,1)} %param.8), kind=kOutput, calls=%fused_computation.1 | convolution fusion | flops 537395200 | bytes 5373952 | tf_op jit(solution)/shard_map/dot_general | solution.py:260
  121.6 7.6 %all-to-all-done.2.returned_ref = bf16[64,8,128]{2,1,0:T(8,128)(2,1)S(1)} async-done(((bf16[64,8,128]{2,1,0:T(8,128)(2,1)}), bf16[64,8,128]{2,1,0:T(8,128)(2,1)S(1)}, u32[]{:S(2)}, u32[]{:S(2)}) %all-to-all-start.2) | async-done | bytes 131104 | tf_op jit(solution)/shard_map/all_to_all | solution.py:193
  129.2 5.4 %all-to-all-start.3 = ((bf16[64,64,128]{2,1,0:T(8,128)(2,1)}), bf16[64,64,128]{2,1,0:T(8,128)(2,1)S(1)}, u32[]{:S(2)}, u32[]{:S(2)}) async-start(bf16[64,64,128]{2,1,0:T(8,128)(2,1)} %bitcast.29), calls=%async_computation.3 | async-start | bytes 2097152 | tf_op jit(solution)/shard_map/all_to_all | solution.py:193
  134.6 1.8 %settle.1 = f32[8,8,128]{2,1,0:T(8,128)} custom-call(s32[64,128]{1,0:T(8,128)} %bitcast.54, bf16[64,8,128]{2,1,0:T(8,128)(2,1)} %copy-done.1, f32[8,8,128]{2,1,0:T(8,128)} %get-tuple-element.13.own_ref), custom_call_target="tpu_custom_call" | custom-call | flops 1048576 | bytes 1048576 | tf_op jit(solution)/shard_map/settle/pallas_call | solution.py:166
  136.4 2.5 %collective-permute-start.14 = (f32[8,8,128]{2,1,0:T(8,128)}, f32[8,8,128]{2,1,0:T(8,128)S(1)}, u32[]{:S(2)}, u32[]{:S(2)}) collective-permute-start(f32[8,8,128]{2,1,0:T(8,128)} %settle.1), channel_id=1, source_target_pairs={{0,6},{2,0},{4,2},{6,4},{1,7},{3,1},{5,3},{7,5},{8,14},{10,8},{12,... | collective-permute-start | bytes 98312 | tf_op jit(solution)/shard_map/ppermute | solution.py:181
  138.8 4.0 %collective-permute-start.13 = (f32[8,8,128]{2,1,0:T(8,128)}, f32[8,8,128]{2,1,0:T(8,128)S(1)}, u32[]{:S(2)}, u32[]{:S(2)}) collective-permute-start(f32[8,8,128]{2,1,0:T(8,128)} %settle.1), channel_id=1, source_target_pairs={{0,4},{2,6},{4,0},{6,2},{1,5},{3,7},{5,1},{7,3},{8,12},{10,14},{12... | collective-permute-start | bytes 98312 | tf_op jit(solution)/shard_map/ppermute | solution.py:181
  142.9 1.9 %collective-permute-start.12 = (f32[8,8,128]{2,1,0:T(8,128)}, f32[8,8,128]{2,1,0:T(8,128)S(1)}, u32[]{:S(2)}, u32[]{:S(2)}) collective-permute-start(f32[8,8,128]{2,1,0:T(8,128)} %settle.1), channel_id=1, source_target_pairs={{0,2},{2,4},{4,6},{6,0},{1,3},{3,5},{5,7},{7,1},{8,10},{10,12},{12... | collective-permute-start | bytes 98312 | tf_op jit(solution)/shard_map/ppermute | solution.py:181
  146.4 3.7 %collective-permute-done.12 = f32[8,8,128]{2,1,0:T(8,128)S(1)} collective-permute-done((f32[8,8,128]{2,1,0:T(8,128)}, f32[8,8,128]{2,1,0:T(8,128)S(1)}, u32[]{:S(2)}, u32[]{:S(2)}) %collective-permute-start.12) | collective-permute-done | bytes 32800 | tf_op jit(solution)/shard_map/ppermute | solution.py:181
  150.9 1.9 %collective-permute-start.15 = (f32[4,8,8,128]{3,2,1,0:T(8,128)S(1)}, f32[4,8,8,128]{3,2,1,0:T(8,128)S(1)}, u32[]{:S(2)}, u32[]{:S(2)}) collective-permute-start(f32[4,8,8,128]{3,2,1,0:T(8,128)S(1)} %pad_maximum_fusion.2.near_ref), channel_id=1, source_target_pairs={{0,1},{1,0},{2,3},{3,2},{4,5},{5,4},{6,7},{7,6},{8,9},{9,8},{10,11... | collective-permute-start | bytes 393224 | tf_op jit(solution)/shard_map/ppermute | solution.py:189
  154.8 1.8 %place.1 = (f32[512,64]{1,0:T(8,128)}, f32[512,64]{1,0:T(8,128)}) custom-call(s32[2]{0:T(128)} %pad_add_fusion.at_ref, f32[4,8,8,128]{3,2,1,0:T(8,128)} %copy-done.2, f32[4,8,8,128]{3,2,1,0:T(8,128)} %copy-done.9), custom_call_target="tpu_custom_call" | custom-call | flops 1048576 | bytes 1048576 | tf_op jit(solution)/shard_map/place/pallas_call | solution.py:166
  160.0 3.1 %all-to-all-done.3 = bf16[64,64,128]{2,1,0:T(8,128)(2,1)S(1)} async-done(((bf16[64,64,128]{2,1,0:T(8,128)(2,1)}), bf16[64,64,128]{2,1,0:T(8,128)(2,1)S(1)}, u32[]{:S(2)}, u32[]{:S(2)}) %all-to-all-start.3) | async-done | bytes 1048608 | tf_op jit(solution)/shard_map/all_to_all | solution.py:193
  (73 shorter events, 27.0 us)
Async XLA Ops:
  0.6 74.9 %copy-start.10 = (s32[8,16]{1,0:T(8,128)S(1)}, s32[8,16]{1,0:T(8,128)}, u32[]{:S(2)}) copy-start(s32[8,16]{1,0:T(8,128)} %chosen_ref.1) | copy-start | bytes 1540
  2.5 83.1 %copy-start = (bf16[1024,128]{1,0:T(8,128)(2,1)}, bf16[1024,128]{1,0:T(8,128)(2,1)S(1)}, u32[]{:S(2)}) copy-start(bf16[1024,128]{1,0:T(8,128)(2,1)S(1)} %constant_dynamic-update-slice_fusion.q0) | copy-start | bytes 786436
  2.5 15.9 %collective-permute-start.2 = (bf16[1024,128]{1,0:T(8,128)(2,1)S(1)}, bf16[1024,128]{1,0:T(8,128)(2,1)S(1)}, u32[]{:S(2)}, u32[]{:S(2)}) collective-permute-start(bf16[1024,128]{1,0:T(8,128)(2,1)S(1)} %constant_dynamic-update-slice_fusion.q0), channel_id=1, source_target_pairs={{0,6},{2,0},{4,2},{6,4},{1,7},{3,1},{5,3},{7,5},{8,14},{10,8},{12,... | collective-permute-start | bytes 786440 | tf_op jit(solution)/shard_map/ppermute | solution.py:181
  7.2 12.6 %collective-permute-start.1 = (bf16[1024,128]{1,0:T(8,128)(2,1)S(1)}, bf16[1024,128]{1,0:T(8,128)(2,1)S(1)}, u32[]{:S(2)}, u32[]{:S(2)}) collective-permute-start(bf16[1024,128]{1,0:T(8,128)(2,1)S(1)} %constant_dynamic-update-slice_fusion.q0), channel_id=1, source_target_pairs={{0,4},{2,6},{4,0},{6,2},{1,5},{3,7},{5,1},{7,3},{8,12},{10,14},{12... | collective-permute-start | bytes 786440 | tf_op jit(solution)/shard_map/ppermute | solution.py:181
  9.9 14.1 %collective-permute-start = (bf16[1024,128]{1,0:T(8,128)(2,1)S(1)}, bf16[1024,128]{1,0:T(8,128)(2,1)S(1)}, u32[]{:S(2)}, u32[]{:S(2)}) collective-permute-start(bf16[1024,128]{1,0:T(8,128)(2,1)S(1)} %constant_dynamic-update-slice_fusion.q0), channel_id=1, source_target_pairs={{0,2},{2,4},{4,6},{6,0},{1,3},{3,5},{5,7},{7,1},{8,10},{10,12},{12... | collective-permute-start | bytes 786440 | tf_op jit(solution)/shard_map/ppermute | solution.py:181
  18.4 67.2 %copy-start.5 = (bf16[1024,128]{1,0:T(8,128)(2,1)}, bf16[1024,128]{1,0:T(8,128)(2,1)S(1)}, u32[]{:S(2)}) copy-start(bf16[1024,128]{1,0:T(8,128)(2,1)S(1)} %collective-permute-done.2.q3) | copy-start | bytes 786436
  19.8 65.8 %copy-start.6 = (bf16[1024,128]{1,0:T(8,128)(2,1)}, bf16[1024,128]{1,0:T(8,128)(2,1)S(1)}, u32[]{:S(2)}) copy-start(bf16[1024,128]{1,0:T(8,128)(2,1)S(1)} %collective-permute-done.1.q2) | copy-start | bytes 786436
  24.0 61.6 %copy-start.7 = (bf16[1024,128]{1,0:T(8,128)(2,1)}, bf16[1024,128]{1,0:T(8,128)(2,1)S(1)}, u32[]{:S(2)}) copy-start(bf16[1024,128]{1,0:T(8,128)(2,1)S(1)} %collective-permute-done.q1) | copy-start | bytes 786436
  24.1 61.4 %collective-permute-start.3 = (bf16[4,1024,128]{2,1,0:T(8,128)(2,1)S(1)}, bf16[4,1024,128]{2,1,0:T(8,128)(2,1)S(1)}, u32[]{:S(2)}, u32[]{:S(2)}) collective-permute-start(bf16[4,1024,128]{2,1,0:T(8,128)(2,1)S(1)} %pad_maximum_fusion), channel_id=1, source_target_pairs={{0,1},{1,0},{2,3},{3,2},{4,5},{5,4},{6,7},{7,6},{8,9},{9,8},{10,11... | collective-permute-start | bytes 3145736 | tf_op jit(solution)/shard_map/ppermute | solution.py:189
  28.8 44.7 %collective-permute-start.6 = (f32[4,512]{1,0:T(4,128)S(1)}, f32[4,512]{1,0:T(4,128)S(1)}, u32[]{:S(2)}, u32[]{:S(2)}) collective-permute-start(f32[4,512]{1,0:T(4,128)S(1)} %get-tuple-element.34), channel_id=1, source_target_pairs={{0,6},{2,0},{4,2},{6,4},{1,7},{3,1},{5,3},{7,5},{8,14},{10,8},{12,... | collective-permute-start | bytes 24584 | tf_op jit(solution)/shard_map/ppermute | solution.py:181
  31.3 42.2 %collective-permute-start.5 = (f32[4,512]{1,0:T(4,128)S(1)}, f32[4,512]{1,0:T(4,128)S(1)}, u32[]{:S(2)}, u32[]{:S(2)}) collective-permute-start(f32[4,512]{1,0:T(4,128)S(1)} %get-tuple-element.34), channel_id=1, source_target_pairs={{0,4},{2,6},{4,0},{6,2},{1,5},{3,7},{5,1},{7,3},{8,12},{10,14},{12... | collective-permute-start | bytes 24584 | tf_op jit(solution)/shard_map/ppermute | solution.py:181
  34.0 39.6 %collective-permute-start.4 = (f32[4,512]{1,0:T(4,128)S(1)}, f32[4,512]{1,0:T(4,128)S(1)}, u32[]{:S(2)}, u32[]{:S(2)}) collective-permute-start(f32[4,512]{1,0:T(4,128)S(1)} %get-tuple-element.34), channel_id=1, source_target_pairs={{0,2},{2,4},{4,6},{6,0},{1,3},{3,5},{5,7},{7,1},{8,10},{10,12},{12... | collective-permute-start | bytes 24584 | tf_op jit(solution)/shard_map/ppermute | solution.py:181
  38.3 27.6 %all-to-all-start = ((s32[64,1,128]{2,1,0:T(1,128)}), s32[64,1,128]{2,1,0:T(1,128)S(1)}, u32[]{:S(2)}, u32[]{:S(2)}) async-start(s32[64,1,128]{2,1,0:T(1,128)} %bitcast.59), calls=%async_computation | async-start | bytes 65536 | tf_op jit(solution)/shard_map/all_to_all | solution.py:193
  65.9 0.6 copy-start.4
  68.0 17.5 %all-to-all-start.1 = ((bf16[64,8,128]{2,1,0:T(8,128)(2,1)}), bf16[64,8,128]{2,1,0:T(8,128)(2,1)S(1)}, u32[]{:S(2)}, u32[]{:S(2)}) async-start(bf16[64,8,128]{2,1,0:T(8,128)(2,1)} %pick.1), calls=%async_computation.1 | async-start | bytes 262144 | tf_op jit(solution)/shard_map/all_to_all | solution.py:193
  73.6 3.1 %collective-permute-start.7 = (f32[4,4,512]{2,1,0:T(4,128)S(1)}, f32[4,4,512]{2,1,0:T(4,128)S(1)}, u32[]{:S(2)}, u32[]{:S(2)}) collective-permute-start(f32[4,4,512]{2,1,0:T(4,128)S(1)} %pad_maximum_fusion.3), channel_id=1, source_target_pairs={{0,1},{1,0},{2,3},{3,2},{4,5},{5,4},{6,7},{7,6},{8,9},{9,8},{10,11... | collective-permute-start | bytes 98312 | tf_op jit(solution)/shard_map/ppermute | solution.py:189
  85.5 0.7 copy-start.8
  85.5 1.0 copy-start.11
  94.7 4.0 %collective-permute-start.8 = (bf16[4,512,128]{2,1,0:T(8,128)(2,1)}, bf16[4,512,128]{2,1,0:T(8,128)(2,1)S(1)}, u32[]{:S(2)}, u32[]{:S(2)}) collective-permute-start(bf16[4,512,128]{2,1,0:T(8,128)(2,1)} %get-tuple-element.11), channel_id=1, source_target_pairs={{0,1},{1,0},{2,3},{3,2},{4,5},{5,4},{6,7},{7,6},{8,9},{9,8},{10,11... | collective-permute-start | bytes 1572872 | tf_op jit(solution)/shard_map/ppermute | solution.py:189
  100.1 17.1 %collective-permute-start.9 = (bf16[512,128]{1,0:T(8,128)(2,1)S(1)}, bf16[512,128]{1,0:T(8,128)(2,1)S(1)}, u32[]{:S(2)}, u32[]{:S(2)}) collective-permute-start(bf16[512,128]{1,0:T(8,128)(2,1)S(1)} %get-tuple-element.30), channel_id=1, source_target_pairs={{2,0},{4,2},{6,4},{0,6},{3,1},{5,3},{7,5},{1,7},{10,8},{12,10},{14... | collective-permute-start | bytes 393224 | tf_op jit(solution)/shard_map/ppermute | solution.py:185
  104.5 12.7 %collective-permute-start.11 = (bf16[512,128]{1,0:T(8,128)(2,1)S(1)}, bf16[512,128]{1,0:T(8,128)(2,1)S(1)}, u32[]{:S(2)}, u32[]{:S(2)}) collective-permute-start(bf16[512,128]{1,0:T(8,128)(2,1)S(1)} %get-tuple-element.31), channel_id=1, source_target_pairs={{6,0},{0,2},{2,4},{4,6},{7,1},{1,3},{3,5},{5,7},{14,8},{8,10},{10,... | collective-permute-start | bytes 393224 | tf_op jit(solution)/shard_map/ppermute | solution.py:185
  106.4 10.8 %collective-permute-start.10 = (bf16[512,128]{1,0:T(8,128)(2,1)S(1)}, bf16[512,128]{1,0:T(8,128)(2,1)S(1)}, u32[]{:S(2)}, u32[]{:S(2)}) collective-permute-start(bf16[512,128]{1,0:T(8,128)(2,1)S(1)} %get-tuple-element.32), channel_id=1, source_target_pairs={{4,0},{6,2},{0,4},{2,6},{5,1},{7,3},{1,5},{3,7},{12,8},{14,10},{8,... | collective-permute-start | bytes 393224 | tf_op jit(solution)/shard_map/ppermute | solution.py:185
  111.7 17.5 %all-to-all-start.2 = ((bf16[64,8,128]{2,1,0:T(8,128)(2,1)}), bf16[64,8,128]{2,1,0:T(8,128)(2,1)S(1)}, u32[]{:S(2)}, u32[]{:S(2)}) async-start(bf16[64,8,128]{2,1,0:T(8,128)(2,1)} %get-tuple-element.12), calls=%async_computation.2 | async-start | bytes 262144 | tf_op jit(solution)/shard_map/all_to_all | solution.py:193
  117.3 11.9 %copy-start.3 = (bf16[512,128]{1,0:T(8,128)(2,1)}, bf16[512,128]{1,0:T(8,128)(2,1)S(1)}, u32[]{:S(2)}) copy-start(bf16[512,128]{1,0:T(8,128)(2,1)S(1)} %fusion.4) | copy-start | bytes 393220
  129.2 5.4 %copy-start.1 = (bf16[64,8,128]{2,1,0:T(8,128)(2,1)}, bf16[64,8,128]{2,1,0:T(8,128)(2,1)S(1)}, u32[]{:S(2)}) copy-start(bf16[64,8,128]{2,1,0:T(8,128)(2,1)S(1)} %all-to-all-done.2.returned_ref) | copy-start | bytes 393220
  129.2 33.9 %all-to-all-start.3 = ((bf16[64,64,128]{2,1,0:T(8,128)(2,1)}), bf16[64,64,128]{2,1,0:T(8,128)(2,1)S(1)}, u32[]{:S(2)}, u32[]{:S(2)}) async-start(bf16[64,64,128]{2,1,0:T(8,128)(2,1)} %bitcast.29), calls=%async_computation.3 | async-start | bytes 2097152 | tf_op jit(solution)/shard_map/all_to_all | solution.py:193
  136.4 8.4 %collective-permute-start.14 = (f32[8,8,128]{2,1,0:T(8,128)}, f32[8,8,128]{2,1,0:T(8,128)S(1)}, u32[]{:S(2)}, u32[]{:S(2)}) collective-permute-start(f32[8,8,128]{2,1,0:T(8,128)} %settle.1), channel_id=1, source_target_pairs={{0,6},{2,0},{4,2},{6,4},{1,7},{3,1},{5,3},{7,5},{8,14},{10,8},{12,... | collective-permute-start | bytes 98312 | tf_op jit(solution)/shard_map/ppermute | solution.py:181
  138.8 7.5 %collective-permute-start.13 = (f32[8,8,128]{2,1,0:T(8,128)}, f32[8,8,128]{2,1,0:T(8,128)S(1)}, u32[]{:S(2)}, u32[]{:S(2)}) collective-permute-start(f32[8,8,128]{2,1,0:T(8,128)} %settle.1), channel_id=1, source_target_pairs={{0,4},{2,6},{4,0},{6,2},{1,5},{3,7},{5,1},{7,3},{8,12},{10,14},{12... | collective-permute-start | bytes 98312 | tf_op jit(solution)/shard_map/ppermute | solution.py:181
  142.9 7.2 %collective-permute-start.12 = (f32[8,8,128]{2,1,0:T(8,128)}, f32[8,8,128]{2,1,0:T(8,128)S(1)}, u32[]{:S(2)}, u32[]{:S(2)}) collective-permute-start(f32[8,8,128]{2,1,0:T(8,128)} %settle.1), channel_id=1, source_target_pairs={{0,2},{2,4},{4,6},{6,0},{1,3},{3,5},{5,7},{7,1},{8,10},{10,12},{12... | collective-permute-start | bytes 98312 | tf_op jit(solution)/shard_map/ppermute | solution.py:181
  150.9 3.3 %copy-start.2 = (f32[4,8,8,128]{3,2,1,0:T(8,128)}, f32[4,8,8,128]{3,2,1,0:T(8,128)S(1)}, u32[]{:S(2)}) copy-start(f32[4,8,8,128]{3,2,1,0:T(8,128)S(1)} %pad_maximum_fusion.2.near_ref) | copy-start | bytes 393220
  150.9 3.2 %collective-permute-start.15 = (f32[4,8,8,128]{3,2,1,0:T(8,128)S(1)}, f32[4,8,8,128]{3,2,1,0:T(8,128)S(1)}, u32[]{:S(2)}, u32[]{:S(2)}) collective-permute-start(f32[4,8,8,128]{3,2,1,0:T(8,128)S(1)} %pad_maximum_fusion.2.near_ref), channel_id=1, source_target_pairs={{0,1},{1,0},{2,3},{3,2},{4,5},{5,4},{6,7},{7,6},{8,9},{9,8},{10,11... | collective-permute-start | bytes 393224 | tf_op jit(solution)/shard_map/ppermute | solution.py:189
  154.1 0.7 copy-start.9

commit v2 on v1

v2 whole, which is shorter than its diff:
```python
import jax
import jax.numpy as jnp
from jax import lax
from jax.experimental import pallas as pl
from jax.experimental.pallas import tpu as pltpu
from jax.sharding import Mesh
from jax.sharding import PartitionSpec as P


BLOCK = 64
BLOCKS = 8
SLOTS = 16
PEERS = 64
ROWS = 8
TOK = 512
LANES = 128
SCALE = 0.125
KV = ("z", "y")
FAR = 1 << 20
F32 = jnp.float32
BF16 = jnp.bfloat16
VMEM = pl.BlockSpec(memory_space=pltpu.VMEM)
SMEM = pl.BlockSpec(memory_space=pltpu.SMEM)


def low_lanes(shape):
    return lax.broadcasted_iota(jnp.int32, shape, len(shape) - 1) < LANES // 2


def offer_kernel(at_ref, keys_ref, vals_ref, chosen_ref, out_ref, pairs):
    rank = at_ref[0]
    tp = at_ref[1]
    both = jnp.concatenate([keys_ref[...], vals_ref[...]], axis=0).astype(F32)
    pairs[...] = both.T
    peer = lax.broadcasted_iota(jnp.int32, (PEERS, SLOTS), 0)
    best = jnp.zeros((PEERS, SLOTS), jnp.int32)
    for j in range(BLOCKS):
        c = chosen_ref[j : j + 1, :]
        hit = ((c >> 3) == peer) & (c >= 0) & (peer != rank)
        best = jnp.maximum(best, jnp.where(hit, (c & 7) + 1, 0))
    best = jnp.max(best, axis=1, keepdims=True)
    best = jnp.broadcast_to(best, (PEERS, LANES)).astype(F32)
    pieces = []
    for b in range(BLOCKS):
        at = pl.multiple_of(b * BLOCK + tp * ROWS, ROWS)
        pieces.append(pairs[pl.ds(at, ROWS), :].astype(BF16))
    for s in range(PEERS):
        for b in range(BLOCKS):
            out_ref[s, b] = pieces[b]
        out_ref[s, BLOCKS] = jnp.broadcast_to(best[s : s + 1], (ROWS, LANES)).astype(BF16)


def pack_kernel(q_ref, g_ref, o_ref, log_ref, out_ref):
    out_ref[0:TOK] = q_ref[...]
    out_ref[TOK : 2 * TOK] = g_ref[...]
    prod = (g_ref[...].astype(F32) * o_ref[...].astype(F32)).T
    half = LANES // 2
    stats = jnp.concatenate(
        [
            log_ref[...],
            jnp.sum(prod[:half], axis=0, keepdims=True),
            jnp.sum(prod[half:], axis=0, keepdims=True),
        ],
        axis=0,
    )
    rest = jnp.concatenate([stats[:, m * LANES : (m + 1) * LANES] for m in range(4)], axis=0)
    for n in range(3):
        part = rest.astype(BF16)
        out_ref[2 * TOK + 16 * n : 2 * TOK + 16 * (n + 1)] = part
        rest = rest - part.astype(F32)


def attend_kernel(
    src_ref,
    dst_ref,
    rel_ref,
    offered_ref,
    q0,
    q1,
    q2,
    q3,
    qp_ref,
    away_ref,
    own_ref,
    gq_own_ref,
    gq_far_ref,
    stats_tab,
    acc,
):
    near = (q0, q1, q2, q3)
    acc[...] = jnp.zeros(acc.shape, F32)
    low = low_lanes((LANES, LANES))
    low4 = low_lanes((4, LANES))
    row8 = lax.broadcasted_iota(jnp.int32, (ROWS, LANES), 0)
    query_t = lax.broadcasted_iota(jnp.int32, (LANES, LANES), 1) & (BLOCK - 1)

    def stat(p):
        parts = []
        for n in range(3):
            at = 2 * TOK + 16 * n
            parts.append((near[p][at : at + 16, :] if p < 4 else qp_ref[p - 4, at : at + 16, :]).astype(F32))
        return parts[0] + parts[1] + parts[2]

    for pair in range(4):
        even, odd = stat(2 * pair), stat(2 * pair + 1)
        even_turned = pltpu.roll(even, LANES // 2, 1)
        odd_turned = pltpu.roll(odd, LANES // 2, 1)
        for j in range(BLOCKS):
            m = 4 * (j // 2)
            lo = even[m : m + 4] if j % 2 == 0 else even_turned[m : m + 4]
            hi = odd_turned[m : m + 4] if j % 2 == 0 else odd[m : m + 4]
            stats_tab[j, 0:4, pair * LANES : (pair + 1) * LANES] = jnp.where(low4, lo, hi)

    def one_block(j, carry):
        kv = jnp.concatenate([offered_ref[src_ref[j, s]].astype(F32) for s in range(SLOTS)], axis=0)
        turned = pltpu.roll(kv, LANES // 2, 1)
        k2 = jnp.concatenate([jnp.where(low, kv, 0.0), jnp.where(low, 0.0, turned)], axis=0).astype(BF16)
        v2 = jnp.concatenate([jnp.where(low, turned, 0.0), jnp.where(low, 0.0, kv)], axis=0).astype(BF16)
        at = pl.multiple_of(j * BLOCK, BLOCK)
        q = jnp.concatenate(
            [r[pl.ds(at, BLOCK), :] for r in near]
            + [qp_ref[k, pl.ds(at, BLOCK), :] for k in range(4)],
            axis=0,
        )
        g = jnp.concatenate(
            [r[pl.ds(TOK + at, BLOCK), :] for r in near]
            + [qp_ref[k, pl.ds(TOK + at, BLOCK), :] for k in range(4)],
            axis=0,
        )
        last = (((1,), (1,)), ((), ()))
        scores = lax.dot_general(k2, q, last, preferred_element_type=F32)
        dprobs = lax.dot_general(v2, g, last, preferred_element_type=F32)
        rel = jnp.concatenate([row8 + rel_ref[j, s] for s in range(SLOTS)], axis=0)
        seen = (rel <= query_t).astype(F32)
        seen = jnp.concatenate([seen] * 4, axis=1) > 0.0
        stat_j = stats_tab[j]
        probs = []
        dscores = []
        for h in range(2):
            s = scores[h * LANES : (h + 1) * LANES]
            d = dprobs[h * LANES : (h + 1) * LANES]
            p = jnp.where(seen, jnp.exp(s * SCALE - stat_j[h : h + 1, :]), 0.0)
            probs.append(p.astype(BF16))
            dscores.append((p * (d - stat_j[2 + h : 3 + h, :]) * SCALE).astype(BF16))
        probs = jnp.concatenate(probs, axis=0)
        dscores = jnp.concatenate(dscores, axis=0)
        plain = (((1,), (0,)), ((), ()))
        dv = lax.dot_general(probs, g, plain, preferred_element_type=F32)
        dk = lax.dot_general(dscores, q, plain, preferred_element_type=F32)
        gq = lax.dot_general(dscores, k2, (((0,), (0,)), ((), ())), preferred_element_type=F32)
        for k in range(4):
            gq_own_ref[k, pl.ds(at, BLOCK), :] = gq[k * BLOCK : (k + 1) * BLOCK]
            gq_far_ref[k, pl.ds(at, BLOCK), :] = gq[(4 + k) * BLOCK : (5 + k) * BLOCK].astype(BF16)
        both = jnp.where(low, dk[:LANES], dv[LANES:]) + pltpu.roll(
            jnp.where(low, dv[:LANES], dk[LANES:]), LANES // 2, 1
        )
        for s in range(SLOTS):
            acc[dst_ref[j, s]] += both[s * ROWS : (s + 1) * ROWS]
        return carry

    lax.fori_loop(0, BLOCKS, one_block, 0)
    away_ref[...] = acc[:PEERS].astype(BF16)
    own_ref[...] = acc[PEERS:]


def settle_kernel(asked_ref, returned_ref, own_ref, out_ref):
    totals = [own_ref[b] for b in range(BLOCKS)]
    for s in range(PEERS):
        want = asked_ref[s].astype(F32)
        got = returned_ref[s].astype(F32)
        for b in range(BLOCKS):
            totals[b] = totals[b] + jnp.where(want == b + 1.0, got, 0.0)
    for b in range(BLOCKS):
        out_ref[b] = totals[b]


def place_kernel(at_ref, near_ref, far_ref, keys_ref, vals_ref, rows):
    x = at_ref[0]
    mine = jnp.full((ROWS, LANES), at_ref[1], jnp.int32)
    for xa in range(4):
        k = (x + 4 - xa) & 3
        for ca in range(2):
            for b in range(BLOCKS):
                at = b * BLOCK + (xa * 2 + ca) * ROWS
                rows[at : at + ROWS, :] = jnp.where(mine == ca, near_ref[k, b], far_ref[k, b])
    turned = rows[...].T
    keys_ref[...] = turned[: LANES // 2]
    vals_ref[...] = turned[LANES // 2 :]


def call(kernel, ins, out_shape, args, flops, **kw):
    many = isinstance(out_shape, (list, tuple))
    return pl.pallas_call(
        kernel,
        in_specs=ins,
        out_specs=[VMEM] * len(out_shape) if many else VMEM,
        out_shape=out_shape,
        cost_estimate=pl.CostEstimate(flops=flops, bytes_accessed=1 << 20, transcendentals=0),
        **kw,
    )(*args)


def sds(shape, dtype):
    return jax.ShapeDtypeStruct(shape, dtype)


def x_from(arr, k):
    return lax.ppermute(arr, "x", [(i, (i + k) % 4) for i in range(4)])


def x_back(arr, k):
    return lax.ppermute(arr, "x", [((i + k) % 4, i) for i in range(4)])


def swap(arr):
    return lax.ppermute(arr, "c", [(0, 1), (1, 0)])


def exchange(arr):
    return lax.all_to_all(arr, KV, split_axis=0, concat_axis=0, tiled=True)


def step(normed, queries, keys, values, attended, cotangent, log_sum, chosen):
    rank = lax.axis_index(KV).astype(jnp.int32)
    x = lax.axis_index("x").astype(jnp.int32)
    c = lax.axis_index("c").astype(jnp.int32)
    tp = x * 2 + c
    offer = call(
        offer_kernel,
        [SMEM] + [VMEM] * 3,
        sds((PEERS, BLOCKS + 1, ROWS, LANES), BF16),
        (jnp.stack([rank, tp]), keys.T, values.T, chosen),
        1 << 18,
        scratch_shapes=[pltpu.VMEM((TOK, LANES), F32)],
        name="offer",
    )
    offered = exchange(offer)
    asked = offered[:, BLOCKS]

    qd = call(
        pack_kernel,
        [VMEM] * 4,
        sds((2 * TOK + 48, LANES), BF16),
        (queries, cotangent, attended, log_sum.T),
        1 << 18,
        name="pack",
    )
    qds = [qd] + [x_from(qd, k) for k in (1, 2, 3)]
    qd_far = swap(jnp.stack(qds))

    owner = chosen >> 3
    inner = chosen & 7
    listed = chosen >= 0
    src = jnp.where(listed, owner * (BLOCKS + 1) + inner, 0)
    dst = jnp.where(listed, jnp.where(owner == rank, PEERS + inner, owner), 0)
    starts = rank * TOK + lax.broadcasted_iota(jnp.int32, chosen.shape, 0) * BLOCK
    rel = jnp.where(listed, chosen * BLOCK + ROWS * tp - starts, FAR)

    away, own, gq_own, gq_far = call(
        attend_kernel,
        [SMEM] * 3 + [VMEM] * 6,
        [
            sds((PEERS, ROWS, LANES), BF16),
            sds((BLOCKS, ROWS, LANES), F32),
            sds((4, TOK, LANES), F32),
            sds((4, TOK, LANES), BF16),
        ],
        (src, dst, rel, offered.reshape(PEERS * (BLOCKS + 1), ROWS, LANES), *qds, qd_far),
        1 << 30,
        scratch_shapes=[
            pltpu.VMEM((BLOCKS, 8, TOK), F32),
            pltpu.VMEM((PEERS + BLOCKS, ROWS, LANES), F32),
        ],
        name="attend",
    )
    gq4 = gq_own + swap(gq_far).astype(F32)
    returned = exchange(away)
    gq = gq4[0]
    for k in (1, 2, 3):
        gq = gq + x_back(gq4[k].astype(BF16), k).astype(F32)
    grad_queries = gq.astype(BF16)
    part = lax.dot_general(
        normed, grad_queries, (((0,), (0,)), ((), ())), preferred_element_type=F32
    ).astype(BF16)
    parts = exchange(part.reshape(PEERS, 64, LANES))
    weight_grad = jnp.sum(parts.astype(F32), axis=0)

    total = call(
        settle_kernel,
        [VMEM] * 3,
        sds((BLOCKS, ROWS, LANES), F32),
        (asked, returned, own),
        1 << 20,
        name="settle",
    )
    near = jnp.stack([total] + [x_from(total, k) for k in (1, 2, 3)])
    far = swap(near)
    grad_keys, grad_values = call(
        place_kernel,
        [SMEM, VMEM, VMEM],
        [sds((64, TOK), F32), sds((64, TOK), F32)],
        (jnp.stack([x, c]), near, far),
        1 << 20,
        scratch_shapes=[pltpu.VMEM((TOK, LANES), F32)],
        name="place",
    )
    return grad_queries, grad_keys.T, grad_values.T, weight_grad


def solution(mesh):
    torus = Mesh(mesh.devices.reshape(8, 8, 4, 2), ("z", "y", "x", "c"))
    heads = ("x", "c")
    in_specs = (
        P(KV, None),
        P(KV, heads),
        P(KV, None),
        P(KV, None),
        P(KV, heads),
        P(KV, heads),
        P(KV, heads),
        P(KV, None),
    )
    out_specs = (P(KV, heads), P(KV, None), P(KV, None), P(KV, heads))
    return jax.shard_map(step, mesh=torus, in_specs=in_specs, out_specs=out_specs, check_vma=False)
```

time: 165 us -> 134 us (0.81)
  the two profiles are of different devices: /device:TPU:8 before, /device:TPU:2 now
where the time goes in v2:
time: 134 us; the launch traced here: 133 us
  starting transfers between devices  65.3 us (49%)
  waiting for transfers between devices  36.8 us (27%)
  Pallas kernels  16.1 us (12%)
  other arithmetic  6.03 us (4%)
  local copies, waits for them, and re-layouts  4.59 us (3%)
  matrix products  2.98 us (2%)
    all_to_all x3, starting transfers between devices, exchange(): return lax.all_to_all(arr, KV, split_axis=0, concat_axis=0, tiled=True)  28.6 us
    ppermute x6, starting transfers between devices, x_from(): return lax.ppermute(arr, 'x', [(i, (i + k) % 4) for i in range(4)])  19.8 us
    all_to_all x3, waiting for transfers between devices, exchange(): return lax.all_to_all(arr, KV, split_axis=0, concat_axis=0, tiled=True)  19.7 us
    pallas_call x5, Pallas kernels, call(): pl.pallas_call(kernel, in_specs=ins, out_specs=[VMEM] * len(out_shape) if...  16.1 us
    ppermute x6, waiting for transfers between devices, x_from(): return lax.ppermute(arr, 'x', [(i, (i + k) % 4) for i in range(4)])  12.1 us
    ppermute x3, starting transfers between devices, x_back(): return lax.ppermute(arr, 'x', [((i + k) % 4, i) for i in range(4)])  11.1 us
    ppermute x3, starting transfers between devices, swap(): return lax.ppermute(arr, 'c', [(0, 1), (1, 0)])  5.75 us
    ppermute x3, waiting for transfers between devices, swap(): return lax.ppermute(arr, 'c', [(0, 1), (1, 0)])  4.94 us
  transfers between devices with their start and end apart: 15, of which 11 were waited for; matrix products, arithmetic and copies ran while one was open for 7% of the time, Pallas kernels for 4%

profile of v2, /device:TPU:2, one launch (start us, length us, event | category | flops | bytes accessed | tf_op | source)
XLA Modules:
  0.0 132.6 jit_solution(8098035314529054800)
XLA Ops:
  1.2 2.2 %offer.1 = bf16[64,9,8,128]{3,2,1,0:T(8,128)(2,1)} custom-call(s32[2]{0:T(128)} %pad_add_fusion.at_ref, bf16[64,512]{1,0:T(8,128)(2,1)} %bitcast.49, bf16[64,512]{1,0:T(8,128)(2,1)} %bitcast.50, s32[8,16]{1,0:T(8,128)} %chosen_ref.1), custom_call_target="tpu_custom_call" | custom-call | flops 262144 | bytes 1048576 | tf_op jit(solution)/shard_map/offer/pallas_call | solution.py:193
  3.4 16.6 %all-to-all-start = ((bf16[64,9,8,128]{3,2,1,0:T(8,128)(2,1)}), bf16[64,9,8,128]{3,2,1,0:T(8,128)(2,1)S(1)}, u32[]{:S(2)}, u32[]{:S(2)}) async-start(bf16[64,9,8,128]{3,2,1,0:T(8,128)(2,1)} %offer.1), calls=%async_computation | async-start | bytes 2359296 | tf_op jit(solution)/shard_map/all_to_all | solution.py:220
  20.0 1.9 %pack.1.q0 = bf16[1072,128]{1,0:T(8,128)(2,1)} custom-call(bf16[512,128]{1,0:T(8,128)(2,1)} %q_ref.1, bf16[512,128]{1,0:T(8,128)(2,1)} %g_ref.1, bf16[512,128]{1,0:T(8,128)(2,1)} %o_ref.1, f32[2,512]{1,0:T(2,128)} %bitcast.54), custom_call_target="tpu_custom_call" | custom-call | flops 262144 | bytes 1048576 | tf_op jit(solution)/shard_map/pack/pallas_call | solution.py:193
  21.9 2.6 %collective-permute-start.2 = (bf16[1072,128]{1,0:T(8,128)(2,1)}, bf16[1072,128]{1,0:T(8,128)(2,1)S(1)}, u32[]{:S(2)}, u32[]{:S(2)}) collective-permute-start(bf16[1072,128]{1,0:T(8,128)(2,1)} %pack.1.q0), channel_id=1, source_target_pairs={{0,6},{2,0},{4,2},{6,4},{1,7},{3,1},{5,3},{7,5},{8,14},{10,8},{12,... | collective-permute-start | bytes 823304 | tf_op jit(solution)/shard_map/ppermute | solution.py:208
  24.4 4.3 %collective-permute-start.1 = (bf16[1072,128]{1,0:T(8,128)(2,1)}, bf16[1072,128]{1,0:T(8,128)(2,1)S(1)}, u32[]{:S(2)}, u32[]{:S(2)}) collective-permute-start(bf16[1072,128]{1,0:T(8,128)(2,1)} %pack.1.q0), channel_id=1, source_target_pairs={{0,4},{2,6},{4,0},{6,2},{1,5},{3,7},{5,1},{7,3},{8,12},{10,14},{12... | collective-permute-start | bytes 823304 | tf_op jit(solution)/shard_map/ppermute | solution.py:208
  28.8 3.7 %collective-permute-start = (bf16[1072,128]{1,0:T(8,128)(2,1)}, bf16[1072,128]{1,0:T(8,128)(2,1)S(1)}, u32[]{:S(2)}, u32[]{:S(2)}) collective-permute-start(bf16[1072,128]{1,0:T(8,128)(2,1)} %pack.1.q0), channel_id=1, source_target_pairs={{0,2},{2,4},{4,6},{6,0},{1,3},{3,5},{5,7},{7,1},{8,10},{10,12},{12... | collective-permute-start | bytes 823304 | tf_op jit(solution)/shard_map/ppermute | solution.py:208
  32.6 6.3 %collective-permute-done.1.q2 = bf16[1072,128]{1,0:T(8,128)(2,1)S(1)} collective-permute-done((bf16[1072,128]{1,0:T(8,128)(2,1)}, bf16[1072,128]{1,0:T(8,128)(2,1)S(1)}, u32[]{:S(2)}, u32[]{:S(2)}) %collective-permute-start.1) | collective-permute-done | bytes 274464 | tf_op jit(solution)/shard_map/ppermute | solution.py:208
  38.9 2.8 %collective-permute-done.q1 = bf16[1072,128]{1,0:T(8,128)(2,1)S(1)} collective-permute-done((bf16[1072,128]{1,0:T(8,128)(2,1)}, bf16[1072,128]{1,0:T(8,128)(2,1)S(1)}, u32[]{:S(2)}, u32[]{:S(2)}) %collective-permute-start) | collective-permute-done | bytes 274464 | tf_op jit(solution)/shard_map/ppermute | solution.py:208
  42.9 1.9 %collective-permute-start.3 = (bf16[4,1072,128]{2,1,0:T(8,128)(2,1)S(1)}, bf16[4,1072,128]{2,1,0:T(8,128)(2,1)}, u32[]{:S(2)}, u32[]{:S(2)}) collective-permute-start(bf16[4,1072,128]{2,1,0:T(8,128)(2,1)S(1)} %pad_maximum_fusion), channel_id=1, source_target_pairs={{0,1},{1,0},{2,3},{3,2},{4,5},{5,4},{6,7},{7,6},{8,9},{9,8},{10,11... | collective-permute-start | bytes 3293192 | tf_op jit(solution)/shard_map/ppermute | solution.py:216
  45.5 2.1 %collective-permute-done.3.qp_ref = bf16[4,1072,128]{2,1,0:T(8,128)(2,1)} collective-permute-done((bf16[4,1072,128]{2,1,0:T(8,128)(2,1)S(1)}, bf16[4,1072,128]{2,1,0:T(8,128)(2,1)}, u32[]{:S(2)}, u32[]{:S(2)}) %collective-permute-start.3) | collective-permute-done | bytes 1097760 | tf_op jit(solution)/shard_map/ppermute | solution.py:216
  47.7 5.0 %all-to-all-done = bf16[64,9,8,128]{3,2,1,0:T(8,128)(2,1)S(1)} async-done(((bf16[64,9,8,128]{3,2,1,0:T(8,128)(2,1)}), bf16[64,9,8,128]{3,2,1,0:T(8,128)(2,1)S(1)}, u32[]{:S(2)}, u32[]{:S(2)}) %all-to-all-start) | async-done | bytes 1179680 | tf_op jit(solution)/shard_map/all_to_all | solution.py:220
  53.7 8.4 %attend.1 = (bf16[64,8,128]{2,1,0:T(8,128)(2,1)}, f32[8,8,128]{2,1,0:T(8,128)}, f32[4,512,128]{2,1,0:T(8,128)}, bf16[4,512,128]{2,1,0:T(8,128)(2,1)}) custom-call(s32[8,16]{1,0:T(8,128)} %get-tuple-element.23.src_ref, s32[8,16]{1,0:T(8,128)} %get-tuple-element.22.dst_ref, s32[8,16]{1,0:T(8,128)} %get-tuple-element.21.rel_ref, bf16[576,8,128]{2,1,0:T(8,128)(2,1)} %bitcast.43, ...), custom_call_target="tpu_custom_call" | custom-call | flops 1073741824 | bytes 1048576 | tf_op jit(solution)/shard_map/attend/pallas_call | solution.py:193
  62.1 1.9 %collective-permute-start.4 = (bf16[4,512,128]{2,1,0:T(8,128)(2,1)}, bf16[4,512,128]{2,1,0:T(8,128)(2,1)S(1)}, u32[]{:S(2)}, u32[]{:S(2)}) collective-permute-start(bf16[4,512,128]{2,1,0:T(8,128)(2,1)} %get-tuple-element.11), channel_id=1, source_target_pairs={{0,1},{1,0},{2,3},{3,2},{4,5},{5,4},{6,7},{7,6},{8,9},{9,8},{10,11... | collective-permute-start | bytes 1572872 | tf_op jit(solution)/shard_map/ppermute | solution.py:216
  64.0 2.1 %collective-permute-done.4 = bf16[4,512,128]{2,1,0:T(8,128)(2,1)S(1)} collective-permute-done((bf16[4,512,128]{2,1,0:T(8,128)(2,1)}, bf16[4,512,128]{2,1,0:T(8,128)(2,1)S(1)}, u32[]{:S(2)}, u32[]{:S(2)}) %collective-permute-start.4) | collective-permute-done | bytes 524320 | tf_op jit(solution)/shard_map/ppermute | solution.py:216
  66.1 1.4 %fusion.6 = (bf16[4,512,128]{2,1,0:T(8,128)(2,1)S(1)}, f32[4,512,128]{2,1,0:T(8,128)S(1)}) fusion(f32[4,512,128]{2,1,0:T(8,128)} %get-tuple-element.10, bf16[4,512,128]{2,1,0:T(8,128)(2,1)S(1)} %collective-permute-done.4), kind=kLoop, calls=%fused_computation.23 | loop fusion | flops 786432 | bytes 3145728 | tf_op jit(solution)/shard_map/convert.2
  67.5 2.4 %collective-permute-start.5 = (bf16[512,128]{1,0:T(8,128)(2,1)S(1)}, bf16[512,128]{1,0:T(8,128)(2,1)S(1)}, u32[]{:S(2)}, u32[]{:S(2)}) collective-permute-start(bf16[512,128]{1,0:T(8,128)(2,1)S(1)} %get-tuple-element.18), channel_id=1, source_target_pairs={{2,0},{4,2},{6,4},{0,6},{3,1},{5,3},{7,5},{1,7},{10,8},{12,10},{14... | collective-permute-start | bytes 393224 | tf_op jit(solution)/shard_map/ppermute | solution.py:212
  69.9 3.4 %collective-permute-start.7 = (bf16[512,128]{1,0:T(8,128)(2,1)S(1)}, bf16[512,128]{1,0:T(8,128)(2,1)S(1)}, u32[]{:S(2)}, u32[]{:S(2)}) collective-permute-start(bf16[512,128]{1,0:T(8,128)(2,1)S(1)} %get-tuple-element.19), channel_id=1, source_target_pairs={{6,0},{0,2},{2,4},{4,6},{7,1},{1,3},{3,5},{5,7},{14,8},{8,10},{10,... | collective-permute-start | bytes 393224 | tf_op jit(solution)/shard_map/ppermute | solution.py:212
  73.3 5.2 %collective-permute-start.6 = (bf16[512,128]{1,0:T(8,128)(2,1)S(1)}, bf16[512,128]{1,0:T(8,128)(2,1)S(1)}, u32[]{:S(2)}, u32[]{:S(2)}) collective-permute-start(bf16[512,128]{1,0:T(8,128)(2,1)S(1)} %get-tuple-element.20), channel_id=1, source_target_pairs={{4,0},{6,2},{0,4},{2,6},{5,1},{7,3},{1,5},{3,7},{12,8},{14,10},{8,... | collective-permute-start | bytes 393224 | tf_op jit(solution)/shard_map/ppermute | solution.py:212
  78.6 7.4 %all-to-all-start.1 = ((bf16[64,8,128]{2,1,0:T(8,128)(2,1)}), bf16[64,8,128]{2,1,0:T(8,128)(2,1)S(1)}, u32[]{:S(2)}, u32[]{:S(2)}) async-start(bf16[64,8,128]{2,1,0:T(8,128)(2,1)} %get-tuple-element.12), calls=%async_computation.1 | async-start | bytes 262144 | tf_op jit(solution)/shard_map/all_to_all | solution.py:220
  86.1 3.0 %fusion = bf16[4096,128]{0,1:T(8,128)(2,1)S(1)} fusion(bf16[512,128]{1,0:T(8,128)(2,1)S(1)} %fusion.4, bf16[512,4096]{1,0:T(8,128)(2,1)} %param.8), kind=kOutput, calls=%fused_computation.1 | convolution fusion | flops 537395200 | bytes 5373952 | tf_op jit(solution)/shard_map/dot_general | solution.py:282
  89.1 1.3 copy.17
  90.4 8.3 %all-to-all-done.1.returned_ref = bf16[64,8,128]{2,1,0:T(8,128)(2,1)S(1)} async-done(((bf16[64,8,128]{2,1,0:T(8,128)(2,1)}), bf16[64,8,128]{2,1,0:T(8,128)(2,1)S(1)}, u32[]{:S(2)}, u32[]{:S(2)}) %all-to-all-start.1) | async-done | bytes 131104 | tf_op jit(solution)/shard_map/all_to_all | solution.py:220
  98.7 4.7 %all-to-all-start.2 = ((bf16[64,64,128]{2,1,0:T(8,128)(2,1)}), bf16[64,64,128]{2,1,0:T(8,128)(2,1)S(1)}, u32[]{:S(2)}, u32[]{:S(2)}) async-start(bf16[64,64,128]{2,1,0:T(8,128)(2,1)} %bitcast.24), calls=%async_computation.2 | async-start | bytes 2097152 | tf_op jit(solution)/shard_map/all_to_all | solution.py:220
  103.4 1.6 %slice_bitcast_fusion.1.asked_ref = bf16[64,8,128]{2,1,0:T(8,128)(2,1)} fusion(bf16[64,9,8,128]{3,2,1,0:T(8,128)(2,1)} %copy-done), kind=kLoop, calls=%fused_computation.10 | loop fusion | bytes 262144 | tf_op jit(solution)/shard_map/squeeze | solution.py:238
  105.0 1.8 %settle.1 = f32[8,8,128]{2,1,0:T(8,128)} custom-call(bf16[64,8,128]{2,1,0:T(8,128)(2,1)} %slice_bitcast_fusion.1.asked_ref, bf16[64,8,128]{2,1,0:T(8,128)(2,1)} %copy-done.1, f32[8,8,128]{2,1,0:T(8,128)} %get-tuple-element.13.own_ref), custom_call_target="tpu_custom_call" | custom-call | flops 1048576 | bytes 1048576 | tf_op jit(solution)/shard_map/settle/pallas_call | solution.py:193
  106.8 2.0 %collective-permute-start.10 = (f32[8,8,128]{2,1,0:T(8,128)}, f32[8,8,128]{2,1,0:T(8,128)S(1)}, u32[]{:S(2)}, u32[]{:S(2)}) collective-permute-start(f32[8,8,128]{2,1,0:T(8,128)} %settle.1), channel_id=1, source_target_pairs={{0,6},{2,0},{4,2},{6,4},{1,7},{3,1},{5,3},{7,5},{8,14},{10,8},{12,... | collective-permute-start | bytes 98312 | tf_op jit(solution)/shard_map/ppermute | solution.py:208
  108.8 4.0 %collective-permute-start.9 = (f32[8,8,128]{2,1,0:T(8,128)}, f32[8,8,128]{2,1,0:T(8,128)S(1)}, u32[]{:S(2)}, u32[]{:S(2)}) collective-permute-start(f32[8,8,128]{2,1,0:T(8,128)} %settle.1), channel_id=1, source_target_pairs={{0,4},{2,6},{4,0},{6,2},{1,5},{3,7},{5,1},{7,3},{8,12},{10,14},{12... | collective-permute-start | bytes 98312 | tf_op jit(solution)/shard_map/ppermute | solution.py:208
  112.9 3.1 %collective-permute-start.8 = (f32[8,8,128]{2,1,0:T(8,128)}, f32[8,8,128]{2,1,0:T(8,128)S(1)}, u32[]{:S(2)}, u32[]{:S(2)}) collective-permute-start(f32[8,8,128]{2,1,0:T(8,128)} %settle.1), channel_id=1, source_target_pairs={{0,2},{2,4},{4,6},{6,0},{1,3},{3,5},{5,7},{7,1},{8,10},{10,12},{12... | collective-permute-start | bytes 98312 | tf_op jit(solution)/shard_map/ppermute | solution.py:208
  116.4 2.5 %collective-permute-done.8 = f32[8,8,128]{2,1,0:T(8,128)S(1)} collective-permute-done((f32[8,8,128]{2,1,0:T(8,128)}, f32[8,8,128]{2,1,0:T(8,128)S(1)}, u32[]{:S(2)}, u32[]{:S(2)}) %collective-permute-start.8) | collective-permute-done | bytes 32800 | tf_op jit(solution)/shard_map/ppermute | solution.py:208
  119.7 1.9 %collective-permute-start.11 = (f32[4,8,8,128]{3,2,1,0:T(8,128)S(1)}, f32[4,8,8,128]{3,2,1,0:T(8,128)S(1)}, u32[]{:S(2)}, u32[]{:S(2)}) collective-permute-start(f32[4,8,8,128]{3,2,1,0:T(8,128)S(1)} %pad_maximum_fusion.1.near_ref), channel_id=1, source_target_pairs={{0,1},{1,0},{2,3},{3,2},{4,5},{5,4},{6,7},{7,6},{8,9},{9,8},{10,11... | collective-permute-start | bytes 393224 | tf_op jit(solution)/shard_map/ppermute | solution.py:216
  123.6 1.8 %place.1 = (f32[64,512]{1,0:T(8,128)}, f32[64,512]{1,0:T(8,128)}) custom-call(s32[2]{0:T(128)} %pad_add_fusion.1.at_ref, f32[4,8,8,128]{3,2,1,0:T(8,128)} %copy-done.2, f32[4,8,8,128]{3,2,1,0:T(8,128)} %copy-done.7), custom_call_target="tpu_custom_call" | custom-call | flops 1048576 | bytes 1048576 | tf_op jit(solution)/shard_map/place/pallas_call | solution.py:193
  125.4 6.4 %all-to-all-done.2 = bf16[64,64,128]{2,1,0:T(8,128)(2,1)S(1)} async-done(((bf16[64,64,128]{2,1,0:T(8,128)(2,1)}), bf16[64,64,128]{2,1,0:T(8,128)(2,1)S(1)}, u32[]{:S(2)}, u32[]{:S(2)}) %all-to-all-start.2) | async-done | bytes 1048608 | tf_op jit(solution)/shard_map/all_to_all | solution.py:220
  (34 shorter events, 7.5 us)
Async XLA Ops:
  3.4 49.2 %all-to-all-start = ((bf16[64,9,8,128]{3,2,1,0:T(8,128)(2,1)}), bf16[64,9,8,128]{3,2,1,0:T(8,128)(2,1)S(1)}, u32[]{:S(2)}, u32[]{:S(2)}) async-start(bf16[64,9,8,128]{3,2,1,0:T(8,128)(2,1)} %offer.1), calls=%async_computation | async-start | bytes 2359296 | tf_op jit(solution)/shard_map/all_to_all | solution.py:220
  21.9 23.0 %copy-start.8 = (s32[8,16]{1,0:T(8,128)S(1)}, s32[8,16]{1,0:T(8,128)}, u32[]{:S(2)}) copy-start(s32[8,16]{1,0:T(8,128)} %chosen_ref.1) | copy-start | bytes 1540
  21.9 10.7 %collective-permute-start.2 = (bf16[1072,128]{1,0:T(8,128)(2,1)}, bf16[1072,128]{1,0:T(8,128)(2,1)S(1)}, u32[]{:S(2)}, u32[]{:S(2)}) collective-permute-start(bf16[1072,128]{1,0:T(8,128)(2,1)} %pack.1.q0), channel_id=1, source_target_pairs={{0,6},{2,0},{4,2},{6,4},{1,7},{3,1},{5,3},{7,5},{8,14},{10,8},{12,... | collective-permute-start | bytes 823304 | tf_op jit(solution)/shard_map/ppermute | solution.py:208
  24.4 14.5 %collective-permute-start.1 = (bf16[1072,128]{1,0:T(8,128)(2,1)}, bf16[1072,128]{1,0:T(8,128)(2,1)S(1)}, u32[]{:S(2)}, u32[]{:S(2)}) collective-permute-start(bf16[1072,128]{1,0:T(8,128)(2,1)} %pack.1.q0), channel_id=1, source_target_pairs={{0,4},{2,6},{4,0},{6,2},{1,5},{3,7},{5,1},{7,3},{8,12},{10,14},{12... | collective-permute-start | bytes 823304 | tf_op jit(solution)/shard_map/ppermute | solution.py:208
  28.8 12.9 %collective-permute-start = (bf16[1072,128]{1,0:T(8,128)(2,1)}, bf16[1072,128]{1,0:T(8,128)(2,1)S(1)}, u32[]{:S(2)}, u32[]{:S(2)}) collective-permute-start(bf16[1072,128]{1,0:T(8,128)(2,1)} %pack.1.q0), channel_id=1, source_target_pairs={{0,2},{2,4},{4,6},{6,0},{1,3},{3,5},{5,7},{7,1},{8,10},{10,12},{12... | collective-permute-start | bytes 823304 | tf_op jit(solution)/shard_map/ppermute | solution.py:208
  32.6 20.0 %copy-start.4 = (bf16[1072,128]{1,0:T(8,128)(2,1)}, bf16[1072,128]{1,0:T(8,128)(2,1)S(1)}, u32[]{:S(2)}) copy-start(bf16[1072,128]{1,0:T(8,128)(2,1)S(1)} %collective-permute-done.2.q3) | copy-start | bytes 823300
  38.9 13.7 %copy-start.5 = (bf16[1072,128]{1,0:T(8,128)(2,1)}, bf16[1072,128]{1,0:T(8,128)(2,1)S(1)}, u32[]{:S(2)}) copy-start(bf16[1072,128]{1,0:T(8,128)(2,1)S(1)} %collective-permute-done.1.q2) | copy-start | bytes 823300
  41.7 10.9 %copy-start.6 = (bf16[1072,128]{1,0:T(8,128)(2,1)}, bf16[1072,128]{1,0:T(8,128)(2,1)S(1)}, u32[]{:S(2)}) copy-start(bf16[1072,128]{1,0:T(8,128)(2,1)S(1)} %collective-permute-done.q1) | copy-start | bytes 823300
  42.9 4.8 %collective-permute-start.3 = (bf16[4,1072,128]{2,1,0:T(8,128)(2,1)S(1)}, bf16[4,1072,128]{2,1,0:T(8,128)(2,1)}, u32[]{:S(2)}, u32[]{:S(2)}) collective-permute-start(bf16[4,1072,128]{2,1,0:T(8,128)(2,1)S(1)} %pad_maximum_fusion), channel_id=1, source_target_pairs={{0,1},{1,0},{2,3},{3,2},{4,5},{5,4},{6,7},{7,6},{8,9},{9,8},{10,11... | collective-permute-start | bytes 3293192 | tf_op jit(solution)/shard_map/ppermute | solution.py:216
  52.6 1.0 copy-start
  62.1 4.0 %collective-permute-start.4 = (bf16[4,512,128]{2,1,0:T(8,128)(2,1)}, bf16[4,512,128]{2,1,0:T(8,128)(2,1)S(1)}, u32[]{:S(2)}, u32[]{:S(2)}) collective-permute-start(bf16[4,512,128]{2,1,0:T(8,128)(2,1)} %get-tuple-element.11), channel_id=1, source_target_pairs={{0,1},{1,0},{2,3},{3,2},{4,5},{5,4},{6,7},{7,6},{8,9},{9,8},{10,11... | collective-permute-start | bytes 1572872 | tf_op jit(solution)/shard_map/ppermute | solution.py:216
  67.5 18.5 %collective-permute-start.5 = (bf16[512,128]{1,0:T(8,128)(2,1)S(1)}, bf16[512,128]{1,0:T(8,128)(2,1)S(1)}, u32[]{:S(2)}, u32[]{:S(2)}) collective-permute-start(bf16[512,128]{1,0:T(8,128)(2,1)S(1)} %get-tuple-element.18), channel_id=1, source_target_pairs={{2,0},{4,2},{6,4},{0,6},{3,1},{5,3},{7,5},{1,7},{10,8},{12,10},{14... | collective-permute-start | bytes 393224 | tf_op jit(solution)/shard_map/ppermute | solution.py:212
  69.9 16.1 %collective-permute-start.7 = (bf16[512,128]{1,0:T(8,128)(2,1)S(1)}, bf16[512,128]{1,0:T(8,128)(2,1)S(1)}, u32[]{:S(2)}, u32[]{:S(2)}) collective-permute-start(bf16[512,128]{1,0:T(8,128)(2,1)S(1)} %get-tuple-element.19), channel_id=1, source_target_pairs={{6,0},{0,2},{2,4},{4,6},{7,1},{1,3},{3,5},{5,7},{14,8},{8,10},{10,... | collective-permute-start | bytes 393224 | tf_op jit(solution)/shard_map/ppermute | solution.py:212
  73.3 12.7 %collective-permute-start.6 = (bf16[512,128]{1,0:T(8,128)(2,1)S(1)}, bf16[512,128]{1,0:T(8,128)(2,1)S(1)}, u32[]{:S(2)}, u32[]{:S(2)}) collective-permute-start(bf16[512,128]{1,0:T(8,128)(2,1)S(1)} %get-tuple-element.20), channel_id=1, source_target_pairs={{4,0},{6,2},{0,4},{2,6},{5,1},{7,3},{1,5},{3,7},{12,8},{14,10},{8,... | collective-permute-start | bytes 393224 | tf_op jit(solution)/shard_map/ppermute | solution.py:212
  78.6 20.2 %all-to-all-start.1 = ((bf16[64,8,128]{2,1,0:T(8,128)(2,1)}), bf16[64,8,128]{2,1,0:T(8,128)(2,1)S(1)}, u32[]{:S(2)}, u32[]{:S(2)}) async-start(bf16[64,8,128]{2,1,0:T(8,128)(2,1)} %get-tuple-element.12), calls=%async_computation.1 | async-start | bytes 262144 | tf_op jit(solution)/shard_map/all_to_all | solution.py:220
  86.1 3.0 %copy-start.3 = (bf16[512,128]{1,0:T(8,128)(2,1)}, bf16[512,128]{1,0:T(8,128)(2,1)S(1)}, u32[]{:S(2)}) copy-start(bf16[512,128]{1,0:T(8,128)(2,1)S(1)} %fusion.4) | copy-start | bytes 393220
  98.7 6.2 %copy-start.1 = (bf16[64,8,128]{2,1,0:T(8,128)(2,1)}, bf16[64,8,128]{2,1,0:T(8,128)(2,1)S(1)}, u32[]{:S(2)}) copy-start(bf16[64,8,128]{2,1,0:T(8,128)(2,1)S(1)} %all-to-all-done.1.returned_ref) | copy-start | bytes 393220
  98.7 33.1 %all-to-all-start.2 = ((bf16[64,64,128]{2,1,0:T(8,128)(2,1)}), bf16[64,64,128]{2,1,0:T(8,128)(2,1)S(1)}, u32[]{:S(2)}, u32[]{:S(2)}) async-start(bf16[64,64,128]{2,1,0:T(8,128)(2,1)} %bitcast.24), calls=%async_computation.2 | async-start | bytes 2097152 | tf_op jit(solution)/shard_map/all_to_all | solution.py:220
  106.8 9.2 %collective-permute-start.10 = (f32[8,8,128]{2,1,0:T(8,128)}, f32[8,8,128]{2,1,0:T(8,128)S(1)}, u32[]{:S(2)}, u32[]{:S(2)}) collective-permute-start(f32[8,8,128]{2,1,0:T(8,128)} %settle.1), channel_id=1, source_target_pairs={{0,6},{2,0},{4,2},{6,4},{1,7},{3,1},{5,3},{7,5},{8,14},{10,8},{12,... | collective-permute-start | bytes 98312 | tf_op jit(solution)/shard_map/ppermute | solution.py:208
  108.8 7.5 %collective-permute-start.9 = (f32[8,8,128]{2,1,0:T(8,128)}, f32[8,8,128]{2,1,0:T(8,128)S(1)}, u32[]{:S(2)}, u32[]{:S(2)}) collective-permute-start(f32[8,8,128]{2,1,0:T(8,128)} %settle.1), channel_id=1, source_target_pairs={{0,4},{2,6},{4,0},{6,2},{1,5},{3,7},{5,1},{7,3},{8,12},{10,14},{12... | collective-permute-start | bytes 98312 | tf_op jit(solution)/shard_map/ppermute | solution.py:208
  112.9 6.0 %collective-permute-start.8 = (f32[8,8,128]{2,1,0:T(8,128)}, f32[8,8,128]{2,1,0:T(8,128)S(1)}, u32[]{:S(2)}, u32[]{:S(2)}) collective-permute-start(f32[8,8,128]{2,1,0:T(8,128)} %settle.1), channel_id=1, source_target_pairs={{0,2},{2,4},{4,6},{6,0},{1,3},{3,5},{5,7},{7,1},{8,10},{10,12},{12... | collective-permute-start | bytes 98312 | tf_op jit(solution)/shard_map/ppermute | solution.py:208
  119.7 3.3 %copy-start.2 = (f32[4,8,8,128]{3,2,1,0:T(8,128)}, f32[4,8,8,128]{3,2,1,0:T(8,128)S(1)}, u32[]{:S(2)}) copy-start(f32[4,8,8,128]{3,2,1,0:T(8,128)S(1)} %pad_maximum_fusion.1.near_ref) | copy-start | bytes 393220
  119.7 3.2 %collective-permute-start.11 = (f32[4,8,8,128]{3,2,1,0:T(8,128)S(1)}, f32[4,8,8,128]{3,2,1,0:T(8,128)S(1)}, u32[]{:S(2)}, u32[]{:S(2)}) collective-permute-start(f32[4,8,8,128]{3,2,1,0:T(8,128)S(1)} %pad_maximum_fusion.1.near_ref), channel_id=1, source_target_pairs={{0,1},{1,0},{2,3},{3,2},{4,5},{5,4},{6,7},{7,6},{8,9},{9,8},{10,11... | collective-permute-start | bytes 393224 | tf_op jit(solution)/shard_map/ppermute | solution.py:216
  122.9 0.6 copy-start.7

commit v3 on v2

--- a/solution.py
+++ b/solution.py
@@ -11,11 +11,13 @@
 BLOCKS = 8
 SLOTS = 16
 PEERS = 64
+SIDE = 8
 ROWS = 8
 TOK = 512
 LANES = 128
 SCALE = 0.125
 KV = ("z", "y")
+ALL = ("z", "y", "x", "c")
 FAR = 1 << 20
 F32 = jnp.float32
 BF16 = jnp.bfloat16
@@ -27,12 +29,14 @@
     return lax.broadcasted_iota(jnp.int32, shape, len(shape) - 1) < LANES // 2
 
 
-def offer_kernel(at_ref, keys_ref, vals_ref, chosen_ref, out_ref, pairs):
+def offer_kernel(at_ref, keys_ref, vals_ref, chosen_ref, out_ref, piece_ref, pairs):
     rank = at_ref[0]
     tp = at_ref[1]
+    flip = at_ref[2]
     both = jnp.concatenate([keys_ref[...], vals_ref[...]], axis=0).astype(F32)
     pairs[...] = both.T
-    peer = lax.broadcasted_iota(jnp.int32, (PEERS, SLOTS), 0)
+    at = lax.broadcasted_iota(jnp.int32, (PEERS, SLOTS), 0)
+    peer = jnp.where(jnp.full(at.shape, flip, jnp.int32) == 0, at, (at & 7) * 8 + (at >> 3))
     best = jnp.zeros((PEERS, SLOTS), jnp.int32)
     for j in range(BLOCKS):
         c = chosen_ref[j : j + 1, :]
@@ -40,14 +44,62 @@
         best = jnp.maximum(best, jnp.where(hit, (c & 7) + 1, 0))
     best = jnp.max(best, axis=1, keepdims=True)
     best = jnp.broadcast_to(best, (PEERS, LANES)).astype(F32)
-    pieces = []
     for b in range(BLOCKS):
         at = pl.multiple_of(b * BLOCK + tp * ROWS, ROWS)
-        pieces.append(pairs[pl.ds(at, ROWS), :].astype(BF16))
-    for s in range(PEERS):
+        piece = pairs[pl.ds(at, ROWS), :].astype(BF16)
+        piece_ref[b] = piece
+        for i in range(SIDE):
+            out_ref[i, b] = piece
+    for i in range(SIDE):
+        out_ref[i, BLOCKS] = best[i * SIDE : (i + 1) * SIDE].astype(BF16)
+
+
+def pick_kernel(wants_ref, pushed_ref, out_ref):
+    for r in range(SIDE):
+        pieces = [pushed_ref[r, b].astype(F32) for b in range(BLOCKS)]
+        for i in range(SIDE):
+            want = jnp.broadcast_to(wants_ref[i].astype(F32)[r : r + 1], (ROWS, LANES))
+            got = jnp.zeros((ROWS, LANES), F32)
+            for b in range(BLOCKS):
+                got = jnp.where(want == b + 1.0, pieces[b], got)
+            out_ref[i, r] = got.astype(BF16)
+
+
+def relay_kernel(wants_ref, given_ref, out_ref):
+    for r in range(SIDE):
+        totals = [jnp.zeros((ROWS, LANES), F32) for _ in range(BLOCKS)]
+        for i in range(SIDE):
+            want = jnp.broadcast_to(wants_ref[i].astype(F32)[r : r + 1], (ROWS, LANES))
+            got = given_ref[i, r].astype(F32)
+            for b in range(BLOCKS):
+                totals[b] = totals[b] + jnp.where(want == b + 1.0, got, 0.0)
         for b in range(BLOCKS):
-            out_ref[s, b] = pieces[b]
-        out_ref[s, BLOCKS] = jnp.broadcast_to(best[s : s + 1], (ROWS, LANES)).astype(BF16)
+            out_ref[r, b] = totals[b].astype(BF16)
+
+
+def settle_kernel(own_ref, given_ref, out_ref):
+    for b in range(BLOCKS):
+        total = own_ref[b]
+        for i in range(SIDE):
+            total = total + given_ref[i, b].astype(F32)
+        out_ref[b] = total
+
+
+def weight_kernel(at_ref, grad_ref, normed_ref, out_ref, grad_t):
+    i = pl.program_id(0)
+    flip = at_ref[2]
+
+    @pl.when(i == 0)
+    def _():
+        grad_t[...] = grad_ref[...].astype(F32).T.astype(BF16)
+
+    part = lax.dot_general(
+        grad_t[...], normed_ref[...], (((1,), (0,)), ((), ())), preferred_element_type=F32
+    )
+    part = part.T.astype(BF16)
+    for n in range(SIDE):
+        at = jnp.where(flip == 0, i * SIDE + n, n * SIDE + i)
+        out_ref[at] = part[n * BLOCK : (n + 1) * BLOCK]
 
 
 def pack_kernel(q_ref, g_ref, o_ref, log_ref, out_ref):
@@ -71,10 +123,10 @@
 
 
 def attend_kernel(
-    src_ref,
-    dst_ref,
+    slot_ref,
     rel_ref,
-    offered_ref,
+    fetched_ref,
+    piece_ref,
     q0,
     q1,
     q2,
@@ -85,9 +137,12 @@
     gq_own_ref,
     gq_far_ref,
     stats_tab,
+    table,
     acc,
 ):
     near = (q0, q1, q2, q3)
+    table[:PEERS] = fetched_ref[...].astype(F32)
+    table[PEERS:] = piece_ref[...].astype(F32)
     acc[...] = jnp.zeros(acc.shape, F32)
     low = low_lanes((LANES, LANES))
     low4 = low_lanes((4, LANES))
@@ -112,7 +167,7 @@
             stats_tab[j, 0:4, pair * LANES : (pair + 1) * LANES] = jnp.where(low4, lo, hi)
 
     def one_block(j, carry):
-        kv = jnp.concatenate([offered_ref[src_ref[j, s]].astype(F32) for s in range(SLOTS)], axis=0)
+        kv = jnp.concatenate([table[slot_ref[j, s]] for s in range(SLOTS)], axis=0)
         turned = pltpu.roll(kv, LANES // 2, 1)
         k2 = jnp.concatenate([jnp.where(low, kv, 0.0), jnp.where(low, 0.0, turned)], axis=0).astype(BF16)
         v2 = jnp.concatenate([jnp.where(low, turned, 0.0), jnp.where(low, 0.0, kv)], axis=0).astype(BF16)
@@ -155,23 +210,12 @@
             jnp.where(low, dv[:LANES], dk[LANES:]), LANES // 2, 1
         )
         for s in range(SLOTS):
-            acc[dst_ref[j, s]] += both[s * ROWS : (s + 1) * ROWS]
+            acc[slot_ref[j, s]] += both[s * ROWS : (s + 1) * ROWS]
         return carry
 
     lax.fori_loop(0, BLOCKS, one_block, 0)
     away_ref[...] = acc[:PEERS].astype(BF16)
     own_ref[...] = acc[PEERS:]
-
-
-def settle_kernel(asked_ref, returned_ref, own_ref, out_ref):
-    totals = [own_ref[b] for b in range(BLOCKS)]
-    for s in range(PEERS):
-        want = asked_ref[s].astype(F32)
-        got = returned_ref[s].astype(F32)
-        for b in range(BLOCKS):
-            totals[b] = totals[b] + jnp.where(want == b + 1.0, got, 0.0)
-    for b in range(BLOCKS):
-        out_ref[b] = totals[b]
 
 
 def place_kernel(at_ref, near_ref, far_ref, keys_ref, vals_ref, rows):
@@ -216,8 +260,26 @@
     return lax.ppermute(arr, "c", [(0, 1), (1, 0)])
 
 
-def exchange(arr):
-    return lax.all_to_all(arr, KV, split_axis=0, concat_axis=0, tiled=True)
+def device(z, y, x, c):
+    return ((z * 8 + y) * 4 + x) * 2 + c
+
+
+def lines(first):
+    out = []
+    for x in range(4):
+        for c in range(2):
+            for a in range(SIDE):
+                if (c == 0) == first:
+                    out.append([device(i, a, x, c) for i in range(SIDE)])
+                else:
+                    out.append([device(a, i, x, c) for i in range(SIDE)])
+    return out
+
+
+def along(arr, first):
+    return lax.all_to_all(
+        arr, ALL, split_axis=0, concat_axis=0, tiled=True, axis_index_groups=lines(first)
+    )
 
 
 def step(normed, queries, keys, values, attended, cotangent, log_sum, chosen):
@@ -225,17 +287,30 @@
     x = lax.axis_index("x").astype(jnp.int32)
     c = lax.axis_index("c").astype(jnp.int32)
     tp = x * 2 + c
-    offer = call(
+    spot = jnp.stack([rank, tp, c])
+    offer, piece = call(
         offer_kernel,
         [SMEM] + [VMEM] * 3,
-        sds((PEERS, BLOCKS + 1, ROWS, LANES), BF16),
-        (jnp.stack([rank, tp]), keys.T, values.T, chosen),
+        [
+            sds((SIDE, BLOCKS + 1, ROWS, LANES), BF16),
+            sds((BLOCKS, ROWS, LANES), BF16),
+        ],
+        (spot, keys.T, values.T, chosen),
         1 << 18,
         scratch_shapes=[pltpu.VMEM((TOK, LANES), F32)],
         name="offer",
     )
-    offered = exchange(offer)
-    asked = offered[:, BLOCKS]
+    pushed = along(offer, True)
+    wants = swap(pushed[:, BLOCKS])
+    picked = call(
+        pick_kernel,
+        [VMEM] * 2,
+        sds((SIDE, SIDE, ROWS, LANES), BF16),
+        (wants, pushed),
+        1 << 20,
+        name="pick",
+    )
+    fetched = along(picked, False).reshape(PEERS, ROWS, LANES)
 
     qd = call(
         pack_kernel,
@@ -251,45 +326,68 @@
     owner = chosen >> 3
     inner = chosen & 7
     listed = chosen >= 0
-    src = jnp.where(listed, owner * (BLOCKS + 1) + inner, 0)
-    dst = jnp.where(listed, jnp.where(owner == rank, PEERS + inner, owner), 0)
+    peer = jnp.where(c == 0, (owner & 7) * 8 + (owner >> 3), owner)
+    slot = jnp.where(listed, jnp.where(owner == rank, PEERS + inner, peer), 0)
     starts = rank * TOK + lax.broadcasted_iota(jnp.int32, chosen.shape, 0) * BLOCK
     rel = jnp.where(listed, chosen * BLOCK + ROWS * tp - starts, FAR)
 
     away, own, gq_own, gq_far = call(
         attend_kernel,
-        [SMEM] * 3 + [VMEM] * 6,
+        [SMEM] * 2 + [VMEM] * 7,
         [
             sds((PEERS, ROWS, LANES), BF16),
             sds((BLOCKS, ROWS, LANES), F32),
             sds((4, TOK, LANES), F32),
             sds((4, TOK, LANES), BF16),
         ],
-        (src, dst, rel, offered.reshape(PEERS * (BLOCKS + 1), ROWS, LANES), *qds, qd_far),
+        (slot, rel, fetched, piece, *qds, qd_far),
         1 << 30,
         scratch_shapes=[
             pltpu.VMEM((BLOCKS, 8, TOK), F32),
             pltpu.VMEM((PEERS + BLOCKS, ROWS, LANES), F32),
+            pltpu.VMEM((PEERS + BLOCKS, ROWS, LANES), F32),
         ],
         name="attend",
     )
     gq4 = gq_own + swap(gq_far).astype(F32)
-    returned = exchange(away)
+    given = along(away.reshape(SIDE, SIDE, ROWS, LANES), False)
+    relayed = call(
+        relay_kernel,
+        [VMEM] * 2,
+        sds((SIDE, BLOCKS, ROWS, LANES), BF16),
+        (wants, given),
+        1 << 20,
+        name="relay",
+    )
+    returned = along(relayed, True)
     gq = gq4[0]
     for k in (1, 2, 3):
         gq = gq + x_back(gq4[k].astype(BF16), k).astype(F32)
     grad_queries = gq.astype(BF16)
-    part = lax.dot_general(
-        normed, grad_queries, (((0,), (0,)), ((), ())), preferred_element_type=F32
-    ).astype(BF16)
-    parts = exchange(part.reshape(PEERS, 64, LANES))
+    part = pl.pallas_call(
+        weight_kernel,
+        grid=(SIDE,),
+        in_specs=[
+            SMEM,
+            pl.BlockSpec((TOK, LANES), lambda i: (0, 0)),
+            pl.BlockSpec((TOK, TOK), lambda i: (0, i)),
+        ],
+        out_specs=pl.BlockSpec((PEERS, BLOCK, LANES), lambda i: (0, 0, 0)),
+        out_shape=sds((PEERS, BLOCK, LANES), BF16),
+        scratch_shapes=[pltpu.VMEM((LANES, TOK), BF16)],
+        cost_estimate=pl.CostEstimate(flops=1 << 29, bytes_accessed=5 << 20, transcendentals=0),
+        name="product",
+    )(spot, grad_queries, normed)
+    parts = along(part.reshape(SIDE, SIDE, BLOCK, LANES), True)
+    half = jnp.sum(parts.astype(F32), axis=0).astype(BF16)
+    parts = along(half, False)
     weight_grad = jnp.sum(parts.astype(F32), axis=0)
 
     total = call(
         settle_kernel,
-        [VMEM] * 3,
+        [VMEM] * 2,
         sds((BLOCKS, ROWS, LANES), F32),
-        (asked, returned, own),
+        (own, returned),
         1 << 20,
         name="settle",
     )

time: 134 us -> 155 us (1.16)
  blocking collectives: 0 us -> 19.6 us
  Pallas kernels: 16.1 us -> 25.7 us
  waiting for transfers between devices: 36.8 us -> 29.7 us
  matrix products: 2.98 us -> 0 us
  starting transfers between devices: 65.3 us -> 68.1 us
  local copies, waits for them, and re-layouts: 4.59 us -> 2.99 us
    all_to_all x0 -> x1, blocking collectives: none -> 19.6 us  [along(): lax.all_to_all(arr, ALL, split_axis=0, concat_axis=0, tiled=True, axis_in...]
    pallas_call x0 -> x1, Pallas kernels: none -> 7.05 us  [step(): pl.pallas_call(weight_kernel, grid=(SIDE,), in_specs=[SMEM, pl.BlockSpec(...]
    ppermute x6, waiting for transfers between devices: 12.1 us -> 6.88 us  [x_from(): return lax.ppermute(arr, 'x', [(i, (i + k) % 4) for i in range(4)])]
    ppermute x3 -> x4, waiting for transfers between devices: 4.94 us -> 1.88 us  [swap(): return lax.ppermute(arr, 'c', [(0, 1), (1, 0)])]
    dot_general x1 -> x0, matrix products: 2.98 us -> none  [step(): lax.dot_general(normed, grad_queries, (((0,), (0,)), ((), ())), preferred...]
    pallas_call x5 -> x7, Pallas kernels: 16.1 us -> 18.7 us  [call(): pl.pallas_call(kernel, in_specs=ins, out_specs=[VMEM] * len(out_shape) if...]
    ppermute x6, starting transfers between devices: 19.8 us -> 22.4 us  [x_from(): return lax.ppermute(arr, 'x', [(i, (i + k) % 4) for i in range(4)])]
    ppermute x3 -> x4, starting transfers between devices: 5.75 us -> 7.66 us  [swap(): return lax.ppermute(arr, 'c', [(0, 1), (1, 0)])]
  transfers between devices with their start and end apart: 15 -> 18, of which waited for: 11 -> 8; matrix products, arithmetic and copies ran while one was open for 7% -> 3% of each run, Pallas kernels for 4% -> 10%
where the time goes in v3:
time: 155 us; the launch traced here: 154 us
  starting transfers between devices  68.1 us (44%)
  waiting for transfers between devices  29.7 us (19%)
  Pallas kernels  25.7 us (17%)
  blocking collectives  19.6 us (13%)
  other arithmetic  6.7 us (4%)
  local copies, waits for them, and re-layouts  2.99 us (2%)
    all_to_all x5, starting transfers between devices, along(): lax.all_to_all(arr, ALL, split_axis=0, concat_axis=0, tiled=True, axis_in...  26.9 us
    ppermute x6, starting transfers between devices, x_from(): return lax.ppermute(arr, 'x', [(i, (i + k) % 4) for i in range(4)])  22.4 us
    all_to_all x5, waiting for transfers between devices, along(): lax.all_to_all(arr, ALL, split_axis=0, concat_axis=0, tiled=True, axis_in...  20.9 us
    all_to_all x1, blocking collectives, along(): lax.all_to_all(arr, ALL, split_axis=0, concat_axis=0, tiled=True, axis_in...  19.6 us
    pallas_call x7, Pallas kernels, call(): pl.pallas_call(kernel, in_specs=ins, out_specs=[VMEM] * len(out_shape) if...  18.7 us
    ppermute x3, starting transfers between devices, x_back(): return lax.ppermute(arr, 'x', [((i + k) % 4, i) for i in range(4)])  11.1 us
    ppermute x4, starting transfers between devices, swap(): return lax.ppermute(arr, 'c', [(0, 1), (1, 0)])  7.66 us
    pallas_call x1, Pallas kernels, step(): pl.pallas_call(weight_kernel, grid=(SIDE,), in_specs=[SMEM, pl.BlockSpec(...  7.05 us
  transfers between devices with their start and end apart: 18, of which 8 were waited for; matrix products, arithmetic and copies ran while one was open for 3% of the time, Pallas kernels for 10%

profile of v3, /device:TPU:2, one launch (start us, length us, event | category | flops | bytes accessed | tf_op | source)
XLA Modules:
  0.0 153.7 jit_solution(16371905314655127378)
XLA Ops:
  0.6 1.9 %pack.1.q0 = bf16[1072,128]{1,0:T(8,128)(2,1)} custom-call(bf16[512,128]{1,0:T(8,128)(2,1)} %q_ref.1, bf16[512,128]{1,0:T(8,128)(2,1)} %g_ref.1, bf16[512,128]{1,0:T(8,128)(2,1)} %o_ref.1, f32[2,512]{1,0:T(2,128)} %bitcast.53), custom_call_target="tpu_custom_call" | custom-call | flops 262144 | bytes 1048576 | tf_op jit(solution)/shard_map/pack/pallas_call | solution.py:237
  2.5 7.8 %collective-permute-start.3 = (bf16[1072,128]{1,0:T(8,128)(2,1)}, bf16[1072,128]{1,0:T(8,128)(2,1)S(1)}, u32[]{:S(2)}, u32[]{:S(2)}) collective-permute-start(bf16[1072,128]{1,0:T(8,128)(2,1)} %pack.1.q0), channel_id=1, source_target_pairs={{0,6},{2,0},{4,2},{6,4},{1,7},{3,1},{5,3},{7,5},{8,14},{10,8},{12,... | collective-permute-start | bytes 823304 | tf_op jit(solution)/shard_map/ppermute | solution.py:252
  10.3 1.9 %collective-permute-start.2 = (bf16[1072,128]{1,0:T(8,128)(2,1)}, bf16[1072,128]{1,0:T(8,128)(2,1)S(1)}, u32[]{:S(2)}, u32[]{:S(2)}) collective-permute-start(bf16[1072,128]{1,0:T(8,128)(2,1)} %pack.1.q0), channel_id=1, source_target_pairs={{0,4},{2,6},{4,0},{6,2},{1,5},{3,7},{5,1},{7,3},{8,12},{10,14},{12... | collective-permute-start | bytes 823304 | tf_op jit(solution)/shard_map/ppermute | solution.py:252
  12.2 3.4 %collective-permute-start.1 = (bf16[1072,128]{1,0:T(8,128)(2,1)}, bf16[1072,128]{1,0:T(8,128)(2,1)S(1)}, u32[]{:S(2)}, u32[]{:S(2)}) collective-permute-start(bf16[1072,128]{1,0:T(8,128)(2,1)} %pack.1.q0), channel_id=1, source_target_pairs={{0,2},{2,4},{4,6},{6,0},{1,3},{3,5},{5,7},{7,1},{8,10},{10,12},{12... | collective-permute-start | bytes 823304 | tf_op jit(solution)/shard_map/ppermute | solution.py:252
  15.6 4.8 %collective-permute-done.2.q2 = bf16[1072,128]{1,0:T(8,128)(2,1)S(1)} collective-permute-done((bf16[1072,128]{1,0:T(8,128)(2,1)}, bf16[1072,128]{1,0:T(8,128)(2,1)S(1)}, u32[]{:S(2)}, u32[]{:S(2)}) %collective-permute-start.2) | collective-permute-done | bytes 274464 | tf_op jit(solution)/shard_map/ppermute | solution.py:252
  20.4 2.1 %collective-permute-done.1.q1 = bf16[1072,128]{1,0:T(8,128)(2,1)S(1)} collective-permute-done((bf16[1072,128]{1,0:T(8,128)(2,1)}, bf16[1072,128]{1,0:T(8,128)(2,1)S(1)}, u32[]{:S(2)}, u32[]{:S(2)}) %collective-permute-start.1) | collective-permute-done | bytes 274464 | tf_op jit(solution)/shard_map/ppermute | solution.py:252
  23.8 1.9 %collective-permute-start.4 = (bf16[4,1072,128]{2,1,0:T(8,128)(2,1)S(1)}, bf16[4,1072,128]{2,1,0:T(8,128)(2,1)S(1)}, u32[]{:S(2)}, u32[]{:S(2)}) collective-permute-start(bf16[4,1072,128]{2,1,0:T(8,128)(2,1)S(1)} %pad_maximum_fusion), channel_id=1, source_target_pairs={{0,1},{1,0},{2,3},{3,2},{4,5},{5,4},{6,7},{7,6},{8,9},{9,8},{10,11... | collective-permute-start | bytes 3293192 | tf_op jit(solution)/shard_map/ppermute | solution.py:260
  26.4 1.8 %offer.1 = (bf16[8,9,8,128]{3,2,1,0:T(8,128)(2,1)}, bf16[8,8,128]{2,1,0:T(8,128)(2,1)}) custom-call(s32[3]{0:T(128)} %pad_add_fusion.at_ref, bf16[64,512]{1,0:T(8,128)(2,1)} %bitcast.48, bf16[64,512]{1,0:T(8,128)(2,1)} %bitcast.49, s32[8,16]{1,0:T(8,128)} %chosen_ref.1), custom_call_target="tpu_custom_call" | custom-call | flops 262144 | bytes 1048576 | tf_op jit(solution)/shard_map/offer/pallas_call | solution.py:237
  28.1 19.6 %all_to_all.30.pushed_ref = bf16[8,9,8,128]{3,2,1,0:T(8,128)(2,1)S(1)} all-to-all(bf16[8,9,8,128]{3,2,1,0:T(8,128)(2,1)} %get-tuple-element.12), channel_id=1, replica_groups={{0,64,128,192,256,320,384,448},{8,72,136,200,264,328,392,456},{16,80,14..., dimensions={0} | all-to-all | bytes 294912 | tf_op jit(solution)/shard_map/all_to_all | solution.py:280
  47.7 1.9 %collective-permute-start = (bf16[8,8,128]{2,1,0:T(8,128)(2,1)S(1)}, bf16[8,8,128]{2,1,0:T(8,128)(2,1)S(1)}, u32[]{:S(2)}, u32[]{:S(2)}) collective-permute-start(bf16[8,8,128]{2,1,0:T(8,128)(2,1)S(1)} %slice_bitcast_fusion.4), channel_id=1, source_target_pairs={{0,1},{1,0},{2,3},{3,2},{4,5},{5,4},{6,7},{7,6},{8,9},{9,8},{10,11... | collective-permute-start | bytes 49160 | tf_op jit(solution)/shard_map/ppermute | solution.py:260
  51.4 1.7 %pick.1 = bf16[8,8,8,128]{3,2,1,0:T(8,128)(2,1)} custom-call(bf16[8,8,128]{2,1,0:T(8,128)(2,1)} %copy-done.10, bf16[8,9,8,128]{3,2,1,0:T(8,128)(2,1)} %copy-done), custom_call_target="tpu_custom_call" | custom-call | flops 1048576 | bytes 1048576 | tf_op jit(solution)/shard_map/pick/pallas_call | solution.py:237
  53.1 7.1 %all-to-all-start.1 = ((bf16[8,8,8,128]{3,2,1,0:T(8,128)(2,1)}), bf16[8,8,8,128]{3,2,1,0:T(8,128)(2,1)S(1)}, u32[]{:S(2)}, u32[]{:S(2)}) async-start(bf16[8,8,8,128]{3,2,1,0:T(8,128)(2,1)} %pick.1), calls=%async_computation.1 | async-start | bytes 262144 | tf_op jit(solution)/shard_map/all_to_all | solution.py:280
  60.9 8.4 %all-to-all-done.1 = bf16[8,8,8,128]{3,2,1,0:T(8,128)(2,1)S(1)} async-done(((bf16[8,8,8,128]{3,2,1,0:T(8,128)(2,1)}), bf16[8,8,8,128]{3,2,1,0:T(8,128)(2,1)S(1)}, u32[]{:S(2)}, u32[]{:S(2)}) %all-to-all-start.1) | async-done | bytes 131104 | tf_op jit(solution)/shard_map/all_to_all | solution.py:280
  70.4 8.1 %attend.1 = (bf16[64,8,128]{2,1,0:T(8,128)(2,1)}, f32[8,8,128]{2,1,0:T(8,128)}, f32[4,512,128]{2,1,0:T(8,128)}, bf16[4,512,128]{2,1,0:T(8,128)(2,1)}) custom-call(s32[8,16]{1,0:T(8,128)} %get-tuple-element.26.slot_ref, s32[8,16]{1,0:T(8,128)} %get-tuple-element.25.rel_ref, bf16[64,8,128]{2,1,0:T(8,128)(2,1)} %bitcast.46, ...), custom_call_target="tpu_custom_call" | custom-call | flops 1073741824 | bytes 1048576 | tf_op jit(solution)/shard_map/attend/pallas_call | solution.py:237
  78.5 1.9 %collective-permute-start.5 = (bf16[4,512,128]{2,1,0:T(8,128)(2,1)}, bf16[4,512,128]{2,1,0:T(8,128)(2,1)S(1)}, u32[]{:S(2)}, u32[]{:S(2)}) collective-permute-start(bf16[4,512,128]{2,1,0:T(8,128)(2,1)} %get-tuple-element.15), channel_id=1, source_target_pairs={{0,1},{1,0},{2,3},{3,2},{4,5},{5,4},{6,7},{7,6},{8,9},{9,8},{10,11... | collective-permute-start | bytes 1572872 | tf_op jit(solution)/shard_map/ppermute | solution.py:260
  80.4 3.4 %all-to-all-start.2 = ((bf16[8,8,8,128]{3,2,1,0:T(8,128)(2,1)}), bf16[8,8,8,128]{3,2,1,0:T(8,128)(2,1)S(1)}, u32[]{:S(2)}, u32[]{:S(2)}) async-start(bf16[8,8,8,128]{3,2,1,0:T(8,128)(2,1)} %bitcast.45), calls=%async_computation.2 | async-start | bytes 262144 | tf_op jit(solution)/shard_map/all_to_all | solution.py:280
  85.2 4.6 %collective-permute-start.6 = (bf16[512,128]{1,0:T(8,128)(2,1)S(1)}, bf16[512,128]{1,0:T(8,128)(2,1)S(1)}, u32[]{:S(2)}, u32[]{:S(2)}) collective-permute-start(bf16[512,128]{1,0:T(8,128)(2,1)S(1)} %get-tuple-element.22), channel_id=1, source_target_pairs={{2,0},{4,2},{6,4},{0,6},{3,1},{5,3},{7,5},{1,7},{10,8},{12,10},{14... | collective-permute-start | bytes 393224 | tf_op jit(solution)/shard_map/ppermute | solution.py:256
  89.8 1.9 %collective-permute-start.8 = (bf16[512,128]{1,0:T(8,128)(2,1)S(1)}, bf16[512,128]{1,0:T(8,128)(2,1)S(1)}, u32[]{:S(2)}, u32[]{:S(2)}) collective-permute-start(bf16[512,128]{1,0:T(8,128)(2,1)S(1)} %get-tuple-element.23), channel_id=1, source_target_pairs={{6,0},{0,2},{2,4},{4,6},{7,1},{1,3},{3,5},{5,7},{14,8},{8,10},{10,... | collective-permute-start | bytes 393224 | tf_op jit(solution)/shard_map/ppermute | solution.py:256
  91.8 4.6 %collective-permute-start.7 = (bf16[512,128]{1,0:T(8,128)(2,1)S(1)}, bf16[512,128]{1,0:T(8,128)(2,1)S(1)}, u32[]{:S(2)}, u32[]{:S(2)}) collective-permute-start(bf16[512,128]{1,0:T(8,128)(2,1)S(1)} %get-tuple-element.24), channel_id=1, source_target_pairs={{4,0},{6,2},{0,4},{2,6},{5,1},{7,3},{1,5},{3,7},{12,8},{14,10},{8,... | collective-permute-start | bytes 393224 | tf_op jit(solution)/shard_map/ppermute | solution.py:256
  97.0 1.8 %relay.1 = bf16[8,8,8,128]{3,2,1,0:T(8,128)(2,1)} custom-call(bf16[8,8,128]{2,1,0:T(8,128)(2,1)} %copy-done.10, bf16[8,8,8,128]{3,2,1,0:T(8,128)(2,1)} %copy-done.1), custom_call_target="tpu_custom_call" | custom-call | flops 1048576 | bytes 1048576 | tf_op jit(solution)/shard_map/relay/pallas_call | solution.py:237
  98.8 3.4 %all-to-all-start.3 = ((bf16[8,8,8,128]{3,2,1,0:T(8,128)(2,1)}), bf16[8,8,8,128]{3,2,1,0:T(8,128)(2,1)S(1)}, u32[]{:S(2)}, u32[]{:S(2)}) async-start(bf16[8,8,8,128]{3,2,1,0:T(8,128)(2,1)} %relay.1), calls=%async_computation.3 | async-start | bytes 262144 | tf_op jit(solution)/shard_map/all_to_all | solution.py:280
  102.9 7.1 %product.1 = bf16[64,64,128]{2,1,0:T(8,128)(2,1)} custom-call(s32[3]{0:T(128)} %pad_add_fusion.at_ref, bf16[512,128]{1,0:T(8,128)(2,1)} %fusion.3.grad_ref, bf16[512,4096]{1,0:T(8,128)(2,1)} %normed_ref.1), custom_call_target="tpu_custom_call" | custom-call | flops 536870912 | bytes 5242880 | tf_op jit(solution)/shard_map/product/pallas_call | solution.py:367
  111.2 5.9 %all-to-all-start.4 = ((bf16[8,8,64,128]{3,2,1,0:T(8,128)(2,1)}), bf16[8,8,64,128]{3,2,1,0:T(8,128)(2,1)S(1)}, u32[]{:S(2)}, u32[]{:S(2)}) async-start(bf16[8,8,64,128]{3,2,1,0:T(8,128)(2,1)} %bitcast.40), calls=%async_computation.4 | async-start | bytes 2097152 | tf_op jit(solution)/shard_map/all_to_all | solution.py:280
  117.1 1.6 %settle.1 = f32[8,8,128]{2,1,0:T(8,128)} custom-call(f32[8,8,128]{2,1,0:T(8,128)} %get-tuple-element.16.own_ref, bf16[8,8,8,128]{3,2,1,0:T(8,128)(2,1)} %copy-done.2), custom_call_target="tpu_custom_call" | custom-call | flops 1048576 | bytes 1048576 | tf_op jit(solution)/shard_map/settle/pallas_call | solution.py:237
  118.7 2.2 %collective-permute-start.11 = (f32[8,8,128]{2,1,0:T(8,128)}, f32[8,8,128]{2,1,0:T(8,128)S(1)}, u32[]{:S(2)}, u32[]{:S(2)}) collective-permute-start(f32[8,8,128]{2,1,0:T(8,128)} %settle.1), channel_id=1, source_target_pairs={{0,6},{2,0},{4,2},{6,4},{1,7},{3,1},{5,3},{7,5},{8,14},{10,8},{12,... | collective-permute-start | bytes 98312 | tf_op jit(solution)/shard_map/ppermute | solution.py:252
  120.9 4.0 %collective-permute-start.10 = (f32[8,8,128]{2,1,0:T(8,128)}, f32[8,8,128]{2,1,0:T(8,128)S(1)}, u32[]{:S(2)}, u32[]{:S(2)}) collective-permute-start(f32[8,8,128]{2,1,0:T(8,128)} %settle.1), channel_id=1, source_target_pairs={{0,4},{2,6},{4,0},{6,2},{1,5},{3,7},{5,1},{7,3},{8,12},{10,14},{12... | collective-permute-start | bytes 98312 | tf_op jit(solution)/shard_map/ppermute | solution.py:252
  124.9 3.1 %collective-permute-start.9 = (f32[8,8,128]{2,1,0:T(8,128)}, f32[8,8,128]{2,1,0:T(8,128)S(1)}, u32[]{:S(2)}, u32[]{:S(2)}) collective-permute-start(f32[8,8,128]{2,1,0:T(8,128)} %settle.1), channel_id=1, source_target_pairs={{0,2},{2,4},{4,6},{6,0},{1,3},{3,5},{5,7},{7,1},{8,10},{10,12},{12... | collective-permute-start | bytes 98312 | tf_op jit(solution)/shard_map/ppermute | solution.py:252
  128.1 8.0 %all-to-all-done.4 = bf16[8,8,64,128]{3,2,1,0:T(8,128)(2,1)S(1)} async-done(((bf16[8,8,64,128]{3,2,1,0:T(8,128)(2,1)}), bf16[8,8,64,128]{3,2,1,0:T(8,128)(2,1)S(1)}, u32[]{:S(2)}, u32[]{:S(2)}) %all-to-all-start.4) | async-done | bytes 1048608 | tf_op jit(solution)/shard_map/all_to_all | solution.py:280
  136.9 7.1 %all-to-all-start.5 = ((bf16[8,64,128]{2,1,0:T(8,128)(2,1)}), bf16[8,64,128]{2,1,0:T(8,128)(2,1)S(1)}, u32[]{:S(2)}, u32[]{:S(2)}) async-start(bf16[8,64,128]{2,1,0:T(8,128)(2,1)} %reduce_sum.21), calls=%async_computation.5 | async-start | bytes 262144 | tf_op jit(solution)/shard_map/all_to_all | solution.py:280
  144.1 1.9 %collective-permute-start.12 = (f32[4,8,8,128]{3,2,1,0:T(8,128)S(1)}, f32[4,8,8,128]{3,2,1,0:T(8,128)S(1)}, u32[]{:S(2)}, u32[]{:S(2)}) collective-permute-start(f32[4,8,8,128]{3,2,1,0:T(8,128)S(1)} %pad_maximum_fusion.1.near_ref), channel_id=1, source_target_pairs={{0,1},{1,0},{2,3},{3,2},{4,5},{5,4},{6,7},{7,6},{8,9},{9,8},{10,11... | collective-permute-start | bytes 393224 | tf_op jit(solution)/shard_map/ppermute | solution.py:260
  148.0 1.8 %place.1 = (f32[64,512]{1,0:T(8,128)}, f32[64,512]{1,0:T(8,128)}) custom-call(s32[2]{0:T(128)} %pad_add_fusion.1.at_ref, f32[4,8,8,128]{3,2,1,0:T(8,128)} %copy-done.3, f32[4,8,8,128]{3,2,1,0:T(8,128)} %copy-done.8), custom_call_target="tpu_custom_call" | custom-call | flops 1048576 | bytes 1048576 | tf_op jit(solution)/shard_map/place/pallas_call | solution.py:237
  149.8 3.3 %all-to-all-done.5 = bf16[8,64,128]{2,1,0:T(8,128)(2,1)S(1)} async-done(((bf16[8,64,128]{2,1,0:T(8,128)(2,1)}), bf16[8,64,128]{2,1,0:T(8,128)(2,1)S(1)}, u32[]{:S(2)}, u32[]{:S(2)}) %all-to-all-start.5) | async-done | bytes 131104 | tf_op jit(solution)/shard_map/all_to_all | solution.py:280
  (51 shorter events, 12.8 us)
Async XLA Ops:
  2.5 13.1 %collective-permute-start.3 = (bf16[1072,128]{1,0:T(8,128)(2,1)}, bf16[1072,128]{1,0:T(8,128)(2,1)S(1)}, u32[]{:S(2)}, u32[]{:S(2)}) collective-permute-start(bf16[1072,128]{1,0:T(8,128)(2,1)} %pack.1.q0), channel_id=1, source_target_pairs={{0,6},{2,0},{4,2},{6,4},{1,7},{3,1},{5,3},{7,5},{8,14},{10,8},{12,... | collective-permute-start | bytes 823304 | tf_op jit(solution)/shard_map/ppermute | solution.py:252
  10.3 10.1 %collective-permute-start.2 = (bf16[1072,128]{1,0:T(8,128)(2,1)}, bf16[1072,128]{1,0:T(8,128)(2,1)S(1)}, u32[]{:S(2)}, u32[]{:S(2)}) collective-permute-start(bf16[1072,128]{1,0:T(8,128)(2,1)} %pack.1.q0), channel_id=1, source_target_pairs={{0,4},{2,6},{4,0},{6,2},{1,5},{3,7},{5,1},{7,3},{8,12},{10,14},{12... | collective-permute-start | bytes 823304 | tf_op jit(solution)/shard_map/ppermute | solution.py:252
  12.2 10.3 %collective-permute-start.1 = (bf16[1072,128]{1,0:T(8,128)(2,1)}, bf16[1072,128]{1,0:T(8,128)(2,1)S(1)}, u32[]{:S(2)}, u32[]{:S(2)}) collective-permute-start(bf16[1072,128]{1,0:T(8,128)(2,1)} %pack.1.q0), channel_id=1, source_target_pairs={{0,2},{2,4},{4,6},{6,0},{1,3},{3,5},{5,7},{7,1},{8,10},{10,12},{12... | collective-permute-start | bytes 823304 | tf_op jit(solution)/shard_map/ppermute | solution.py:252
  15.6 8.1 %copy-start.4 = (bf16[1072,128]{1,0:T(8,128)(2,1)}, bf16[1072,128]{1,0:T(8,128)(2,1)S(1)}, u32[]{:S(2)}) copy-start(bf16[1072,128]{1,0:T(8,128)(2,1)S(1)} %collective-permute-done.3.q3) | copy-start | bytes 823300
  20.4 3.3 %copy-start.5 = (bf16[1072,128]{1,0:T(8,128)(2,1)}, bf16[1072,128]{1,0:T(8,128)(2,1)S(1)}, u32[]{:S(2)}) copy-start(bf16[1072,128]{1,0:T(8,128)(2,1)S(1)} %collective-permute-done.2.q2) | copy-start | bytes 823300
  22.5 1.2 copy-start.6
  22.5 37.7 %copy-start.11 = (s32[8,16]{1,0:T(8,128)S(1)}, s32[8,16]{1,0:T(8,128)}, u32[]{:S(2)}) copy-start(s32[8,16]{1,0:T(8,128)} %chosen_ref.1) | copy-start | bytes 1540
  23.8 45.6 %collective-permute-start.4 = (bf16[4,1072,128]{2,1,0:T(8,128)(2,1)S(1)}, bf16[4,1072,128]{2,1,0:T(8,128)(2,1)S(1)}, u32[]{:S(2)}, u32[]{:S(2)}) collective-permute-start(bf16[4,1072,128]{2,1,0:T(8,128)(2,1)S(1)} %pad_maximum_fusion), channel_id=1, source_target_pairs={{0,1},{1,0},{2,3},{3,2},{4,5},{5,4},{6,7},{7,6},{8,9},{9,8},{10,11... | collective-permute-start | bytes 3293192 | tf_op jit(solution)/shard_map/ppermute | solution.py:260
  47.7 3.1 %copy-start = (bf16[8,9,8,128]{3,2,1,0:T(8,128)(2,1)}, bf16[8,9,8,128]{3,2,1,0:T(8,128)(2,1)S(1)}, u32[]{:S(2)}) copy-start(bf16[8,9,8,128]{3,2,1,0:T(8,128)(2,1)S(1)} %all_to_all.30.pushed_ref) | copy-start | bytes 442372
  47.7 3.1 %collective-permute-start = (bf16[8,8,128]{2,1,0:T(8,128)(2,1)S(1)}, bf16[8,8,128]{2,1,0:T(8,128)(2,1)S(1)}, u32[]{:S(2)}, u32[]{:S(2)}) collective-permute-start(bf16[8,8,128]{2,1,0:T(8,128)(2,1)S(1)} %slice_bitcast_fusion.4), channel_id=1, source_target_pairs={{0,1},{1,0},{2,3},{3,2},{4,5},{5,4},{6,7},{7,6},{8,9},{9,8},{10,11... | collective-permute-start | bytes 49160 | tf_op jit(solution)/shard_map/ppermute | solution.py:260
  50.8 0.6 copy-start.10
  53.1 16.2 %all-to-all-start.1 = ((bf16[8,8,8,128]{3,2,1,0:T(8,128)(2,1)}), bf16[8,8,8,128]{3,2,1,0:T(8,128)(2,1)S(1)}, u32[]{:S(2)}, u32[]{:S(2)}) async-start(bf16[8,8,8,128]{3,2,1,0:T(8,128)(2,1)} %pick.1), calls=%async_computation.1 | async-start | bytes 262144 | tf_op jit(solution)/shard_map/all_to_all | solution.py:280
  69.3 0.7 copy-start.7
  69.3 1.0 copy-start.12
  78.5 5.3 %collective-permute-start.5 = (bf16[4,512,128]{2,1,0:T(8,128)(2,1)}, bf16[4,512,128]{2,1,0:T(8,128)(2,1)S(1)}, u32[]{:S(2)}, u32[]{:S(2)}) collective-permute-start(bf16[4,512,128]{2,1,0:T(8,128)(2,1)} %get-tuple-element.15), channel_id=1, source_target_pairs={{0,1},{1,0},{2,3},{3,2},{4,5},{5,4},{6,7},{7,6},{8,9},{9,8},{10,11... | collective-permute-start | bytes 1572872 | tf_op jit(solution)/shard_map/ppermute | solution.py:260
  80.4 15.9 %all-to-all-start.2 = ((bf16[8,8,8,128]{3,2,1,0:T(8,128)(2,1)}), bf16[8,8,8,128]{3,2,1,0:T(8,128)(2,1)S(1)}, u32[]{:S(2)}, u32[]{:S(2)}) async-start(bf16[8,8,8,128]{3,2,1,0:T(8,128)(2,1)} %bitcast.45), calls=%async_computation.2 | async-start | bytes 262144 | tf_op jit(solution)/shard_map/all_to_all | solution.py:280
  85.2 17.0 %collective-permute-start.6 = (bf16[512,128]{1,0:T(8,128)(2,1)S(1)}, bf16[512,128]{1,0:T(8,128)(2,1)S(1)}, u32[]{:S(2)}, u32[]{:S(2)}) collective-permute-start(bf16[512,128]{1,0:T(8,128)(2,1)S(1)} %get-tuple-element.22), channel_id=1, source_target_pairs={{2,0},{4,2},{6,4},{0,6},{3,1},{5,3},{7,5},{1,7},{10,8},{12,10},{14... | collective-permute-start | bytes 393224 | tf_op jit(solution)/shard_map/ppermute | solution.py:256
  89.8 12.4 %collective-permute-start.8 = (bf16[512,128]{1,0:T(8,128)(2,1)S(1)}, bf16[512,128]{1,0:T(8,128)(2,1)S(1)}, u32[]{:S(2)}, u32[]{:S(2)}) collective-permute-start(bf16[512,128]{1,0:T(8,128)(2,1)S(1)} %get-tuple-element.23), channel_id=1, source_target_pairs={{6,0},{0,2},{2,4},{4,6},{7,1},{1,3},{3,5},{5,7},{14,8},{8,10},{10,... | collective-permute-start | bytes 393224 | tf_op jit(solution)/shard_map/ppermute | solution.py:256
  91.8 10.4 %collective-permute-start.7 = (bf16[512,128]{1,0:T(8,128)(2,1)S(1)}, bf16[512,128]{1,0:T(8,128)(2,1)S(1)}, u32[]{:S(2)}, u32[]{:S(2)}) collective-permute-start(bf16[512,128]{1,0:T(8,128)(2,1)S(1)} %get-tuple-element.24), channel_id=1, source_target_pairs={{4,0},{6,2},{0,4},{2,6},{5,1},{7,3},{1,5},{3,7},{12,8},{14,10},{8,... | collective-permute-start | bytes 393224 | tf_op jit(solution)/shard_map/ppermute | solution.py:256
  96.4 0.7 copy-start.1
  98.8 12.4 %all-to-all-start.3 = ((bf16[8,8,8,128]{3,2,1,0:T(8,128)(2,1)}), bf16[8,8,8,128]{3,2,1,0:T(8,128)(2,1)S(1)}, u32[]{:S(2)}, u32[]{:S(2)}) async-start(bf16[8,8,8,128]{3,2,1,0:T(8,128)(2,1)} %relay.1), calls=%async_computation.3 | async-start | bytes 262144 | tf_op jit(solution)/shard_map/all_to_all | solution.py:280
  111.2 5.9 %copy-start.2 = (bf16[8,8,8,128]{3,2,1,0:T(8,128)(2,1)}, bf16[8,8,8,128]{3,2,1,0:T(8,128)(2,1)S(1)}, u32[]{:S(2)}) copy-start(bf16[8,8,8,128]{3,2,1,0:T(8,128)(2,1)S(1)} %all-to-all-done.3.given_ref) | copy-start | bytes 393220
  111.2 24.9 %all-to-all-start.4 = ((bf16[8,8,64,128]{3,2,1,0:T(8,128)(2,1)}), bf16[8,8,64,128]{3,2,1,0:T(8,128)(2,1)S(1)}, u32[]{:S(2)}, u32[]{:S(2)}) async-start(bf16[8,8,64,128]{3,2,1,0:T(8,128)(2,1)} %bitcast.40), calls=%async_computation.4 | async-start | bytes 2097152 | tf_op jit(solution)/shard_map/all_to_all | solution.py:280
  118.7 25.4 %copy-start.9 = (f32[8,8,128]{2,1,0:T(8,128)S(1)}, f32[8,8,128]{2,1,0:T(8,128)}, u32[]{:S(2)}) copy-start(f32[8,8,128]{2,1,0:T(8,128)} %settle.1) | copy-start | bytes 98308
  118.7 25.3 %collective-permute-start.11 = (f32[8,8,128]{2,1,0:T(8,128)}, f32[8,8,128]{2,1,0:T(8,128)S(1)}, u32[]{:S(2)}, u32[]{:S(2)}) collective-permute-start(f32[8,8,128]{2,1,0:T(8,128)} %settle.1), channel_id=1, source_target_pairs={{0,6},{2,0},{4,2},{6,4},{1,7},{3,1},{5,3},{7,5},{8,14},{10,8},{12,... | collective-permute-start | bytes 98312 | tf_op jit(solution)/shard_map/ppermute | solution.py:252
  120.9 23.2 %collective-permute-start.10 = (f32[8,8,128]{2,1,0:T(8,128)}, f32[8,8,128]{2,1,0:T(8,128)S(1)}, u32[]{:S(2)}, u32[]{:S(2)}) collective-permute-start(f32[8,8,128]{2,1,0:T(8,128)} %settle.1), channel_id=1, source_target_pairs={{0,4},{2,6},{4,0},{6,2},{1,5},{3,7},{5,1},{7,3},{8,12},{10,14},{12... | collective-permute-start | bytes 98312 | tf_op jit(solution)/shard_map/ppermute | solution.py:252
  124.9 19.1 %collective-permute-start.9 = (f32[8,8,128]{2,1,0:T(8,128)}, f32[8,8,128]{2,1,0:T(8,128)S(1)}, u32[]{:S(2)}, u32[]{:S(2)}) collective-permute-start(f32[8,8,128]{2,1,0:T(8,128)} %settle.1), channel_id=1, source_target_pairs={{0,2},{2,4},{4,6},{6,0},{1,3},{3,5},{5,7},{7,1},{8,10},{10,12},{12... | collective-permute-start | bytes 98312 | tf_op jit(solution)/shard_map/ppermute | solution.py:252
  136.9 16.2 %all-to-all-start.5 = ((bf16[8,64,128]{2,1,0:T(8,128)(2,1)}), bf16[8,64,128]{2,1,0:T(8,128)(2,1)S(1)}, u32[]{:S(2)}, u32[]{:S(2)}) async-start(bf16[8,64,128]{2,1,0:T(8,128)(2,1)} %reduce_sum.21), calls=%async_computation.5 | async-start | bytes 262144 | tf_op jit(solution)/shard_map/all_to_all | solution.py:280
  144.1 3.3 %copy-start.3 = (f32[4,8,8,128]{3,2,1,0:T(8,128)}, f32[4,8,8,128]{3,2,1,0:T(8,128)S(1)}, u32[]{:S(2)}) copy-start(f32[4,8,8,128]{3,2,1,0:T(8,128)S(1)} %pad_maximum_fusion.1.near_ref) | copy-start | bytes 393220
  144.1 3.2 %collective-permute-start.12 = (f32[4,8,8,128]{3,2,1,0:T(8,128)S(1)}, f32[4,8,8,128]{3,2,1,0:T(8,128)S(1)}, u32[]{:S(2)}, u32[]{:S(2)}) collective-permute-start(f32[4,8,8,128]{3,2,1,0:T(8,128)S(1)} %pad_maximum_fusion.1.near_ref), channel_id=1, source_target_pairs={{0,1},{1,0},{2,3},{3,2},{4,5},{5,4},{6,7},{7,6},{8,9},{9,8},{10,11... | collective-permute-start | bytes 393224 | tf_op jit(solution)/shard_map/ppermute | solution.py:260
  147.3 0.7 copy-start.8

commit v4 on v3

--- a/solution.py
+++ b/solution.py
@@ -29,10 +29,10 @@
     return lax.broadcasted_iota(jnp.int32, shape, len(shape) - 1) < LANES // 2
 
 
-def offer_kernel(at_ref, keys_ref, vals_ref, chosen_ref, out_ref, piece_ref, pairs):
-    rank = at_ref[0]
-    tp = at_ref[1]
-    flip = at_ref[2]
+def offer_kernel(rank_ref, tp_ref, keys_ref, vals_ref, chosen_ref, out_ref, piece_ref, pairs):
+    rank = rank_ref[0]
+    tp = tp_ref[0]
+    flip = tp & 1
     both = jnp.concatenate([keys_ref[...], vals_ref[...]], axis=0).astype(F32)
     pairs[...] = both.T
     at = lax.broadcasted_iota(jnp.int32, (PEERS, SLOTS), 0)
@@ -83,23 +83,6 @@
         for i in range(SIDE):
             total = total + given_ref[i, b].astype(F32)
         out_ref[b] = total
-
-
-def weight_kernel(at_ref, grad_ref, normed_ref, out_ref, grad_t):
-    i = pl.program_id(0)
-    flip = at_ref[2]
-
-    @pl.when(i == 0)
-    def _():
-        grad_t[...] = grad_ref[...].astype(F32).T.astype(BF16)
-
-    part = lax.dot_general(
-        grad_t[...], normed_ref[...], (((1,), (0,)), ((), ())), preferred_element_type=F32
-    )
-    part = part.T.astype(BF16)
-    for n in range(SIDE):
-        at = jnp.where(flip == 0, i * SIDE + n, n * SIDE + i)
-        out_ref[at] = part[n * BLOCK : (n + 1) * BLOCK]
 
 
 def pack_kernel(q_ref, g_ref, o_ref, log_ref, out_ref):
@@ -218,9 +201,9 @@
     own_ref[...] = acc[PEERS:]
 
 
-def place_kernel(at_ref, near_ref, far_ref, keys_ref, vals_ref, rows):
-    x = at_ref[0]
-    mine = jnp.full((ROWS, LANES), at_ref[1], jnp.int32)
+def place_kernel(tp_ref, near_ref, far_ref, keys_ref, vals_ref, rows):
+    x = tp_ref[0] >> 1
+    mine = jnp.full((ROWS, LANES), tp_ref[0] & 1, jnp.int32)
     for xa in range(4):
         k = (x + 4 - xa) & 3
         for ca in range(2):
@@ -240,12 +223,17 @@
         out_specs=[VMEM] * len(out_shape) if many else VMEM,
         out_shape=out_shape,
         cost_estimate=pl.CostEstimate(flops=flops, bytes_accessed=1 << 20, transcendentals=0),
+        compiler_params=pltpu.CompilerParams(vmem_limit_bytes=24 << 20),
         **kw,
     )(*args)
 
 
 def sds(shape, dtype):
     return jax.ShapeDtypeStruct(shape, dtype)
+
+
+def held(shape, dtype):
+    return pltpu.VMEM(shape, dtype)
 
 
 def x_from(arr, k):
@@ -282,20 +270,27 @@
     )
 
 
+def exchange(arr):
+    return lax.all_to_all(arr, KV, split_axis=0, concat_axis=0, tiled=True)
+
+
+def near_core(arr):
+    return pltpu.with_memory_space_constraint(arr, pltpu.VMEM)
+
+
 def step(normed, queries, keys, values, attended, cotangent, log_sum, chosen):
     rank = lax.axis_index(KV).astype(jnp.int32)
     x = lax.axis_index("x").astype(jnp.int32)
     c = lax.axis_index("c").astype(jnp.int32)
     tp = x * 2 + c
-    spot = jnp.stack([rank, tp, c])
     offer, piece = call(
         offer_kernel,
-        [SMEM] + [VMEM] * 3,
+        [SMEM] * 2 + [VMEM] * 3,
         [
-            sds((SIDE, BLOCKS + 1, ROWS, LANES), BF16),
-            sds((BLOCKS, ROWS, LANES), BF16),
+            held((SIDE, BLOCKS + 1, ROWS, LANES), BF16),
+            held((BLOCKS, ROWS, LANES), BF16),
         ],
-        (spot, keys.T, values.T, chosen),
+        (rank.reshape(1), tp.reshape(1), keys.T, values.T, chosen),
         1 << 18,
         scratch_shapes=[pltpu.VMEM((TOK, LANES), F32)],
         name="offer",
@@ -305,8 +300,8 @@
     picked = call(
         pick_kernel,
         [VMEM] * 2,
-        sds((SIDE, SIDE, ROWS, LANES), BF16),
-        (wants, pushed),
+        held((SIDE, SIDE, ROWS, LANES), BF16),
+        (near_core(wants), near_core(pushed)),
         1 << 20,
         name="pick",
     )
@@ -315,7 +310,7 @@
     qd = call(
         pack_kernel,
         [VMEM] * 4,
-        sds((2 * TOK + 48, LANES), BF16),
+        held((2 * TOK + 48, LANES), BF16),
         (queries, cotangent, attended, log_sum.T),
         1 << 18,
         name="pack",
@@ -335,12 +330,12 @@
         attend_kernel,
         [SMEM] * 2 + [VMEM] * 7,
         [
-            sds((PEERS, ROWS, LANES), BF16),
-            sds((BLOCKS, ROWS, LANES), F32),
-            sds((4, TOK, LANES), F32),
-            sds((4, TOK, LANES), BF16),
+            held((PEERS, ROWS, LANES), BF16),
+            held((BLOCKS, ROWS, LANES), F32),
+            held((4, TOK, LANES), F32),
+            held((4, TOK, LANES), BF16),
         ],
-        (slot, rel, fetched, piece, *qds, qd_far),
+        (slot, rel, near_core(fetched), near_core(piece), *map(near_core, qds), near_core(qd_far)),
         1 << 30,
         scratch_shapes=[
             pltpu.VMEM((BLOCKS, 8, TOK), F32),
@@ -354,8 +349,8 @@
     relayed = call(
         relay_kernel,
         [VMEM] * 2,
-        sds((SIDE, BLOCKS, ROWS, LANES), BF16),
-        (wants, given),
+        held((SIDE, BLOCKS, ROWS, LANES), BF16),
+        (near_core(wants), near_core(given)),
         1 << 20,
         name="relay",
     )
@@ -364,30 +359,17 @@
     for k in (1, 2, 3):
         gq = gq + x_back(gq4[k].astype(BF16), k).astype(F32)
     grad_queries = gq.astype(BF16)
-    part = pl.pallas_call(
-        weight_kernel,
-        grid=(SIDE,),
-        in_specs=[
-            SMEM,
-            pl.BlockSpec((TOK, LANES), lambda i: (0, 0)),
-            pl.BlockSpec((TOK, TOK), lambda i: (0, i)),
-        ],
-        out_specs=pl.BlockSpec((PEERS, BLOCK, LANES), lambda i: (0, 0, 0)),
-        out_shape=sds((PEERS, BLOCK, LANES), BF16),
-        scratch_shapes=[pltpu.VMEM((LANES, TOK), BF16)],
-        cost_estimate=pl.CostEstimate(flops=1 << 29, bytes_accessed=5 << 20, transcendentals=0),
-        name="product",
-    )(spot, grad_queries, normed)
-    parts = along(part.reshape(SIDE, SIDE, BLOCK, LANES), True)
-    half = jnp.sum(parts.astype(F32), axis=0).astype(BF16)
-    parts = along(half, False)
+    part = lax.dot_general(
+        normed, grad_queries, (((0,), (0,)), ((), ())), preferred_element_type=F32
+    ).astype(BF16)
+    parts = exchange(part.reshape(PEERS, BLOCK, LANES))
     weight_grad = jnp.sum(parts.astype(F32), axis=0)
 
     total = call(
         settle_kernel,
         [VMEM] * 2,
-        sds((BLOCKS, ROWS, LANES), F32),
-        (own, returned),
+        held((BLOCKS, ROWS, LANES), F32),
+        (near_core(own), near_core(returned)),
         1 << 20,
         name="settle",
     )
@@ -397,7 +379,7 @@
         place_kernel,
         [SMEM, VMEM, VMEM],
         [sds((64, TOK), F32), sds((64, TOK), F32)],
-        (jnp.stack([x, c]), near, far),
+        (tp.reshape(1), near_core(near), near_core(far)),
         1 << 20,
         scratch_shapes=[pltpu.VMEM((TOK, LANES), F32)],
         name="place",

time: 155 us -> 145 us (0.935)
  Pallas kernels: 25.7 us -> 9.7 us
  waiting for transfers between devices: 29.7 us -> 38.4 us
  starting transfers between devices: 68.1 us -> 63.8 us
  other arithmetic: 6.7 us -> 3.27 us
  matrix products: 0 us -> 2.98 us
  local copies, waits for them, and re-layouts: 2.99 us -> 5.54 us
    all_to_all x5 -> x3, starting transfers between devices: 26.9 us -> 13.9 us  [along(): lax.all_to_all(arr, ALL, split_axis=0, concat_axis=0, tiled=True, axis_in...]
    all_to_all x0 -> x1, waiting for transfers between devices: none -> 13 us  [exchange(): return lax.all_to_all(arr, KV, split_axis=0, concat_axis=0, tiled=True)]
    pallas_call x7, Pallas kernels: 18.7 us -> 9.7 us  [call(): pl.pallas_call(kernel, in_specs=ins, out_specs=[VMEM] * len(out_shape) if...]
    all_to_all x0 -> x1, starting transfers between devices: none -> 8.85 us  [exchange(): return lax.all_to_all(arr, KV, split_axis=0, concat_axis=0, tiled=True)]
    all_to_all x5 -> x3, waiting for transfers between devices: 20.9 us -> 13.4 us  [along(): lax.all_to_all(arr, ALL, split_axis=0, concat_axis=0, tiled=True, axis_in...]
    pallas_call x1 -> x0, Pallas kernels: 7.05 us -> none  [step(): pl.pallas_call(weight_kernel, grid=(SIDE,), in_specs=[SMEM, pl.BlockSpec(...]
    dot_general x0 -> x1, matrix products: none -> 2.98 us  [step(): lax.dot_general(normed, grad_queries, (((0,), (0,)), ((), ())), preferred...]
    ppermute x6, waiting for transfers between devices: 6.88 us -> 9.34 us  [x_from(): return lax.ppermute(arr, 'x', [(i, (i + k) % 4) for i in range(4)])]
  transfers between devices with their start and end apart: 18 -> 17, of which waited for: 8 -> 10; matrix products, arithmetic and copies ran while one was open for 3% -> 4% of each run, Pallas kernels for 10% -> 2%
where the time goes in v4:
time: 145 us; the launch traced here: 144 us
  starting transfers between devices  63.8 us (44%)
  waiting for transfers between devices  38.4 us (26%)
  blocking collectives  19.4 us (13%)
  Pallas kernels  9.7 us (7%)
  local copies, waits for them, and re-layouts  5.54 us (4%)
  other arithmetic  3.27 us (2%)
  matrix products  2.98 us (2%)
    ppermute x6, starting transfers between devices, x_from(): return lax.ppermute(arr, 'x', [(i, (i + k) % 4) for i in range(4)])  22.3 us
    all_to_all x1, blocking collectives, along(): lax.all_to_all(arr, ALL, split_axis=0, concat_axis=0, tiled=True, axis_in...  19.4 us
    all_to_all x3, starting transfers between devices, along(): lax.all_to_all(arr, ALL, split_axis=0, concat_axis=0, tiled=True, axis_in...  13.9 us
    all_to_all x3, waiting for transfers between devices, along(): lax.all_to_all(arr, ALL, split_axis=0, concat_axis=0, tiled=True, axis_in...  13.4 us
    all_to_all x1, waiting for transfers between devices, exchange(): return lax.all_to_all(arr, KV, split_axis=0, concat_axis=0, tiled=True)  13 us
    ppermute x3, starting transfers between devices, x_back(): return lax.ppermute(arr, 'x', [((i + k) % 4, i) for i in range(4)])  11.1 us
    pallas_call x7, Pallas kernels, call(): pl.pallas_call(kernel, in_specs=ins, out_specs=[VMEM] * len(out_shape) if...  9.7 us
    ppermute x6, waiting for transfers between devices, x_from(): return lax.ppermute(arr, 'x', [(i, (i + k) % 4) for i in range(4)])  9.34 us
  transfers between devices with their start and end apart: 17, of which 10 were waited for; matrix products, arithmetic and copies ran while one was open for 4% of the time, Pallas kernels for 2%

profile of v4, /device:TPU:2, one launch (start us, length us, event | category | flops | bytes accessed | tf_op | source)
XLA Modules:
  0.0 144.0 jit_solution(2829661356851357388)
XLA Ops:
  1.5 0.9 copy-done.1
  4.2 7.8 %collective-permute-start.3 = (bf16[1072,128]{1,0:T(8,128)(2,1)S(1)}, bf16[1072,128]{1,0:T(8,128)(2,1)S(1)}, u32[]{:S(2)}, u32[]{:S(2)}) collective-permute-start(bf16[1072,128]{1,0:T(8,128)(2,1)S(1)} %pack.1.q0), channel_id=1, source_target_pairs={{0,6},{2,0},{4,2},{6,4},{1,7},{3,1},{5,3},{7,5},{8,14},{10,8},{12,... | collective-permute-start | bytes 823304 | tf_op jit(solution)/shard_map/ppermute | solution.py:240
  12.0 1.9 %collective-permute-start.2 = (bf16[1072,128]{1,0:T(8,128)(2,1)S(1)}, bf16[1072,128]{1,0:T(8,128)(2,1)S(1)}, u32[]{:S(2)}, u32[]{:S(2)}) collective-permute-start(bf16[1072,128]{1,0:T(8,128)(2,1)S(1)} %pack.1.q0), channel_id=1, source_target_pairs={{0,4},{2,6},{4,0},{6,2},{1,5},{3,7},{5,1},{7,3},{8,12},{10,14},{12... | collective-permute-start | bytes 823304 | tf_op jit(solution)/shard_map/ppermute | solution.py:240
  13.9 3.4 %collective-permute-start.1 = (bf16[1072,128]{1,0:T(8,128)(2,1)S(1)}, bf16[1072,128]{1,0:T(8,128)(2,1)S(1)}, u32[]{:S(2)}, u32[]{:S(2)}) collective-permute-start(bf16[1072,128]{1,0:T(8,128)(2,1)S(1)} %pack.1.q0), channel_id=1, source_target_pairs={{0,2},{2,4},{4,6},{6,0},{1,3},{3,5},{5,7},{7,1},{8,10},{10,12},{12... | collective-permute-start | bytes 823304 | tf_op jit(solution)/shard_map/ppermute | solution.py:240
  17.3 4.6 %collective-permute-done.2.q2 = bf16[1072,128]{1,0:T(8,128)(2,1)S(1)} collective-permute-done((bf16[1072,128]{1,0:T(8,128)(2,1)S(1)}, bf16[1072,128]{1,0:T(8,128)(2,1)S(1)}, u32[]{:S(2)}, u32[]{:S(2)}) %collective-permute-start.2) | collective-permute-done | bytes 274464 | tf_op jit(solution)/shard_map/ppermute | solution.py:240
  21.9 2.1 %collective-permute-done.1.q1 = bf16[1072,128]{1,0:T(8,128)(2,1)S(1)} collective-permute-done((bf16[1072,128]{1,0:T(8,128)(2,1)S(1)}, bf16[1072,128]{1,0:T(8,128)(2,1)S(1)}, u32[]{:S(2)}, u32[]{:S(2)}) %collective-permute-start.1) | collective-permute-done | bytes 274464 | tf_op jit(solution)/shard_map/ppermute | solution.py:240
  24.0 1.1 pad_maximum_fusion
  25.1 1.9 %collective-permute-start.4 = (bf16[4,1072,128]{2,1,0:T(8,128)(2,1)}, bf16[4,1072,128]{2,1,0:T(8,128)(2,1)S(1)}, u32[]{:S(2)}, u32[]{:S(2)}) collective-permute-start(bf16[4,1072,128]{2,1,0:T(8,128)(2,1)} %pad_maximum_fusion), channel_id=1, source_target_pairs={{0,1},{1,0},{2,3},{3,2},{4,5},{5,4},{6,7},{7,6},{8,9},{9,8},{10,11... | collective-permute-start | bytes 3293192 | tf_op jit(solution)/shard_map/ppermute | solution.py:248
  27.3 19.4 %all_to_all.25.pushed_ref = bf16[8,9,8,128]{3,2,1,0:T(8,128)(2,1)S(1)} all-to-all(bf16[8,9,8,128]{3,2,1,0:T(8,128)(2,1)S(1)} %get-tuple-element.12), channel_id=1, replica_groups={{0,64,128,192,256,320,384,448},{8,72,136,200,264,328,392,456},{16,80,14..., dimensions={0} | all-to-all | bytes 294912 | tf_op jit(solution)/shard_map/all_to_all | solution.py:268
  46.7 1.9 %collective-permute-start = (bf16[8,8,128]{2,1,0:T(8,128)(2,1)S(1)}, bf16[8,8,128]{2,1,0:T(8,128)(2,1)S(1)}, u32[]{:S(2)}, u32[]{:S(2)}) collective-permute-start(bf16[8,8,128]{2,1,0:T(8,128)(2,1)S(1)} %slice_bitcast_fusion.4), channel_id=1, source_target_pairs={{0,1},{1,0},{2,3},{3,2},{4,5},{5,4},{6,7},{7,6},{8,9},{9,8},{10,11... | collective-permute-start | bytes 49160 | tf_op jit(solution)/shard_map/ppermute | solution.py:248
  48.6 1.1 collective-permute-done.wants_ref
  50.6 7.1 %all-to-all-start.1 = ((bf16[8,8,8,128]{3,2,1,0:T(8,128)(2,1)}), bf16[8,8,8,128]{3,2,1,0:T(8,128)(2,1)S(1)}, u32[]{:S(2)}, u32[]{:S(2)}) async-start(bf16[8,8,8,128]{3,2,1,0:T(8,128)(2,1)} %pick.1), calls=%async_computation.1 | async-start | bytes 262144 | tf_op jit(solution)/shard_map/all_to_all | solution.py:268
  57.8 9.0 %all-to-all-done.1 = bf16[8,8,8,128]{3,2,1,0:T(8,128)(2,1)S(1)} async-done(((bf16[8,8,8,128]{3,2,1,0:T(8,128)(2,1)}), bf16[8,8,8,128]{3,2,1,0:T(8,128)(2,1)S(1)}, u32[]{:S(2)}, u32[]{:S(2)}) %all-to-all-start.1) | async-done | bytes 131104 | tf_op jit(solution)/shard_map/all_to_all | solution.py:268
  66.8 6.8 %attend.1 = (bf16[64,8,128]{2,1,0:T(8,128)(2,1)}, f32[8,8,128]{2,1,0:T(8,128)S(1)}, f32[4,512,128]{2,1,0:T(8,128)S(1)}, bf16[4,512,128]{2,1,0:T(8,128)(2,1)}) custom-call(s32[8,16]{1,0:T(8,128)S(1)} %get-tuple-element.26.slot_ref, s32[8,16]{1,0:T(8,128)S(1)} %get-tuple-element.25.rel_ref, bf16[64,8,128]{2,1,0:T(8,128)(2,1)S(1)} %bitcast.46, ...), custom_call_target="tpu_custom_call" | custom-call | flops 1073741824 | bytes 1048576 | tf_op jit(solution)/shard_map/attend/pallas_call | solution.py:220
  73.5 1.9 %collective-permute-start.5 = (bf16[4,512,128]{2,1,0:T(8,128)(2,1)}, bf16[4,512,128]{2,1,0:T(8,128)(2,1)S(1)}, u32[]{:S(2)}, u32[]{:S(2)}) collective-permute-start(bf16[4,512,128]{2,1,0:T(8,128)(2,1)} %get-tuple-element.15), channel_id=1, source_target_pairs={{0,1},{1,0},{2,3},{3,2},{4,5},{5,4},{6,7},{7,6},{8,9},{9,8},{10,11... | collective-permute-start | bytes 1572872 | tf_op jit(solution)/shard_map/ppermute | solution.py:248
  75.4 3.4 %all-to-all-start.2 = ((bf16[8,8,8,128]{3,2,1,0:T(8,128)(2,1)}), bf16[8,8,8,128]{3,2,1,0:T(8,128)(2,1)S(1)}, u32[]{:S(2)}, u32[]{:S(2)}) async-start(bf16[8,8,8,128]{3,2,1,0:T(8,128)(2,1)} %bitcast.15), calls=%async_computation.2 | async-start | bytes 262144 | tf_op jit(solution)/shard_map/all_to_all | solution.py:268
  79.6 1.2 fusion.5
  80.9 4.6 %collective-permute-start.6 = (bf16[512,128]{1,0:T(8,128)(2,1)S(1)}, bf16[512,128]{1,0:T(8,128)(2,1)S(1)}, u32[]{:S(2)}, u32[]{:S(2)}) collective-permute-start(bf16[512,128]{1,0:T(8,128)(2,1)S(1)} %get-tuple-element.22), channel_id=1, source_target_pairs={{2,0},{4,2},{6,4},{0,6},{3,1},{5,3},{7,5},{1,7},{10,8},{12,10},{14... | collective-permute-start | bytes 393224 | tf_op jit(solution)/shard_map/ppermute | solution.py:244
  85.5 1.9 %collective-permute-start.8 = (bf16[512,128]{1,0:T(8,128)(2,1)S(1)}, bf16[512,128]{1,0:T(8,128)(2,1)S(1)}, u32[]{:S(2)}, u32[]{:S(2)}) collective-permute-start(bf16[512,128]{1,0:T(8,128)(2,1)S(1)} %get-tuple-element.23), channel_id=1, source_target_pairs={{6,0},{0,2},{2,4},{4,6},{7,1},{1,3},{3,5},{5,7},{14,8},{8,10},{10,... | collective-permute-start | bytes 393224 | tf_op jit(solution)/shard_map/ppermute | solution.py:244
  87.4 4.6 %collective-permute-start.7 = (bf16[512,128]{1,0:T(8,128)(2,1)S(1)}, bf16[512,128]{1,0:T(8,128)(2,1)S(1)}, u32[]{:S(2)}, u32[]{:S(2)}) collective-permute-start(bf16[512,128]{1,0:T(8,128)(2,1)S(1)} %get-tuple-element.24), channel_id=1, source_target_pairs={{4,0},{6,2},{0,4},{2,6},{5,1},{7,3},{1,5},{3,7},{12,8},{14,10},{8,... | collective-permute-start | bytes 393224 | tf_op jit(solution)/shard_map/ppermute | solution.py:244
  92.9 3.4 %all-to-all-start.3 = ((bf16[8,8,8,128]{3,2,1,0:T(8,128)(2,1)}), bf16[8,8,8,128]{3,2,1,0:T(8,128)(2,1)S(1)}, u32[]{:S(2)}, u32[]{:S(2)}) async-start(bf16[8,8,8,128]{3,2,1,0:T(8,128)(2,1)} %relay.1), calls=%async_computation.3 | async-start | bytes 262144 | tf_op jit(solution)/shard_map/all_to_all | solution.py:268
  96.5 3.0 %fusion = bf16[4096,128]{0,1:T(8,128)(2,1)S(1)} fusion(bf16[512,128]{1,0:T(8,128)(2,1)S(1)} %fusion.4, bf16[512,4096]{1,0:T(8,128)(2,1)} %param.8), kind=kOutput, calls=%fused_computation.1 | convolution fusion | flops 537395200 | bytes 5373952 | tf_op jit(solution)/shard_map/dot_general | solution.py:362
  99.5 1.3 copy.18
  100.9 4.4 %all-to-all-done.3.given_ref = bf16[8,8,8,128]{3,2,1,0:T(8,128)(2,1)S(1)} async-done(((bf16[8,8,8,128]{3,2,1,0:T(8,128)(2,1)}), bf16[8,8,8,128]{3,2,1,0:T(8,128)(2,1)S(1)}, u32[]{:S(2)}, u32[]{:S(2)}) %all-to-all-start.3) | async-done | bytes 131104 | tf_op jit(solution)/shard_map/all_to_all | solution.py:268
  105.3 8.8 %all-to-all-start.4 = ((bf16[64,64,128]{2,1,0:T(8,128)(2,1)}), bf16[64,64,128]{2,1,0:T(8,128)(2,1)S(1)}, u32[]{:S(2)}, u32[]{:S(2)}) async-start(bf16[64,64,128]{2,1,0:T(8,128)(2,1)} %bitcast.23), calls=%async_computation.4 | async-start | bytes 2097152 | tf_op jit(solution)/shard_map/all_to_all | solution.py:274
  114.2 2.1 %collective-permute-start.11 = (f32[8,8,128]{2,1,0:T(8,128)S(1)}, f32[8,8,128]{2,1,0:T(8,128)S(1)}, u32[]{:S(2)}, u32[]{:S(2)}) collective-permute-start(f32[8,8,128]{2,1,0:T(8,128)S(1)} %settle.1), channel_id=1, source_target_pairs={{0,6},{2,0},{4,2},{6,4},{1,7},{3,1},{5,3},{7,5},{8,14},{10,8},{12,... | collective-permute-start | bytes 98312 | tf_op jit(solution)/shard_map/ppermute | solution.py:240
  116.3 4.0 %collective-permute-start.10 = (f32[8,8,128]{2,1,0:T(8,128)S(1)}, f32[8,8,128]{2,1,0:T(8,128)S(1)}, u32[]{:S(2)}, u32[]{:S(2)}) collective-permute-start(f32[8,8,128]{2,1,0:T(8,128)S(1)} %settle.1), channel_id=1, source_target_pairs={{0,4},{2,6},{4,0},{6,2},{1,5},{3,7},{5,1},{7,3},{8,12},{10,14},{12... | collective-permute-start | bytes 98312 | tf_op jit(solution)/shard_map/ppermute | solution.py:240
  120.3 3.1 %collective-permute-start.9 = (f32[8,8,128]{2,1,0:T(8,128)S(1)}, f32[8,8,128]{2,1,0:T(8,128)S(1)}, u32[]{:S(2)}, u32[]{:S(2)}) collective-permute-start(f32[8,8,128]{2,1,0:T(8,128)S(1)} %settle.1), channel_id=1, source_target_pairs={{0,2},{2,4},{4,6},{6,0},{1,3},{3,5},{5,7},{7,1},{8,10},{10,12},{12... | collective-permute-start | bytes 98312 | tf_op jit(solution)/shard_map/ppermute | solution.py:240
  123.6 2.5 %collective-permute-done.9 = f32[8,8,128]{2,1,0:T(8,128)S(1)} collective-permute-done((f32[8,8,128]{2,1,0:T(8,128)S(1)}, f32[8,8,128]{2,1,0:T(8,128)S(1)}, u32[]{:S(2)}, u32[]{:S(2)}) %collective-permute-start.9) | collective-permute-done | bytes 32800 | tf_op jit(solution)/shard_map/ppermute | solution.py:240
  126.1 1.9 %collective-permute-start.12 = (f32[4,8,8,128]{3,2,1,0:T(8,128)S(1)}, f32[4,8,8,128]{3,2,1,0:T(8,128)S(1)}, u32[]{:S(2)}, u32[]{:S(2)}) collective-permute-start(f32[4,8,8,128]{3,2,1,0:T(8,128)S(1)} %pad_maximum_fusion.1.near_ref), channel_id=1, source_target_pairs={{0,1},{1,0},{2,3},{3,2},{4,5},{5,4},{6,7},{7,6},{8,9},{9,8},{10,11... | collective-permute-start | bytes 393224 | tf_op jit(solution)/shard_map/ppermute | solution.py:248
  128.0 1.3 collective-permute-done.12.far_ref
  130.2 13.0 %all-to-all-done.4 = bf16[64,64,128]{2,1,0:T(8,128)(2,1)S(1)} async-done(((bf16[64,64,128]{2,1,0:T(8,128)(2,1)}), bf16[64,64,128]{2,1,0:T(8,128)(2,1)S(1)}, u32[]{:S(2)}, u32[]{:S(2)}) %all-to-all-start.4) | async-done | bytes 1048608 | tf_op jit(solution)/shard_map/all_to_all | solution.py:274
  (39 shorter events, 7.5 us)
Async XLA Ops:
  0.6 0.9 copy-start
  1.5 0.9 copy-start.1
  2.4 0.9 copy-start.2
  3.3 0.7 copy-start.6
  4.2 13.1 %collective-permute-start.3 = (bf16[1072,128]{1,0:T(8,128)(2,1)S(1)}, bf16[1072,128]{1,0:T(8,128)(2,1)S(1)}, u32[]{:S(2)}, u32[]{:S(2)}) collective-permute-start(bf16[1072,128]{1,0:T(8,128)(2,1)S(1)} %pack.1.q0), channel_id=1, source_target_pairs={{0,6},{2,0},{4,2},{6,4},{1,7},{3,1},{5,3},{7,5},{8,14},{10,8},{12,... | collective-permute-start | bytes 823304 | tf_op jit(solution)/shard_map/ppermute | solution.py:240
  12.0 9.9 %collective-permute-start.2 = (bf16[1072,128]{1,0:T(8,128)(2,1)S(1)}, bf16[1072,128]{1,0:T(8,128)(2,1)S(1)}, u32[]{:S(2)}, u32[]{:S(2)}) collective-permute-start(bf16[1072,128]{1,0:T(8,128)(2,1)S(1)} %pack.1.q0), channel_id=1, source_target_pairs={{0,4},{2,6},{4,0},{6,2},{1,5},{3,7},{5,1},{7,3},{8,12},{10,14},{12... | collective-permute-start | bytes 823304 | tf_op jit(solution)/shard_map/ppermute | solution.py:240
  13.9 10.1 %collective-permute-start.1 = (bf16[1072,128]{1,0:T(8,128)(2,1)S(1)}, bf16[1072,128]{1,0:T(8,128)(2,1)S(1)}, u32[]{:S(2)}, u32[]{:S(2)}) collective-permute-start(bf16[1072,128]{1,0:T(8,128)(2,1)S(1)} %pack.1.q0), channel_id=1, source_target_pairs={{0,2},{2,4},{4,6},{6,0},{1,3},{3,5},{5,7},{7,1},{8,10},{10,12},{12... | collective-permute-start | bytes 823304 | tf_op jit(solution)/shard_map/ppermute | solution.py:240
  24.0 3.1 %copy-start.3 = (bf16[512,64]{0,1:T(8,128)(2,1)S(1)}, bf16[512,64]{0,1:T(8,128)(2,1)}, u32[]{:S(2)}) copy-start(bf16[512,64]{0,1:T(8,128)(2,1)} %param.10) | copy-start | bytes 196612
  24.0 3.1 %copy-start.4 = (bf16[512,64]{0,1:T(8,128)(2,1)S(1)}, bf16[512,64]{0,1:T(8,128)(2,1)}, u32[]{:S(2)}) copy-start(bf16[512,64]{0,1:T(8,128)(2,1)} %param.11) | copy-start | bytes 196612
  24.0 3.1 %copy-start.5 = (s32[8,16]{1,0:T(8,128)S(1)}, s32[8,16]{1,0:T(8,128)}, u32[]{:S(2)}) copy-start(s32[8,16]{1,0:T(8,128)} %chosen_ref.1) | copy-start | bytes 1540
  25.1 41.6 %collective-permute-start.4 = (bf16[4,1072,128]{2,1,0:T(8,128)(2,1)}, bf16[4,1072,128]{2,1,0:T(8,128)(2,1)S(1)}, u32[]{:S(2)}, u32[]{:S(2)}) collective-permute-start(bf16[4,1072,128]{2,1,0:T(8,128)(2,1)} %pad_maximum_fusion), channel_id=1, source_target_pairs={{0,1},{1,0},{2,3},{3,2},{4,5},{5,4},{6,7},{7,6},{8,9},{9,8},{10,11... | collective-permute-start | bytes 3293192 | tf_op jit(solution)/shard_map/ppermute | solution.py:248
  46.7 3.1 %collective-permute-start = (bf16[8,8,128]{2,1,0:T(8,128)(2,1)S(1)}, bf16[8,8,128]{2,1,0:T(8,128)(2,1)S(1)}, u32[]{:S(2)}, u32[]{:S(2)}) collective-permute-start(bf16[8,8,128]{2,1,0:T(8,128)(2,1)S(1)} %slice_bitcast_fusion.4), channel_id=1, source_target_pairs={{0,1},{1,0},{2,3},{3,2},{4,5},{5,4},{6,7},{7,6},{8,9},{9,8},{10,11... | collective-permute-start | bytes 49160 | tf_op jit(solution)/shard_map/ppermute | solution.py:248
  50.6 16.2 %all-to-all-start.1 = ((bf16[8,8,8,128]{3,2,1,0:T(8,128)(2,1)}), bf16[8,8,8,128]{3,2,1,0:T(8,128)(2,1)S(1)}, u32[]{:S(2)}, u32[]{:S(2)}) async-start(bf16[8,8,8,128]{3,2,1,0:T(8,128)(2,1)} %pick.1), calls=%async_computation.1 | async-start | bytes 262144 | tf_op jit(solution)/shard_map/all_to_all | solution.py:268
  73.5 5.3 %collective-permute-start.5 = (bf16[4,512,128]{2,1,0:T(8,128)(2,1)}, bf16[4,512,128]{2,1,0:T(8,128)(2,1)S(1)}, u32[]{:S(2)}, u32[]{:S(2)}) collective-permute-start(bf16[4,512,128]{2,1,0:T(8,128)(2,1)} %get-tuple-element.15), channel_id=1, source_target_pairs={{0,1},{1,0},{2,3},{3,2},{4,5},{5,4},{6,7},{7,6},{8,9},{9,8},{10,11... | collective-permute-start | bytes 1572872 | tf_op jit(solution)/shard_map/ppermute | solution.py:248
  75.4 16.6 %all-to-all-start.2 = ((bf16[8,8,8,128]{3,2,1,0:T(8,128)(2,1)}), bf16[8,8,8,128]{3,2,1,0:T(8,128)(2,1)S(1)}, u32[]{:S(2)}, u32[]{:S(2)}) async-start(bf16[8,8,8,128]{3,2,1,0:T(8,128)(2,1)} %bitcast.15), calls=%async_computation.2 | async-start | bytes 262144 | tf_op jit(solution)/shard_map/all_to_all | solution.py:268
  78.8 0.8 copy-start.7
  80.9 15.4 %collective-permute-start.6 = (bf16[512,128]{1,0:T(8,128)(2,1)S(1)}, bf16[512,128]{1,0:T(8,128)(2,1)S(1)}, u32[]{:S(2)}, u32[]{:S(2)}) collective-permute-start(bf16[512,128]{1,0:T(8,128)(2,1)S(1)} %get-tuple-element.22), channel_id=1, source_target_pairs={{2,0},{4,2},{6,4},{0,6},{3,1},{5,3},{7,5},{1,7},{10,8},{12,10},{14... | collective-permute-start | bytes 393224 | tf_op jit(solution)/shard_map/ppermute | solution.py:244
  85.5 10.8 %collective-permute-start.8 = (bf16[512,128]{1,0:T(8,128)(2,1)S(1)}, bf16[512,128]{1,0:T(8,128)(2,1)S(1)}, u32[]{:S(2)}, u32[]{:S(2)}) collective-permute-start(bf16[512,128]{1,0:T(8,128)(2,1)S(1)} %get-tuple-element.23), channel_id=1, source_target_pairs={{6,0},{0,2},{2,4},{4,6},{7,1},{1,3},{3,5},{5,7},{14,8},{8,10},{10,... | collective-permute-start | bytes 393224 | tf_op jit(solution)/shard_map/ppermute | solution.py:244
  87.4 9.0 %collective-permute-start.7 = (bf16[512,128]{1,0:T(8,128)(2,1)S(1)}, bf16[512,128]{1,0:T(8,128)(2,1)S(1)}, u32[]{:S(2)}, u32[]{:S(2)}) collective-permute-start(bf16[512,128]{1,0:T(8,128)(2,1)S(1)} %get-tuple-element.24), channel_id=1, source_target_pairs={{4,0},{6,2},{0,4},{2,6},{5,1},{7,3},{1,5},{3,7},{12,8},{14,10},{8,... | collective-permute-start | bytes 393224 | tf_op jit(solution)/shard_map/ppermute | solution.py:244
  92.9 12.4 %all-to-all-start.3 = ((bf16[8,8,8,128]{3,2,1,0:T(8,128)(2,1)}), bf16[8,8,8,128]{3,2,1,0:T(8,128)(2,1)S(1)}, u32[]{:S(2)}, u32[]{:S(2)}) async-start(bf16[8,8,8,128]{3,2,1,0:T(8,128)(2,1)} %relay.1), calls=%async_computation.3 | async-start | bytes 262144 | tf_op jit(solution)/shard_map/all_to_all | solution.py:268
  96.5 3.0 %copy-start.8 = (bf16[512,128]{1,0:T(8,128)(2,1)}, bf16[512,128]{1,0:T(8,128)(2,1)S(1)}, u32[]{:S(2)}) copy-start(bf16[512,128]{1,0:T(8,128)(2,1)S(1)} %fusion.4) | copy-start | bytes 393220
  105.3 37.9 %all-to-all-start.4 = ((bf16[64,64,128]{2,1,0:T(8,128)(2,1)}), bf16[64,64,128]{2,1,0:T(8,128)(2,1)S(1)}, u32[]{:S(2)}, u32[]{:S(2)}) async-start(bf16[64,64,128]{2,1,0:T(8,128)(2,1)} %bitcast.23), calls=%async_computation.4 | async-start | bytes 2097152 | tf_op jit(solution)/shard_map/all_to_all | solution.py:274
  114.2 9.3 %collective-permute-start.11 = (f32[8,8,128]{2,1,0:T(8,128)S(1)}, f32[8,8,128]{2,1,0:T(8,128)S(1)}, u32[]{:S(2)}, u32[]{:S(2)}) collective-permute-start(f32[8,8,128]{2,1,0:T(8,128)S(1)} %settle.1), channel_id=1, source_target_pairs={{0,6},{2,0},{4,2},{6,4},{1,7},{3,1},{5,3},{7,5},{8,14},{10,8},{12,... | collective-permute-start | bytes 98312 | tf_op jit(solution)/shard_map/ppermute | solution.py:240
  116.3 7.3 %collective-permute-start.10 = (f32[8,8,128]{2,1,0:T(8,128)S(1)}, f32[8,8,128]{2,1,0:T(8,128)S(1)}, u32[]{:S(2)}, u32[]{:S(2)}) collective-permute-start(f32[8,8,128]{2,1,0:T(8,128)S(1)} %settle.1), channel_id=1, source_target_pairs={{0,4},{2,6},{4,0},{6,2},{1,5},{3,7},{5,1},{7,3},{8,12},{10,14},{12... | collective-permute-start | bytes 98312 | tf_op jit(solution)/shard_map/ppermute | solution.py:240
  120.3 5.8 %collective-permute-start.9 = (f32[8,8,128]{2,1,0:T(8,128)S(1)}, f32[8,8,128]{2,1,0:T(8,128)S(1)}, u32[]{:S(2)}, u32[]{:S(2)}) collective-permute-start(f32[8,8,128]{2,1,0:T(8,128)S(1)} %settle.1), channel_id=1, source_target_pairs={{0,2},{2,4},{4,6},{6,0},{1,3},{3,5},{5,7},{7,1},{8,10},{10,12},{12... | collective-permute-start | bytes 98312 | tf_op jit(solution)/shard_map/ppermute | solution.py:240
  126.1 3.2 %collective-permute-start.12 = (f32[4,8,8,128]{3,2,1,0:T(8,128)S(1)}, f32[4,8,8,128]{3,2,1,0:T(8,128)S(1)}, u32[]{:S(2)}, u32[]{:S(2)}) collective-permute-start(f32[4,8,8,128]{3,2,1,0:T(8,128)S(1)} %pad_maximum_fusion.1.near_ref), channel_id=1, source_target_pairs={{0,1},{1,0},{2,3},{3,2},{4,5},{5,4},{6,7},{7,6},{8,9},{9,8},{10,11... | collective-permute-start | bytes 393224 | tf_op jit(solution)/shard_map/ppermute | solution.py:248

commit v5 on v4

--- a/solution.py
+++ b/solution.py
@@ -29,21 +29,25 @@
     return lax.broadcasted_iota(jnp.int32, shape, len(shape) - 1) < LANES // 2
 
 
-def offer_kernel(rank_ref, tp_ref, keys_ref, vals_ref, chosen_ref, out_ref, piece_ref, pairs):
+def offer_kernel(rank_ref, tp_ref, keys_ref, vals_ref, chosen_ref, out_ref, piece_ref, want_ref, pairs):
     rank = rank_ref[0]
     tp = tp_ref[0]
     flip = tp & 1
     both = jnp.concatenate([keys_ref[...], vals_ref[...]], axis=0).astype(F32)
     pairs[...] = both.T
     at = lax.broadcasted_iota(jnp.int32, (PEERS, SLOTS), 0)
-    peer = jnp.where(jnp.full(at.shape, flip, jnp.int32) == 0, at, (at & 7) * 8 + (at >> 3))
-    best = jnp.zeros((PEERS, SLOTS), jnp.int32)
-    for j in range(BLOCKS):
-        c = chosen_ref[j : j + 1, :]
-        hit = ((c >> 3) == peer) & (c >= 0) & (peer != rank)
-        best = jnp.maximum(best, jnp.where(hit, (c & 7) + 1, 0))
-    best = jnp.max(best, axis=1, keepdims=True)
-    best = jnp.broadcast_to(best, (PEERS, LANES)).astype(F32)
+
+    def wanted(peer):
+        best = jnp.zeros((PEERS, SLOTS), jnp.int32)
+        for j in range(BLOCKS):
+            c = chosen_ref[j : j + 1, :]
+            hit = ((c >> 3) == peer) & (c >= 0) & (peer != rank)
+            best = jnp.maximum(best, jnp.where(hit, (c & 7) + 1, 0))
+        best = jnp.max(best, axis=1, keepdims=True)
+        return jnp.broadcast_to(best, (PEERS, LANES)).astype(F32)
+
+    best = wanted(jnp.where(jnp.full(at.shape, flip, jnp.int32) == 0, at, (at & 7) * 8 + (at >> 3)))
+    want_ref[...] = wanted(at)
     for b in range(BLOCKS):
         at = pl.multiple_of(b * BLOCK + tp * ROWS, ROWS)
         piece = pairs[pl.ds(at, ROWS), :].astype(BF16)
@@ -65,24 +69,15 @@
             out_ref[i, r] = got.astype(BF16)
 
 
-def relay_kernel(wants_ref, given_ref, out_ref):
-    for r in range(SIDE):
-        totals = [jnp.zeros((ROWS, LANES), F32) for _ in range(BLOCKS)]
-        for i in range(SIDE):
-            want = jnp.broadcast_to(wants_ref[i].astype(F32)[r : r + 1], (ROWS, LANES))
-            got = given_ref[i, r].astype(F32)
-            for b in range(BLOCKS):
-                totals[b] = totals[b] + jnp.where(want == b + 1.0, got, 0.0)
+def settle_kernel(own_ref, given_ref, out_ref):
+    totals = [own_ref[b] for b in range(BLOCKS)]
+    for s in range(PEERS):
+        got = given_ref[s, :ROWS].astype(F32)
+        want = given_ref[s, ROWS:].astype(F32)
         for b in range(BLOCKS):
-            out_ref[r, b] = totals[b].astype(BF16)
-
-
-def settle_kernel(own_ref, given_ref, out_ref):
+            totals[b] = totals[b] + jnp.where(want == b + 1.0, got, 0.0)
     for b in range(BLOCKS):
-        total = own_ref[b]
-        for i in range(SIDE):
-            total = total + given_ref[i, b].astype(F32)
-        out_ref[b] = total
+        out_ref[b] = totals[b]
 
 
 def pack_kernel(q_ref, g_ref, o_ref, log_ref, out_ref):
@@ -107,9 +102,11 @@
 
 def attend_kernel(
     slot_ref,
+    home_ref,
     rel_ref,
     fetched_ref,
     piece_ref,
+    want_ref,
     q0,
     q1,
     q2,
@@ -193,11 +190,14 @@
             jnp.where(low, dv[:LANES], dk[LANES:]), LANES // 2, 1
         )
         for s in range(SLOTS):
-            acc[slot_ref[j, s]] += both[s * ROWS : (s + 1) * ROWS]
+            acc[home_ref[j, s]] += both[s * ROWS : (s + 1) * ROWS]
         return carry
 
     lax.fori_loop(0, BLOCKS, one_block, 0)
-    away_ref[...] = acc[:PEERS].astype(BF16)
+    away_ref[:, :ROWS] = acc[:PEERS].astype(BF16)
+    for s in range(PEERS):
+        want = jnp.broadcast_to(want_ref[s : s + 1, :], (ROWS, LANES))
+        away_ref[s, ROWS:] = want.astype(BF16)
     own_ref[...] = acc[PEERS:]
 
 
@@ -215,7 +215,7 @@
     vals_ref[...] = turned[LANES // 2 :]
 
 
-def call(kernel, ins, out_shape, args, flops, **kw):
+def call(kernel, ins, out_shape, args, flops, limit=8 << 20, **kw):
     many = isinstance(out_shape, (list, tuple))
     return pl.pallas_call(
         kernel,
@@ -223,7 +223,7 @@
         out_specs=[VMEM] * len(out_shape) if many else VMEM,
         out_shape=out_shape,
         cost_estimate=pl.CostEstimate(flops=flops, bytes_accessed=1 << 20, transcendentals=0),
-        compiler_params=pltpu.CompilerParams(vmem_limit_bytes=24 << 20),
+        compiler_params=pltpu.CompilerParams(vmem_limit_bytes=limit),
         **kw,
     )(*args)
 
@@ -283,15 +283,17 @@
     x = lax.axis_index("x").astype(jnp.int32)
     c = lax.axis_index("c").astype(jnp.int32)
     tp = x * 2 + c
-    offer, piece = call(
+    offer, piece, want = call(
         offer_kernel,
         [SMEM] * 2 + [VMEM] * 3,
         [
-            held((SIDE, BLOCKS + 1, ROWS, LANES), BF16),
-            held((BLOCKS, ROWS, LANES), BF16),
+            sds((SIDE, BLOCKS + 1, ROWS, LANES), BF16),
+            sds((BLOCKS, ROWS, LANES), BF16),
+            sds((PEERS, LANES), F32),
         ],
         (rank.reshape(1), tp.reshape(1), keys.T, values.T, chosen),
         1 << 18,
+        limit=58 << 20,
         scratch_shapes=[pltpu.VMEM((TOK, LANES), F32)],
         name="offer",
     )
@@ -310,9 +312,10 @@
     qd = call(
         pack_kernel,
         [VMEM] * 4,
-        held((2 * TOK + 48, LANES), BF16),
+        sds((2 * TOK + 48, LANES), BF16),
         (queries, cotangent, attended, log_sum.T),
         1 << 18,
+        limit=58 << 20,
         name="pack",
     )
     qds = [qd] + [x_from(qd, k) for k in (1, 2, 3)]
@@ -324,19 +327,21 @@
     peer = jnp.where(c == 0, (owner & 7) * 8 + (owner >> 3), owner)
     slot = jnp.where(listed, jnp.where(owner == rank, PEERS + inner, peer), 0)
     starts = rank * TOK + lax.broadcasted_iota(jnp.int32, chosen.shape, 0) * BLOCK
+    home = jnp.where(listed, jnp.where(owner == rank, PEERS + inner, owner), 0)
     rel = jnp.where(listed, chosen * BLOCK + ROWS * tp - starts, FAR)
 
     away, own, gq_own, gq_far = call(
         attend_kernel,
-        [SMEM] * 2 + [VMEM] * 7,
+        [SMEM] * 3 + [VMEM] * 8,
         [
-            held((PEERS, ROWS, LANES), BF16),
+            held((PEERS, 2 * ROWS, LANES), BF16),
             held((BLOCKS, ROWS, LANES), F32),
             held((4, TOK, LANES), F32),
             held((4, TOK, LANES), BF16),
         ],
-        (slot, rel, near_core(fetched), near_core(piece), *map(near_core, qds), near_core(qd_far)),
+        (slot, home, rel, near_core(fetched), near_core(piece), near_core(want), *map(near_core, qds), near_core(qd_far)),
         1 << 30,
+        limit=16 << 20,
         scratch_shapes=[
             pltpu.VMEM((BLOCKS, 8, TOK), F32),
             pltpu.VMEM((PEERS + BLOCKS, ROWS, LANES), F32),
@@ -345,16 +350,7 @@
         name="attend",
     )
     gq4 = gq_own + swap(gq_far).astype(F32)
-    given = along(away.reshape(SIDE, SIDE, ROWS, LANES), False)
-    relayed = call(
-        relay_kernel,
-        [VMEM] * 2,
-        held((SIDE, BLOCKS, ROWS, LANES), BF16),
-        (near_core(wants), near_core(given)),
-        1 << 20,
-        name="relay",
-    )
-    returned = along(relayed, True)
+    returned = exchange(away)
     gq = gq4[0]
     for k in (1, 2, 3):
         gq = gq + x_back(gq4[k].astype(BF16), k).astype(F32)

time: 145 us -> 145 us (level)
  waiting for transfers between devices: 38.4 us -> 45.1 us
  starting transfers between devices: 63.8 us -> 57.9 us
  Pallas kernels: 9.7 us -> 12.4 us
  local copies, waits for them, and re-layouts: 5.54 us -> 2.84 us
    all_to_all x1 -> x2, waiting for transfers between devices: 13 us -> 22.6 us  [exchange(): return lax.all_to_all(arr, KV, split_axis=0, concat_axis=0, tiled=True)]
    all_to_all x3 -> x1, starting transfers between devices: 13.9 us -> 7.1 us  [along(): lax.all_to_all(arr, ALL, split_axis=0, concat_axis=0, tiled=True, axis_in...]
    all_to_all x3 -> x1, waiting for transfers between devices: 13.4 us -> 8.98 us  [along(): lax.all_to_all(arr, ALL, split_axis=0, concat_axis=0, tiled=True, axis_in...]
    unnamed x18 -> x10, local copies, waits for them, and re-layouts: 4.19 us -> 1.49 us
    pallas_call x7 -> x6, Pallas kernels: 9.7 us -> 12.4 us  [call(): pl.pallas_call(kernel, in_specs=ins, out_specs=[VMEM] * len(out_shape) if...]
    ppermute x4, waiting for transfers between devices: 2.47 us -> 4.34 us  [swap(): return lax.ppermute(arr, 'c', [(0, 1), (1, 0)])]
    all_to_all x1 -> x2, starting transfers between devices: 8.85 us -> 9.27 us  [exchange(): return lax.all_to_all(arr, KV, split_axis=0, concat_axis=0, tiled=True)]
  transfers between devices with their start and end apart: 17 -> 16, of which waited for: 10 -> 9; matrix products, arithmetic and copies ran while one was open for 4% -> 3% of each run, Pallas kernels for 2% -> 3%
where the time goes in v5:
time: 145 us; the launch traced here: 144 us
  starting transfers between devices  57.9 us (40%)
  waiting for transfers between devices  45.1 us (31%)
  blocking collectives  19.6 us (14%)
  Pallas kernels  12.4 us (9%)
  matrix products  2.99 us (2%)
  local copies, waits for them, and re-layouts  2.84 us (2%)
  other arithmetic  2.18 us (2%)
    ppermute x6, starting transfers between devices, x_from(): return lax.ppermute(arr, 'x', [(i, (i + k) % 4) for i in range(4)])  22.6 us
    all_to_all x2, waiting for transfers between devices, exchange(): return lax.all_to_all(arr, KV, split_axis=0, concat_axis=0, tiled=True)  22.6 us
    all_to_all x1, blocking collectives, along(): lax.all_to_all(arr, ALL, split_axis=0, concat_axis=0, tiled=True, axis_in...  19.6 us
    pallas_call x6, Pallas kernels, call(): pl.pallas_call(kernel, in_specs=ins, out_specs=[VMEM] * len(out_shape) if...  12.4 us
    ppermute x3, starting transfers between devices, x_back(): return lax.ppermute(arr, 'x', [((i + k) % 4, i) for i in range(4)])  11.1 us
    all_to_all x2, starting transfers between devices, exchange(): return lax.all_to_all(arr, KV, split_axis=0, concat_axis=0, tiled=True)  9.27 us
    ppermute x6, waiting for transfers between devices, x_from(): return lax.ppermute(arr, 'x', [(i, (i + k) % 4) for i in range(4)])  9.24 us
    all_to_all x1, waiting for transfers between devices, along(): lax.all_to_all(arr, ALL, split_axis=0, concat_axis=0, tiled=True, axis_in...  8.98 us
  transfers between devices with their start and end apart: 16, of which 9 were waited for; matrix products, arithmetic and copies ran while one was open for 3% of the time, Pallas kernels for 3%

profile of v5, /device:TPU:2, one launch (start us, length us, event | category | flops | bytes accessed | tf_op | source)
XLA Modules:
  0.0 143.9 jit_solution(9495798476118099447)
XLA Ops:
  0.6 1.9 %pack.1.q0 = bf16[1072,128]{1,0:T(8,128)(2,1)} custom-call(bf16[512,128]{1,0:T(8,128)(2,1)} %q_ref.1, bf16[512,128]{1,0:T(8,128)(2,1)} %g_ref.1, bf16[512,128]{1,0:T(8,128)(2,1)} %o_ref.1, f32[2,512]{1,0:T(2,128)} %bitcast.50), custom_call_target="tpu_custom_call" | custom-call | flops 262144 | bytes 1048576 | tf_op jit(solution)/shard_map/pack/pallas_call | solution.py:220
  2.5 7.8 %collective-permute-start.3 = (bf16[1072,128]{1,0:T(8,128)(2,1)}, bf16[1072,128]{1,0:T(8,128)(2,1)S(1)}, u32[]{:S(2)}, u32[]{:S(2)}) collective-permute-start(bf16[1072,128]{1,0:T(8,128)(2,1)} %pack.1.q0), channel_id=1, source_target_pairs={{0,6},{2,0},{4,2},{6,4},{1,7},{3,1},{5,3},{7,5},{8,14},{10,8},{12,... | collective-permute-start | bytes 823304 | tf_op jit(solution)/shard_map/ppermute | solution.py:240
  10.3 1.9 %collective-permute-start.2 = (bf16[1072,128]{1,0:T(8,128)(2,1)}, bf16[1072,128]{1,0:T(8,128)(2,1)S(1)}, u32[]{:S(2)}, u32[]{:S(2)}) collective-permute-start(bf16[1072,128]{1,0:T(8,128)(2,1)} %pack.1.q0), channel_id=1, source_target_pairs={{0,4},{2,6},{4,0},{6,2},{1,5},{3,7},{5,1},{7,3},{8,12},{10,14},{12... | collective-permute-start | bytes 823304 | tf_op jit(solution)/shard_map/ppermute | solution.py:240
  12.2 3.4 %collective-permute-start.1 = (bf16[1072,128]{1,0:T(8,128)(2,1)}, bf16[1072,128]{1,0:T(8,128)(2,1)S(1)}, u32[]{:S(2)}, u32[]{:S(2)}) collective-permute-start(bf16[1072,128]{1,0:T(8,128)(2,1)} %pack.1.q0), channel_id=1, source_target_pairs={{0,2},{2,4},{4,6},{6,0},{1,3},{3,5},{5,7},{7,1},{8,10},{10,12},{12... | collective-permute-start | bytes 823304 | tf_op jit(solution)/shard_map/ppermute | solution.py:240
  15.6 4.8 %collective-permute-done.2.q2 = bf16[1072,128]{1,0:T(8,128)(2,1)S(1)} collective-permute-done((bf16[1072,128]{1,0:T(8,128)(2,1)}, bf16[1072,128]{1,0:T(8,128)(2,1)S(1)}, u32[]{:S(2)}, u32[]{:S(2)}) %collective-permute-start.2) | collective-permute-done | bytes 274464 | tf_op jit(solution)/shard_map/ppermute | solution.py:240
  20.4 2.1 %collective-permute-done.1.q1 = bf16[1072,128]{1,0:T(8,128)(2,1)S(1)} collective-permute-done((bf16[1072,128]{1,0:T(8,128)(2,1)}, bf16[1072,128]{1,0:T(8,128)(2,1)S(1)}, u32[]{:S(2)}, u32[]{:S(2)}) %collective-permute-start.1) | collective-permute-done | bytes 274464 | tf_op jit(solution)/shard_map/ppermute | solution.py:240
  22.5 1.1 pad_maximum_fusion
  23.6 2.1 %collective-permute-start.4 = (bf16[4,1072,128]{2,1,0:T(8,128)(2,1)S(1)}, bf16[4,1072,128]{2,1,0:T(8,128)(2,1)S(1)}, u32[]{:S(2)}, u32[]{:S(2)}) collective-permute-start(bf16[4,1072,128]{2,1,0:T(8,128)(2,1)S(1)} %pad_maximum_fusion), channel_id=1, source_target_pairs={{0,1},{1,0},{2,3},{3,2},{4,5},{5,4},{6,7},{7,6},{8,9},{9,8},{10,11... | collective-permute-start | bytes 3293192 | tf_op jit(solution)/shard_map/ppermute | solution.py:248
  25.7 1.8 %offer.1 = (bf16[8,9,8,128]{3,2,1,0:T(8,128)(2,1)}, bf16[8,8,128]{2,1,0:T(8,128)(2,1)}, f32[64,128]{1,0:T(8,128)}) custom-call(s32[1]{0:T(128)} %bitcast.rank_ref, s32[1]{0:T(128)} %bitcast.1.tp_ref, bf16[64,512]{1,0:T(8,128)(2,1)} %bitcast.45, bf16[64,512]{1,0:T(8,128)(2,1)} %bitcast.46, s32[8,16]{1,0:T(8,128)} %chosen_ref.1), custom_call_target="tpu_custom_call" | custom-call | flops 262144 | bytes 1048576 | tf_op jit(solution)/shard_map/offer/pallas_call | solution.py:220
  27.5 19.6 %all_to_all.20.pushed_ref = bf16[8,9,8,128]{3,2,1,0:T(8,128)(2,1)S(1)} all-to-all(bf16[8,9,8,128]{3,2,1,0:T(8,128)(2,1)} %get-tuple-element.13), channel_id=1, replica_groups={{0,64,128,192,256,320,384,448},{8,72,136,200,264,328,392,456},{16,80,14..., dimensions={0} | all-to-all | bytes 294912 | tf_op jit(solution)/shard_map/all_to_all | solution.py:268
  47.1 1.9 %collective-permute-start = (bf16[8,8,128]{2,1,0:T(8,128)(2,1)S(1)}, bf16[8,8,128]{2,1,0:T(8,128)(2,1)S(1)}, u32[]{:S(2)}, u32[]{:S(2)}) collective-permute-start(bf16[8,8,128]{2,1,0:T(8,128)(2,1)S(1)} %slice_bitcast_fusion.4), channel_id=1, source_target_pairs={{0,1},{1,0},{2,3},{3,2},{4,5},{5,4},{6,7},{7,6},{8,9},{9,8},{10,11... | collective-permute-start | bytes 49160 | tf_op jit(solution)/shard_map/ppermute | solution.py:248
  49.0 1.1 collective-permute-done.wants_ref
  51.0 7.1 %all-to-all-start.1 = ((bf16[8,8,8,128]{3,2,1,0:T(8,128)(2,1)}), bf16[8,8,8,128]{3,2,1,0:T(8,128)(2,1)S(1)}, u32[]{:S(2)}, u32[]{:S(2)}) async-start(bf16[8,8,8,128]{3,2,1,0:T(8,128)(2,1)} %pick.1), calls=%async_computation.1 | async-start | bytes 262144 | tf_op jit(solution)/shard_map/all_to_all | solution.py:268
  58.2 9.0 %all-to-all-done.1 = bf16[8,8,8,128]{3,2,1,0:T(8,128)(2,1)S(1)} async-done(((bf16[8,8,8,128]{3,2,1,0:T(8,128)(2,1)}), bf16[8,8,8,128]{3,2,1,0:T(8,128)(2,1)S(1)}, u32[]{:S(2)}, u32[]{:S(2)}) %all-to-all-start.1) | async-done | bytes 131104 | tf_op jit(solution)/shard_map/all_to_all | solution.py:268
  68.6 6.8 %attend.1 = (bf16[64,16,128]{2,1,0:T(8,128)(2,1)}, f32[8,8,128]{2,1,0:T(8,128)S(1)}, f32[4,512,128]{2,1,0:T(8,128)S(1)}, bf16[4,512,128]{2,1,0:T(8,128)(2,1)S(1)}) custom-call(s32[8,16]{1,0:T(8,128)S(1)} %get-tuple-element.28.slot_ref, s32[8,16]{1,0:T(8,128)S(1)} %get-tuple-element.29.home_ref, s32[8,16]{1,0:T(8,128)S(1)} %get-tuple-element.27.rel_ref, ...), custom_call_target="tpu_custom_call" | custom-call | flops 1073741824 | bytes 1048576 | tf_op jit(solution)/shard_map/attend/pallas_call | solution.py:220
  75.4 1.9 %collective-permute-start.5 = (bf16[4,512,128]{2,1,0:T(8,128)(2,1)S(1)}, bf16[4,512,128]{2,1,0:T(8,128)(2,1)S(1)}, u32[]{:S(2)}, u32[]{:S(2)}) collective-permute-start(bf16[4,512,128]{2,1,0:T(8,128)(2,1)S(1)} %get-tuple-element.17), channel_id=1, source_target_pairs={{0,1},{1,0},{2,3},{3,2},{4,5},{5,4},{6,7},{7,6},{8,9},{9,8},{10,11... | collective-permute-start | bytes 1572872 | tf_op jit(solution)/shard_map/ppermute | solution.py:248
  77.3 1.9 %collective-permute-done.5 = bf16[4,512,128]{2,1,0:T(8,128)(2,1)S(1)} collective-permute-done((bf16[4,512,128]{2,1,0:T(8,128)(2,1)S(1)}, bf16[4,512,128]{2,1,0:T(8,128)(2,1)S(1)}, u32[]{:S(2)}, u32[]{:S(2)}) %collective-permute-start.5) | collective-permute-done | bytes 524320 | tf_op jit(solution)/shard_map/ppermute | solution.py:248
  79.4 4.6 %collective-permute-start.6 = (bf16[512,128]{1,0:T(8,128)(2,1)S(1)}, bf16[512,128]{1,0:T(8,128)(2,1)S(1)}, u32[]{:S(2)}, u32[]{:S(2)}) collective-permute-start(bf16[512,128]{1,0:T(8,128)(2,1)S(1)} %get-tuple-element.24), channel_id=1, source_target_pairs={{2,0},{4,2},{6,4},{0,6},{3,1},{5,3},{7,5},{1,7},{10,8},{12,10},{14... | collective-permute-start | bytes 393224 | tf_op jit(solution)/shard_map/ppermute | solution.py:244
  84.0 1.9 %collective-permute-start.8 = (bf16[512,128]{1,0:T(8,128)(2,1)S(1)}, bf16[512,128]{1,0:T(8,128)(2,1)S(1)}, u32[]{:S(2)}, u32[]{:S(2)}) collective-permute-start(bf16[512,128]{1,0:T(8,128)(2,1)S(1)} %get-tuple-element.25), channel_id=1, source_target_pairs={{6,0},{0,2},{2,4},{4,6},{7,1},{1,3},{3,5},{5,7},{14,8},{8,10},{10,... | collective-permute-start | bytes 393224 | tf_op jit(solution)/shard_map/ppermute | solution.py:244
  86.0 4.6 %collective-permute-start.7 = (bf16[512,128]{1,0:T(8,128)(2,1)S(1)}, bf16[512,128]{1,0:T(8,128)(2,1)S(1)}, u32[]{:S(2)}, u32[]{:S(2)}) collective-permute-start(bf16[512,128]{1,0:T(8,128)(2,1)S(1)} %get-tuple-element.26), channel_id=1, source_target_pairs={{4,0},{6,2},{0,4},{2,6},{5,1},{7,3},{1,5},{3,7},{12,8},{14,10},{8,... | collective-permute-start | bytes 393224 | tf_op jit(solution)/shard_map/ppermute | solution.py:244
  90.5 4.6 %all-to-all-start.2 = ((bf16[64,16,128]{2,1,0:T(8,128)(2,1)}), bf16[64,16,128]{2,1,0:T(8,128)(2,1)S(1)}, u32[]{:S(2)}, u32[]{:S(2)}) async-start(bf16[64,16,128]{2,1,0:T(8,128)(2,1)} %get-tuple-element.19), calls=%async_computation.2 | async-start | bytes 524288 | tf_op jit(solution)/shard_map/all_to_all | solution.py:274
  95.3 3.0 %fusion = bf16[4096,128]{0,1:T(8,128)(2,1)S(1)} fusion(bf16[512,128]{1,0:T(8,128)(2,1)S(1)} %fusion.4, bf16[512,4096]{1,0:T(8,128)(2,1)} %param.8), kind=kOutput, calls=%fused_computation.1 | convolution fusion | flops 537395200 | bytes 5373952 | tf_op jit(solution)/shard_map/dot_general | solution.py:358
  98.3 1.3 copy.12
  99.6 10.2 %all-to-all-done.2.given_ref = bf16[64,16,128]{2,1,0:T(8,128)(2,1)S(1)} async-done(((bf16[64,16,128]{2,1,0:T(8,128)(2,1)}), bf16[64,16,128]{2,1,0:T(8,128)(2,1)S(1)}, u32[]{:S(2)}, u32[]{:S(2)}) %all-to-all-start.2) | async-done | bytes 262176 | tf_op jit(solution)/shard_map/all_to_all | solution.py:274
  109.8 4.7 %all-to-all-start.3 = ((bf16[64,64,128]{2,1,0:T(8,128)(2,1)}), bf16[64,64,128]{2,1,0:T(8,128)(2,1)S(1)}, u32[]{:S(2)}, u32[]{:S(2)}) async-start(bf16[64,64,128]{2,1,0:T(8,128)(2,1)} %bitcast.22), calls=%async_computation.3 | async-start | bytes 2097152 | tf_op jit(solution)/shard_map/all_to_all | solution.py:274
  114.7 2.1 %collective-permute-start.11 = (f32[8,8,128]{2,1,0:T(8,128)S(1)}, f32[8,8,128]{2,1,0:T(8,128)S(1)}, u32[]{:S(2)}, u32[]{:S(2)}) collective-permute-start(f32[8,8,128]{2,1,0:T(8,128)S(1)} %settle.1), channel_id=1, source_target_pairs={{0,6},{2,0},{4,2},{6,4},{1,7},{3,1},{5,3},{7,5},{8,14},{10,8},{12,... | collective-permute-start | bytes 98312 | tf_op jit(solution)/shard_map/ppermute | solution.py:240
  116.8 4.0 %collective-permute-start.10 = (f32[8,8,128]{2,1,0:T(8,128)S(1)}, f32[8,8,128]{2,1,0:T(8,128)S(1)}, u32[]{:S(2)}, u32[]{:S(2)}) collective-permute-start(f32[8,8,128]{2,1,0:T(8,128)S(1)} %settle.1), channel_id=1, source_target_pairs={{0,4},{2,6},{4,0},{6,2},{1,5},{3,7},{5,1},{7,3},{8,12},{10,14},{12... | collective-permute-start | bytes 98312 | tf_op jit(solution)/shard_map/ppermute | solution.py:240
  120.8 3.4 %collective-permute-start.9 = (f32[8,8,128]{2,1,0:T(8,128)S(1)}, f32[8,8,128]{2,1,0:T(8,128)S(1)}, u32[]{:S(2)}, u32[]{:S(2)}) collective-permute-start(f32[8,8,128]{2,1,0:T(8,128)S(1)} %settle.1), channel_id=1, source_target_pairs={{0,2},{2,4},{4,6},{6,0},{1,3},{3,5},{5,7},{7,1},{8,10},{10,12},{12... | collective-permute-start | bytes 98312 | tf_op jit(solution)/shard_map/ppermute | solution.py:240
  124.3 2.3 %collective-permute-done.9 = f32[8,8,128]{2,1,0:T(8,128)S(1)} collective-permute-done((f32[8,8,128]{2,1,0:T(8,128)S(1)}, f32[8,8,128]{2,1,0:T(8,128)S(1)}, u32[]{:S(2)}, u32[]{:S(2)}) %collective-permute-start.9) | collective-permute-done | bytes 32800 | tf_op jit(solution)/shard_map/ppermute | solution.py:240
  126.7 1.9 %collective-permute-start.12 = (f32[4,8,8,128]{3,2,1,0:T(8,128)S(1)}, f32[4,8,8,128]{3,2,1,0:T(8,128)S(1)}, u32[]{:S(2)}, u32[]{:S(2)}) collective-permute-start(f32[4,8,8,128]{3,2,1,0:T(8,128)S(1)} %pad_maximum_fusion.1.near_ref), channel_id=1, source_target_pairs={{0,1},{1,0},{2,3},{3,2},{4,5},{5,4},{6,7},{7,6},{8,9},{9,8},{10,11... | collective-permute-start | bytes 393224 | tf_op jit(solution)/shard_map/ppermute | solution.py:248
  128.6 1.3 collective-permute-done.12.far_ref
  130.7 12.3 %all-to-all-done.3 = bf16[64,64,128]{2,1,0:T(8,128)(2,1)S(1)} async-done(((bf16[64,64,128]{2,1,0:T(8,128)(2,1)}), bf16[64,64,128]{2,1,0:T(8,128)(2,1)S(1)}, u32[]{:S(2)}, u32[]{:S(2)}) %all-to-all-start.3) | async-done | bytes 1048608 | tf_op jit(solution)/shard_map/all_to_all | solution.py:274
  (28 shorter events, 4.5 us)
Async XLA Ops:
  2.5 13.1 %collective-permute-start.3 = (bf16[1072,128]{1,0:T(8,128)(2,1)}, bf16[1072,128]{1,0:T(8,128)(2,1)S(1)}, u32[]{:S(2)}, u32[]{:S(2)}) collective-permute-start(bf16[1072,128]{1,0:T(8,128)(2,1)} %pack.1.q0), channel_id=1, source_target_pairs={{0,6},{2,0},{4,2},{6,4},{1,7},{3,1},{5,3},{7,5},{8,14},{10,8},{12,... | collective-permute-start | bytes 823304 | tf_op jit(solution)/shard_map/ppermute | solution.py:240
  10.3 10.1 %collective-permute-start.2 = (bf16[1072,128]{1,0:T(8,128)(2,1)}, bf16[1072,128]{1,0:T(8,128)(2,1)S(1)}, u32[]{:S(2)}, u32[]{:S(2)}) collective-permute-start(bf16[1072,128]{1,0:T(8,128)(2,1)} %pack.1.q0), channel_id=1, source_target_pairs={{0,4},{2,6},{4,0},{6,2},{1,5},{3,7},{5,1},{7,3},{8,12},{10,14},{12... | collective-permute-start | bytes 823304 | tf_op jit(solution)/shard_map/ppermute | solution.py:240
  12.2 10.3 %collective-permute-start.1 = (bf16[1072,128]{1,0:T(8,128)(2,1)}, bf16[1072,128]{1,0:T(8,128)(2,1)S(1)}, u32[]{:S(2)}, u32[]{:S(2)}) collective-permute-start(bf16[1072,128]{1,0:T(8,128)(2,1)} %pack.1.q0), channel_id=1, source_target_pairs={{0,2},{2,4},{4,6},{6,0},{1,3},{3,5},{5,7},{7,1},{8,10},{10,12},{12... | collective-permute-start | bytes 823304 | tf_op jit(solution)/shard_map/ppermute | solution.py:240
  22.5 35.6 %copy-start.4 = (s32[8,16]{1,0:T(8,128)S(1)}, s32[8,16]{1,0:T(8,128)}, u32[]{:S(2)}) copy-start(s32[8,16]{1,0:T(8,128)} %chosen_ref.1) | copy-start | bytes 1540
  23.6 43.5 %copy-start = (bf16[1072,128]{1,0:T(8,128)(2,1)S(1)}, bf16[1072,128]{1,0:T(8,128)(2,1)}, u32[]{:S(2)}) copy-start(bf16[1072,128]{1,0:T(8,128)(2,1)} %pack.1.q0) | copy-start | bytes 823300
  23.6 43.5 %collective-permute-start.4 = (bf16[4,1072,128]{2,1,0:T(8,128)(2,1)S(1)}, bf16[4,1072,128]{2,1,0:T(8,128)(2,1)S(1)}, u32[]{:S(2)}, u32[]{:S(2)}) collective-permute-start(bf16[4,1072,128]{2,1,0:T(8,128)(2,1)S(1)} %pad_maximum_fusion), channel_id=1, source_target_pairs={{0,1},{1,0},{2,3},{3,2},{4,5},{5,4},{6,7},{7,6},{8,9},{9,8},{10,11... | collective-permute-start | bytes 3293192 | tf_op jit(solution)/shard_map/ppermute | solution.py:248
  47.1 3.1 %collective-permute-start = (bf16[8,8,128]{2,1,0:T(8,128)(2,1)S(1)}, bf16[8,8,128]{2,1,0:T(8,128)(2,1)S(1)}, u32[]{:S(2)}, u32[]{:S(2)}) collective-permute-start(bf16[8,8,128]{2,1,0:T(8,128)(2,1)S(1)} %slice_bitcast_fusion.4), channel_id=1, source_target_pairs={{0,1},{1,0},{2,3},{3,2},{4,5},{5,4},{6,7},{7,6},{8,9},{9,8},{10,11... | collective-permute-start | bytes 49160 | tf_op jit(solution)/shard_map/ppermute | solution.py:248
  51.0 16.2 %all-to-all-start.1 = ((bf16[8,8,8,128]{3,2,1,0:T(8,128)(2,1)}), bf16[8,8,8,128]{3,2,1,0:T(8,128)(2,1)S(1)}, u32[]{:S(2)}, u32[]{:S(2)}) async-start(bf16[8,8,8,128]{3,2,1,0:T(8,128)(2,1)} %pick.1), calls=%async_computation.1 | async-start | bytes 262144 | tf_op jit(solution)/shard_map/all_to_all | solution.py:268
  67.1 0.8 copy-start.1
  67.9 0.7 copy-start.2
  75.4 3.8 %collective-permute-start.5 = (bf16[4,512,128]{2,1,0:T(8,128)(2,1)S(1)}, bf16[4,512,128]{2,1,0:T(8,128)(2,1)S(1)}, u32[]{:S(2)}, u32[]{:S(2)}) collective-permute-start(bf16[4,512,128]{2,1,0:T(8,128)(2,1)S(1)} %get-tuple-element.17), channel_id=1, source_target_pairs={{0,1},{1,0},{2,3},{3,2},{4,5},{5,4},{6,7},{7,6},{8,9},{9,8},{10,11... | collective-permute-start | bytes 1572872 | tf_op jit(solution)/shard_map/ppermute | solution.py:248
  79.4 15.8 %collective-permute-start.6 = (bf16[512,128]{1,0:T(8,128)(2,1)S(1)}, bf16[512,128]{1,0:T(8,128)(2,1)S(1)}, u32[]{:S(2)}, u32[]{:S(2)}) collective-permute-start(bf16[512,128]{1,0:T(8,128)(2,1)S(1)} %get-tuple-element.24), channel_id=1, source_target_pairs={{2,0},{4,2},{6,4},{0,6},{3,1},{5,3},{7,5},{1,7},{10,8},{12,10},{14... | collective-permute-start | bytes 393224 | tf_op jit(solution)/shard_map/ppermute | solution.py:244
  84.0 11.1 %collective-permute-start.8 = (bf16[512,128]{1,0:T(8,128)(2,1)S(1)}, bf16[512,128]{1,0:T(8,128)(2,1)S(1)}, u32[]{:S(2)}, u32[]{:S(2)}) collective-permute-start(bf16[512,128]{1,0:T(8,128)(2,1)S(1)} %get-tuple-element.25), channel_id=1, source_target_pairs={{6,0},{0,2},{2,4},{4,6},{7,1},{1,3},{3,5},{5,7},{14,8},{8,10},{10,... | collective-permute-start | bytes 393224 | tf_op jit(solution)/shard_map/ppermute | solution.py:244
  86.0 9.2 %collective-permute-start.7 = (bf16[512,128]{1,0:T(8,128)(2,1)S(1)}, bf16[512,128]{1,0:T(8,128)(2,1)S(1)}, u32[]{:S(2)}, u32[]{:S(2)}) collective-permute-start(bf16[512,128]{1,0:T(8,128)(2,1)S(1)} %get-tuple-element.26), channel_id=1, source_target_pairs={{4,0},{6,2},{0,4},{2,6},{5,1},{7,3},{1,5},{3,7},{12,8},{14,10},{8,... | collective-permute-start | bytes 393224 | tf_op jit(solution)/shard_map/ppermute | solution.py:244
  90.5 19.3 %all-to-all-start.2 = ((bf16[64,16,128]{2,1,0:T(8,128)(2,1)}), bf16[64,16,128]{2,1,0:T(8,128)(2,1)S(1)}, u32[]{:S(2)}, u32[]{:S(2)}) async-start(bf16[64,16,128]{2,1,0:T(8,128)(2,1)} %get-tuple-element.19), calls=%async_computation.2 | async-start | bytes 524288 | tf_op jit(solution)/shard_map/all_to_all | solution.py:274
  95.3 3.0 %copy-start.3 = (bf16[512,128]{1,0:T(8,128)(2,1)}, bf16[512,128]{1,0:T(8,128)(2,1)S(1)}, u32[]{:S(2)}) copy-start(bf16[512,128]{1,0:T(8,128)(2,1)S(1)} %fusion.4) | copy-start | bytes 393220
  109.8 33.3 %all-to-all-start.3 = ((bf16[64,64,128]{2,1,0:T(8,128)(2,1)}), bf16[64,64,128]{2,1,0:T(8,128)(2,1)S(1)}, u32[]{:S(2)}, u32[]{:S(2)}) async-start(bf16[64,64,128]{2,1,0:T(8,128)(2,1)} %bitcast.22), calls=%async_computation.3 | async-start | bytes 2097152 | tf_op jit(solution)/shard_map/all_to_all | solution.py:274
  114.7 9.5 %collective-permute-start.11 = (f32[8,8,128]{2,1,0:T(8,128)S(1)}, f32[8,8,128]{2,1,0:T(8,128)S(1)}, u32[]{:S(2)}, u32[]{:S(2)}) collective-permute-start(f32[8,8,128]{2,1,0:T(8,128)S(1)} %settle.1), channel_id=1, source_target_pairs={{0,6},{2,0},{4,2},{6,4},{1,7},{3,1},{5,3},{7,5},{8,14},{10,8},{12,... | collective-permute-start | bytes 98312 | tf_op jit(solution)/shard_map/ppermute | solution.py:240
  116.8 7.5 %collective-permute-start.10 = (f32[8,8,128]{2,1,0:T(8,128)S(1)}, f32[8,8,128]{2,1,0:T(8,128)S(1)}, u32[]{:S(2)}, u32[]{:S(2)}) collective-permute-start(f32[8,8,128]{2,1,0:T(8,128)S(1)} %settle.1), channel_id=1, source_target_pairs={{0,4},{2,6},{4,0},{6,2},{1,5},{3,7},{5,1},{7,3},{8,12},{10,14},{12... | collective-permute-start | bytes 98312 | tf_op jit(solution)/shard_map/ppermute | solution.py:240
  120.8 5.8 %collective-permute-start.9 = (f32[8,8,128]{2,1,0:T(8,128)S(1)}, f32[8,8,128]{2,1,0:T(8,128)S(1)}, u32[]{:S(2)}, u32[]{:S(2)}) collective-permute-start(f32[8,8,128]{2,1,0:T(8,128)S(1)} %settle.1), channel_id=1, source_target_pairs={{0,2},{2,4},{4,6},{6,0},{1,3},{3,5},{5,7},{7,1},{8,10},{10,12},{12... | collective-permute-start | bytes 98312 | tf_op jit(solution)/shard_map/ppermute | solution.py:240
  126.7 3.2 %collective-permute-start.12 = (f32[4,8,8,128]{3,2,1,0:T(8,128)S(1)}, f32[4,8,8,128]{3,2,1,0:T(8,128)S(1)}, u32[]{:S(2)}, u32[]{:S(2)}) collective-permute-start(f32[4,8,8,128]{3,2,1,0:T(8,128)S(1)} %pad_maximum_fusion.1.near_ref), channel_id=1, source_target_pairs={{0,1},{1,0},{2,3},{3,2},{4,5},{5,4},{6,7},{7,6},{8,9},{9,8},{10,11... | collective-permute-start | bytes 393224 | tf_op jit(solution)/shard_map/ppermute | solution.py:248

commit v6 on v5

--- a/solution.py
+++ b/solution.py
@@ -17,6 +17,7 @@
 LANES = 128
 SCALE = 0.125
 KV = ("z", "y")
+TP = ("x", "c")
 ALL = ("z", "y", "x", "c")
 FAR = 1 << 20
 F32 = jnp.float32
@@ -76,8 +77,9 @@
         want = given_ref[s, ROWS:].astype(F32)
         for b in range(BLOCKS):
             totals[b] = totals[b] + jnp.where(want == b + 1.0, got, 0.0)
-    for b in range(BLOCKS):
-        out_ref[b] = totals[b]
+    for i in range(SIDE):
+        for b in range(BLOCKS):
+            out_ref[i, b] = totals[b]
 
 
 def pack_kernel(q_ref, g_ref, o_ref, log_ref, out_ref):
@@ -201,15 +203,11 @@
     own_ref[...] = acc[PEERS:]
 
 
-def place_kernel(tp_ref, near_ref, far_ref, keys_ref, vals_ref, rows):
-    x = tp_ref[0] >> 1
-    mine = jnp.full((ROWS, LANES), tp_ref[0] & 1, jnp.int32)
-    for xa in range(4):
-        k = (x + 4 - xa) & 3
-        for ca in range(2):
-            for b in range(BLOCKS):
-                at = b * BLOCK + (xa * 2 + ca) * ROWS
-                rows[at : at + ROWS, :] = jnp.where(mine == ca, near_ref[k, b], far_ref[k, b])
+def place_kernel(pieces_ref, keys_ref, vals_ref, rows):
+    for i in range(SIDE):
+        for b in range(BLOCKS):
+            at = b * BLOCK + i * ROWS
+            rows[at : at + ROWS, :] = pieces_ref[i, b]
     turned = rows[...].T
     keys_ref[...] = turned[: LANES // 2]
     vals_ref[...] = turned[LANES // 2 :]
@@ -364,18 +362,17 @@
     total = call(
         settle_kernel,
         [VMEM] * 2,
-        held((BLOCKS, ROWS, LANES), F32),
+        held((SIDE, BLOCKS, ROWS, LANES), F32),
         (near_core(own), near_core(returned)),
         1 << 20,
         name="settle",
     )
-    near = jnp.stack([total] + [x_from(total, k) for k in (1, 2, 3)])
-    far = swap(near)
+    pieces = lax.all_to_all(total, TP, split_axis=0, concat_axis=0, tiled=True)
     grad_keys, grad_values = call(
         place_kernel,
-        [SMEM, VMEM, VMEM],
+        [VMEM],
         [sds((64, TOK), F32), sds((64, TOK), F32)],
-        (tp.reshape(1), near_core(near), near_core(far)),
+        (near_core(pieces),),
         1 << 20,
         scratch_shapes=[pltpu.VMEM((TOK, LANES), F32)],
         name="place",

time: 145 us -> 152 us (1.048)
  the two profiles are of different devices: /device:TPU:2 before, /device:TPU:24 now
where the time goes in v6:
time: 152 us; the launch traced here: 151 us
  waiting for transfers between devices  53.3 us (35%)
  starting transfers between devices  53 us (35%)
  blocking collectives  19.6 us (13%)
  Pallas kernels  13.2 us (9%)
  other arithmetic  4.23 us (3%)
  local copies, waits for them, and re-layouts  3.63 us (2%)
  matrix products  2.98 us (2%)
    all_to_all x2, waiting for transfers between devices, exchange(): return lax.all_to_all(arr, KV, split_axis=0, concat_axis=0, tiled=True)  31.8 us
    all_to_all x1, blocking collectives, along(): lax.all_to_all(arr, ALL, split_axis=0, concat_axis=0, tiled=True, axis_in...  19.6 us
    all_to_all x2, starting transfers between devices, exchange(): return lax.all_to_all(arr, KV, split_axis=0, concat_axis=0, tiled=True)  17.6 us
    pallas_call x6, Pallas kernels, call(): pl.pallas_call(kernel, in_specs=ins, out_specs=[VMEM] * len(out_shape) if...  13.2 us
    ppermute x3, waiting for transfers between devices, x_from(): return lax.ppermute(arr, 'x', [(i, (i + k) % 4) for i in range(4)])  12 us
    ppermute x3, starting transfers between devices, x_from(): return lax.ppermute(arr, 'x', [(i, (i + k) % 4) for i in range(4)])  10.2 us
    ppermute x3, starting transfers between devices, x_back(): return lax.ppermute(arr, 'x', [((i + k) % 4, i) for i in range(4)])  8.56 us
    all_to_all x1, starting transfers between devices, along(): lax.all_to_all(arr, ALL, split_axis=0, concat_axis=0, tiled=True, axis_in...  7.32 us
  transfers between devices with their start and end apart: 13, of which 8 were waited for; matrix products, arithmetic and copies ran while one was open for 4% of the time, Pallas kernels for 3%

profile of v6, /device:TPU:24, one launch (start us, length us, event | category | flops | bytes accessed | tf_op | source)
XLA Modules:
  0.0 150.7 jit_solution(1978453600901047911)
XLA Ops:
  0.6 1.9 %pack.1.q0 = bf16[1072,128]{1,0:T(8,128)(2,1)} custom-call(bf16[512,128]{1,0:T(8,128)(2,1)} %q_ref.1, bf16[512,128]{1,0:T(8,128)(2,1)} %g_ref.1, bf16[512,128]{1,0:T(8,128)(2,1)} %o_ref.1, f32[2,512]{1,0:T(2,128)} %bitcast.42), custom_call_target="tpu_custom_call" | custom-call | flops 262144 | bytes 1048576 | tf_op jit(solution)/shard_map/pack/pallas_call | solution.py:218
  2.5 4.7 %collective-permute-start.3 = (bf16[1072,128]{1,0:T(8,128)(2,1)}, bf16[1072,128]{1,0:T(8,128)(2,1)S(1)}, u32[]{:S(2)}, u32[]{:S(2)}) collective-permute-start(bf16[1072,128]{1,0:T(8,128)(2,1)} %pack.1.q0), channel_id=1, source_target_pairs={{0,6},{2,0},{4,2},{6,4},{1,7},{3,1},{5,3},{7,5},{8,14},{10,8},{12,... | collective-permute-start | bytes 823304 | tf_op jit(solution)/shard_map/ppermute | solution.py:238
  7.2 2.7 %collective-permute-start.2 = (bf16[1072,128]{1,0:T(8,128)(2,1)}, bf16[1072,128]{1,0:T(8,128)(2,1)S(1)}, u32[]{:S(2)}, u32[]{:S(2)}) collective-permute-start(bf16[1072,128]{1,0:T(8,128)(2,1)} %pack.1.q0), channel_id=1, source_target_pairs={{0,4},{2,6},{4,0},{6,2},{1,5},{3,7},{5,1},{7,3},{8,12},{10,14},{12... | collective-permute-start | bytes 823304 | tf_op jit(solution)/shard_map/ppermute | solution.py:238
  9.9 2.8 %collective-permute-start.1 = (bf16[1072,128]{1,0:T(8,128)(2,1)}, bf16[1072,128]{1,0:T(8,128)(2,1)S(1)}, u32[]{:S(2)}, u32[]{:S(2)}) collective-permute-start(bf16[1072,128]{1,0:T(8,128)(2,1)} %pack.1.q0), channel_id=1, source_target_pairs={{0,2},{2,4},{4,6},{6,0},{1,3},{3,5},{5,7},{7,1},{8,10},{10,12},{12... | collective-permute-start | bytes 823304 | tf_op jit(solution)/shard_map/ppermute | solution.py:238
  12.7 6.5 %collective-permute-done.3.q3 = bf16[1072,128]{1,0:T(8,128)(2,1)S(1)} collective-permute-done((bf16[1072,128]{1,0:T(8,128)(2,1)}, bf16[1072,128]{1,0:T(8,128)(2,1)S(1)}, u32[]{:S(2)}, u32[]{:S(2)}) %collective-permute-start.3) | collective-permute-done | bytes 274464 | tf_op jit(solution)/shard_map/ppermute | solution.py:238
  19.2 1.1 collective-permute-done.2.q2
  20.3 4.4 %collective-permute-done.1.q1 = bf16[1072,128]{1,0:T(8,128)(2,1)S(1)} collective-permute-done((bf16[1072,128]{1,0:T(8,128)(2,1)}, bf16[1072,128]{1,0:T(8,128)(2,1)S(1)}, u32[]{:S(2)}, u32[]{:S(2)}) %collective-permute-start.1) | collective-permute-done | bytes 274464 | tf_op jit(solution)/shard_map/ppermute | solution.py:238
  24.7 2.1 %pad_maximum_fusion = bf16[4,1072,128]{2,1,0:T(8,128)(2,1)} fusion(bf16[1,1072,128]{2,1,0:T(8,128)(2,1)S(1)} %bitcast.36, bf16[1,1072,128]{2,1,0:T(8,128)(2,1)S(1)} %bitcast.37, bf16[1,1072,128]{2,1,0:T(8,128)(2,1)S(1)} %bitcast.38, bf16[1,1072,128]{2,1,0:T(8,128)(2,1)} %bitcast.35), kind=kLoop, calls=%fused_computation.3 | loop fusion | flops 1646592 | bytes 2195456 | tf_op jit(solution)/shard_map/stack | solution.py:320
  26.8 2.0 %collective-permute-start.4 = (bf16[4,1072,128]{2,1,0:T(8,128)(2,1)}, bf16[4,1072,128]{2,1,0:T(8,128)(2,1)S(1)}, u32[]{:S(2)}, u32[]{:S(2)}) collective-permute-start(bf16[4,1072,128]{2,1,0:T(8,128)(2,1)} %pad_maximum_fusion), channel_id=1, source_target_pairs={{0,1},{1,0},{2,3},{3,2},{4,5},{5,4},{6,7},{7,6},{8,9},{9,8},{10,11... | collective-permute-start | bytes 3293192 | tf_op jit(solution)/shard_map/ppermute | solution.py:246
  28.9 1.8 %offer.1 = (bf16[8,9,8,128]{3,2,1,0:T(8,128)(2,1)}, bf16[8,8,128]{2,1,0:T(8,128)(2,1)}, f32[64,128]{1,0:T(8,128)}) custom-call(s32[1]{0:T(128)} %bitcast.rank_ref, s32[1]{0:T(128)} %bitcast.1.tp_ref, bf16[64,512]{1,0:T(8,128)(2,1)} %bitcast.40, bf16[64,512]{1,0:T(8,128)(2,1)} %bitcast.41, s32[8,16]{1,0:T(8,128)} %chosen_ref.1), custom_call_target="tpu_custom_call" | custom-call | flops 262144 | bytes 1048576 | tf_op jit(solution)/shard_map/offer/pallas_call | solution.py:218
  30.7 19.6 %all_to_all.25.pushed_ref = bf16[8,9,8,128]{3,2,1,0:T(8,128)(2,1)S(1)} all-to-all(bf16[8,9,8,128]{3,2,1,0:T(8,128)(2,1)} %get-tuple-element.13), channel_id=1, replica_groups={{0,64,128,192,256,320,384,448},{8,72,136,200,264,328,392,456},{16,80,14..., dimensions={0} | all-to-all | bytes 294912 | tf_op jit(solution)/shard_map/all_to_all | solution.py:266
  50.3 1.9 %collective-permute-start = (bf16[8,8,128]{2,1,0:T(8,128)(2,1)S(1)}, bf16[8,8,128]{2,1,0:T(8,128)(2,1)S(1)}, u32[]{:S(2)}, u32[]{:S(2)}) collective-permute-start(bf16[8,8,128]{2,1,0:T(8,128)(2,1)S(1)} %slice_bitcast_fusion.4), channel_id=1, source_target_pairs={{0,1},{1,0},{2,3},{3,2},{4,5},{5,4},{6,7},{7,6},{8,9},{9,8},{10,11... | collective-permute-start | bytes 49160 | tf_op jit(solution)/shard_map/ppermute | solution.py:246
  52.2 1.1 collective-permute-done.wants_ref
  53.3 0.8 pick.1
  54.1 7.3 %all-to-all-start.1 = ((bf16[8,8,8,128]{3,2,1,0:T(8,128)(2,1)}), bf16[8,8,8,128]{3,2,1,0:T(8,128)(2,1)S(1)}, u32[]{:S(2)}, u32[]{:S(2)}) async-start(bf16[8,8,8,128]{3,2,1,0:T(8,128)(2,1)} %pick.1), calls=%async_computation.1 | async-start | bytes 262144 | tf_op jit(solution)/shard_map/all_to_all | solution.py:266
  61.5 5.4 %all-to-all-done.1 = bf16[8,8,8,128]{3,2,1,0:T(8,128)(2,1)S(1)} async-done(((bf16[8,8,8,128]{3,2,1,0:T(8,128)(2,1)}), bf16[8,8,8,128]{3,2,1,0:T(8,128)(2,1)S(1)}, u32[]{:S(2)}, u32[]{:S(2)}) %all-to-all-start.1) | async-done | bytes 131104 | tf_op jit(solution)/shard_map/all_to_all | solution.py:266
  68.4 6.9 %attend.1 = (bf16[64,16,128]{2,1,0:T(8,128)(2,1)}, f32[8,8,128]{2,1,0:T(8,128)S(1)}, f32[4,512,128]{2,1,0:T(8,128)S(1)}, bf16[4,512,128]{2,1,0:T(8,128)(2,1)}) custom-call(s32[8,16]{1,0:T(8,128)S(1)} %get-tuple-element.28.slot_ref, s32[8,16]{1,0:T(8,128)S(1)} %get-tuple-element.29.home_ref, s32[8,16]{1,0:T(8,128)S(1)} %get-tuple-element.27.rel_ref, ...), custom_call_target="tpu_custom_call" | custom-call | flops 1073741824 | bytes 1048576 | tf_op jit(solution)/shard_map/attend/pallas_call | solution.py:218
  75.3 1.9 %collective-permute-start.5 = (bf16[4,512,128]{2,1,0:T(8,128)(2,1)}, bf16[4,512,128]{2,1,0:T(8,128)(2,1)S(1)}, u32[]{:S(2)}, u32[]{:S(2)}) collective-permute-start(bf16[4,512,128]{2,1,0:T(8,128)(2,1)} %get-tuple-element.17), channel_id=1, source_target_pairs={{0,1},{1,0},{2,3},{3,2},{4,5},{5,4},{6,7},{7,6},{8,9},{9,8},{10,11... | collective-permute-start | bytes 1572872 | tf_op jit(solution)/shard_map/ppermute | solution.py:246
  77.2 7.7 %all-to-all-start.2 = ((bf16[64,16,128]{2,1,0:T(8,128)(2,1)}), bf16[64,16,128]{2,1,0:T(8,128)(2,1)S(1)}, u32[]{:S(2)}, u32[]{:S(2)}) async-start(bf16[64,16,128]{2,1,0:T(8,128)(2,1)} %get-tuple-element.19), calls=%async_computation.2 | async-start | bytes 524288 | tf_op jit(solution)/shard_map/all_to_all | solution.py:272
  85.7 1.2 fusion.7
  87.0 2.5 %collective-permute-start.6 = (bf16[512,128]{1,0:T(8,128)(2,1)S(1)}, bf16[512,128]{1,0:T(8,128)(2,1)S(1)}, u32[]{:S(2)}, u32[]{:S(2)}) collective-permute-start(bf16[512,128]{1,0:T(8,128)(2,1)S(1)} %get-tuple-element.24), channel_id=1, source_target_pairs={{2,0},{4,2},{6,4},{0,6},{3,1},{5,3},{7,5},{1,7},{10,8},{12,10},{14... | collective-permute-start | bytes 393224 | tf_op jit(solution)/shard_map/ppermute | solution.py:242
  89.5 3.3 %collective-permute-start.8 = (bf16[512,128]{1,0:T(8,128)(2,1)S(1)}, bf16[512,128]{1,0:T(8,128)(2,1)S(1)}, u32[]{:S(2)}, u32[]{:S(2)}) collective-permute-start(bf16[512,128]{1,0:T(8,128)(2,1)S(1)} %get-tuple-element.25), channel_id=1, source_target_pairs={{6,0},{0,2},{2,4},{4,6},{7,1},{1,3},{3,5},{5,7},{14,8},{8,10},{10,... | collective-permute-start | bytes 393224 | tf_op jit(solution)/shard_map/ppermute | solution.py:242
  92.8 2.7 %collective-permute-start.7 = (bf16[512,128]{1,0:T(8,128)(2,1)S(1)}, bf16[512,128]{1,0:T(8,128)(2,1)S(1)}, u32[]{:S(2)}, u32[]{:S(2)}) collective-permute-start(bf16[512,128]{1,0:T(8,128)(2,1)S(1)} %get-tuple-element.26), channel_id=1, source_target_pairs={{4,0},{6,2},{0,4},{2,6},{5,1},{7,3},{1,5},{3,7},{12,8},{14,10},{8,... | collective-permute-start | bytes 393224 | tf_op jit(solution)/shard_map/ppermute | solution.py:242
  95.5 3.5 %all-to-all-done.2.given_ref = bf16[64,16,128]{2,1,0:T(8,128)(2,1)S(1)} async-done(((bf16[64,16,128]{2,1,0:T(8,128)(2,1)}), bf16[64,16,128]{2,1,0:T(8,128)(2,1)S(1)}, u32[]{:S(2)}, u32[]{:S(2)}) %all-to-all-start.2) | async-done | bytes 262176 | tf_op jit(solution)/shard_map/all_to_all | solution.py:272
  99.1 1.0 settle.1
  100.0 3.4 %all-to-all-start.3 = ((f32[8,8,8,128]{3,2,1,0:T(8,128)}), f32[8,8,8,128]{3,2,1,0:T(8,128)S(1)}, u32[]{:S(2)}, u32[]{:S(2)}) async-start(f32[8,8,8,128]{3,2,1,0:T(8,128)} %settle.1), calls=%async_computation.3 | async-start | bytes 524288 | tf_op jit(solution)/shard_map/all_to_all | solution.py:370
  103.6 3.0 %fusion = bf16[4096,128]{0,1:T(8,128)(2,1)S(1)} fusion(bf16[512,128]{1,0:T(8,128)(2,1)S(1)} %fusion.4, bf16[512,4096]{1,0:T(8,128)(2,1)} %param.8), kind=kOutput, calls=%fused_computation.1 | convolution fusion | flops 537395200 | bytes 5373952 | tf_op jit(solution)/shard_map/dot_general | solution.py:356
  106.6 1.3 copy.12
  107.9 3.0 %all-to-all-done.3.pieces_ref = f32[8,8,8,128]{3,2,1,0:T(8,128)S(1)} async-done(((f32[8,8,8,128]{3,2,1,0:T(8,128)}), f32[8,8,8,128]{3,2,1,0:T(8,128)S(1)}, u32[]{:S(2)}, u32[]{:S(2)}) %all-to-all-start.3) | async-done | bytes 262176 | tf_op jit(solution)/shard_map/all_to_all | solution.py:370
  110.9 9.9 %all-to-all-start.4 = ((bf16[64,64,128]{2,1,0:T(8,128)(2,1)}), bf16[64,64,128]{2,1,0:T(8,128)(2,1)S(1)}, u32[]{:S(2)}, u32[]{:S(2)}) async-start(bf16[64,64,128]{2,1,0:T(8,128)(2,1)} %bitcast.18), calls=%async_computation.4 | async-start | bytes 2097152 | tf_op jit(solution)/shard_map/all_to_all | solution.py:272
  120.8 0.8 place.1
  121.6 28.3 %all-to-all-done.4 = bf16[64,64,128]{2,1,0:T(8,128)(2,1)S(1)} async-done(((bf16[64,64,128]{2,1,0:T(8,128)(2,1)}), bf16[64,64,128]{2,1,0:T(8,128)(2,1)S(1)}, u32[]{:S(2)}, u32[]{:S(2)}) %all-to-all-start.4) | async-done | bytes 1048608 | tf_op jit(solution)/shard_map/all_to_all | solution.py:272
  (23 shorter events, 3.3 us)
Async XLA Ops:
  2.5 16.7 %collective-permute-start.3 = (bf16[1072,128]{1,0:T(8,128)(2,1)}, bf16[1072,128]{1,0:T(8,128)(2,1)S(1)}, u32[]{:S(2)}, u32[]{:S(2)}) collective-permute-start(bf16[1072,128]{1,0:T(8,128)(2,1)} %pack.1.q0), channel_id=1, source_target_pairs={{0,6},{2,0},{4,2},{6,4},{1,7},{3,1},{5,3},{7,5},{8,14},{10,8},{12,... | collective-permute-start | bytes 823304 | tf_op jit(solution)/shard_map/ppermute | solution.py:238
  7.2 13.1 %collective-permute-start.2 = (bf16[1072,128]{1,0:T(8,128)(2,1)}, bf16[1072,128]{1,0:T(8,128)(2,1)S(1)}, u32[]{:S(2)}, u32[]{:S(2)}) collective-permute-start(bf16[1072,128]{1,0:T(8,128)(2,1)} %pack.1.q0), channel_id=1, source_target_pairs={{0,4},{2,6},{4,0},{6,2},{1,5},{3,7},{5,1},{7,3},{8,12},{10,14},{12... | collective-permute-start | bytes 823304 | tf_op jit(solution)/shard_map/ppermute | solution.py:238
  9.9 14.8 %collective-permute-start.1 = (bf16[1072,128]{1,0:T(8,128)(2,1)}, bf16[1072,128]{1,0:T(8,128)(2,1)S(1)}, u32[]{:S(2)}, u32[]{:S(2)}) collective-permute-start(bf16[1072,128]{1,0:T(8,128)(2,1)} %pack.1.q0), channel_id=1, source_target_pairs={{0,2},{2,4},{4,6},{6,0},{1,3},{3,5},{5,7},{7,1},{8,10},{10,12},{12... | collective-permute-start | bytes 823304 | tf_op jit(solution)/shard_map/ppermute | solution.py:238
  24.7 36.8 %copy-start.5 = (s32[8,16]{1,0:T(8,128)S(1)}, s32[8,16]{1,0:T(8,128)}, u32[]{:S(2)}) copy-start(s32[8,16]{1,0:T(8,128)} %chosen_ref.1) | copy-start | bytes 1540
  26.8 40.1 %copy-start = (bf16[1072,128]{1,0:T(8,128)(2,1)S(1)}, bf16[1072,128]{1,0:T(8,128)(2,1)}, u32[]{:S(2)}) copy-start(bf16[1072,128]{1,0:T(8,128)(2,1)} %pack.1.q0) | copy-start | bytes 823300
  26.8 40.1 %collective-permute-start.4 = (bf16[4,1072,128]{2,1,0:T(8,128)(2,1)}, bf16[4,1072,128]{2,1,0:T(8,128)(2,1)S(1)}, u32[]{:S(2)}, u32[]{:S(2)}) collective-permute-start(bf16[4,1072,128]{2,1,0:T(8,128)(2,1)} %pad_maximum_fusion), channel_id=1, source_target_pairs={{0,1},{1,0},{2,3},{3,2},{4,5},{5,4},{6,7},{7,6},{8,9},{9,8},{10,11... | collective-permute-start | bytes 3293192 | tf_op jit(solution)/shard_map/ppermute | solution.py:246
  50.3 3.1 %collective-permute-start = (bf16[8,8,128]{2,1,0:T(8,128)(2,1)S(1)}, bf16[8,8,128]{2,1,0:T(8,128)(2,1)S(1)}, u32[]{:S(2)}, u32[]{:S(2)}) collective-permute-start(bf16[8,8,128]{2,1,0:T(8,128)(2,1)S(1)} %slice_bitcast_fusion.4), channel_id=1, source_target_pairs={{0,1},{1,0},{2,3},{3,2},{4,5},{5,4},{6,7},{7,6},{8,9},{9,8},{10,11... | collective-permute-start | bytes 49160 | tf_op jit(solution)/shard_map/ppermute | solution.py:246
  54.1 12.8 %all-to-all-start.1 = ((bf16[8,8,8,128]{3,2,1,0:T(8,128)(2,1)}), bf16[8,8,8,128]{3,2,1,0:T(8,128)(2,1)S(1)}, u32[]{:S(2)}, u32[]{:S(2)}) async-start(bf16[8,8,8,128]{3,2,1,0:T(8,128)(2,1)} %pick.1), calls=%async_computation.1 | async-start | bytes 262144 | tf_op jit(solution)/shard_map/all_to_all | solution.py:266
  66.9 0.8 copy-start.1
  67.7 0.7 copy-start.2
  75.3 9.6 %collective-permute-start.5 = (bf16[4,512,128]{2,1,0:T(8,128)(2,1)}, bf16[4,512,128]{2,1,0:T(8,128)(2,1)S(1)}, u32[]{:S(2)}, u32[]{:S(2)}) collective-permute-start(bf16[4,512,128]{2,1,0:T(8,128)(2,1)} %get-tuple-element.17), channel_id=1, source_target_pairs={{0,1},{1,0},{2,3},{3,2},{4,5},{5,4},{6,7},{7,6},{8,9},{9,8},{10,11... | collective-permute-start | bytes 1572872 | tf_op jit(solution)/shard_map/ppermute | solution.py:246
  77.2 21.8 %all-to-all-start.2 = ((bf16[64,16,128]{2,1,0:T(8,128)(2,1)}), bf16[64,16,128]{2,1,0:T(8,128)(2,1)S(1)}, u32[]{:S(2)}, u32[]{:S(2)}) async-start(bf16[64,16,128]{2,1,0:T(8,128)(2,1)} %get-tuple-element.19), calls=%async_computation.2 | async-start | bytes 524288 | tf_op jit(solution)/shard_map/all_to_all | solution.py:272
  84.9 0.8 copy-start.3
  87.0 16.5 %collective-permute-start.6 = (bf16[512,128]{1,0:T(8,128)(2,1)S(1)}, bf16[512,128]{1,0:T(8,128)(2,1)S(1)}, u32[]{:S(2)}, u32[]{:S(2)}) collective-permute-start(bf16[512,128]{1,0:T(8,128)(2,1)S(1)} %get-tuple-element.24), channel_id=1, source_target_pairs={{2,0},{4,2},{6,4},{0,6},{3,1},{5,3},{7,5},{1,7},{10,8},{12,10},{14... | collective-permute-start | bytes 393224 | tf_op jit(solution)/shard_map/ppermute | solution.py:242
  89.5 14.0 %collective-permute-start.8 = (bf16[512,128]{1,0:T(8,128)(2,1)S(1)}, bf16[512,128]{1,0:T(8,128)(2,1)S(1)}, u32[]{:S(2)}, u32[]{:S(2)}) collective-permute-start(bf16[512,128]{1,0:T(8,128)(2,1)S(1)} %get-tuple-element.25), channel_id=1, source_target_pairs={{6,0},{0,2},{2,4},{4,6},{7,1},{1,3},{3,5},{5,7},{14,8},{8,10},{10,... | collective-permute-start | bytes 393224 | tf_op jit(solution)/shard_map/ppermute | solution.py:242
  92.8 10.7 %collective-permute-start.7 = (bf16[512,128]{1,0:T(8,128)(2,1)S(1)}, bf16[512,128]{1,0:T(8,128)(2,1)S(1)}, u32[]{:S(2)}, u32[]{:S(2)}) collective-permute-start(bf16[512,128]{1,0:T(8,128)(2,1)S(1)} %get-tuple-element.26), channel_id=1, source_target_pairs={{4,0},{6,2},{0,4},{2,6},{5,1},{7,3},{1,5},{3,7},{12,8},{14,10},{8,... | collective-permute-start | bytes 393224 | tf_op jit(solution)/shard_map/ppermute | solution.py:242
  100.0 10.8 %all-to-all-start.3 = ((f32[8,8,8,128]{3,2,1,0:T(8,128)}), f32[8,8,8,128]{3,2,1,0:T(8,128)S(1)}, u32[]{:S(2)}, u32[]{:S(2)}) async-start(f32[8,8,8,128]{3,2,1,0:T(8,128)} %settle.1), calls=%async_computation.3 | async-start | bytes 524288 | tf_op jit(solution)/shard_map/all_to_all | solution.py:370
  103.5 3.0 %copy-start.4 = (bf16[512,128]{1,0:T(8,128)(2,1)}, bf16[512,128]{1,0:T(8,128)(2,1)S(1)}, u32[]{:S(2)}) copy-start(bf16[512,128]{1,0:T(8,128)(2,1)S(1)} %fusion.4) | copy-start | bytes 393220
  110.9 39.0 %all-to-all-start.4 = ((bf16[64,64,128]{2,1,0:T(8,128)(2,1)}), bf16[64,64,128]{2,1,0:T(8,128)(2,1)S(1)}, u32[]{:S(2)}, u32[]{:S(2)}) async-start(bf16[64,64,128]{2,1,0:T(8,128)(2,1)} %bitcast.18), calls=%async_computation.4 | async-start | bytes 2097152 | tf_op jit(solution)/shard_map/all_to_all | solution.py:272

commit v7 on v5

--- a/solution.py
+++ b/solution.py
@@ -16,6 +16,7 @@
 TOK = 512
 LANES = 128
 SCALE = 0.125
+LOG2E = 1.4426950408889634
 KV = ("z", "y")
 ALL = ("z", "y", "x", "c")
 FAR = 1 << 20
@@ -78,6 +79,24 @@
             totals[b] = totals[b] + jnp.where(want == b + 1.0, got, 0.0)
     for b in range(BLOCKS):
         out_ref[b] = totals[b]
+
+
+def turn_kernel(tp_ref, part_ref, out_ref):
+    flip = tp_ref[0] & 1
+    for m in range(PEERS // 2):
+        two = part_ref[:, m * LANES : (m + 1) * LANES].astype(F32).T.astype(BF16)
+        for n in range(2):
+            q = 2 * m + n
+            at = jnp.where(flip == 0, q, (q & 7) * SIDE + (q >> 3))
+            out_ref[at] = two[n * BLOCK : (n + 1) * BLOCK]
+
+
+def fold_kernel(parts_ref, out_ref):
+    for q in range(SIDE):
+        total = parts_ref[0, q].astype(F32)
+        for i in range(1, SIDE):
+            total = total + parts_ref[i, q].astype(F32)
+        out_ref[q] = total.astype(BF16)
 
 
 def pack_kernel(q_ref, g_ref, o_ref, log_ref, out_ref):
@@ -134,7 +153,9 @@
         for n in range(3):
             at = 2 * TOK + 16 * n
             parts.append((near[p][at : at + 16, :] if p < 4 else qp_ref[p - 4, at : at + 16, :]).astype(F32))
-        return parts[0] + parts[1] + parts[2]
+        total = parts[0] + parts[1] + parts[2]
+        kind = lax.broadcasted_iota(jnp.int32, total.shape, 0) & 3
+        return total * jnp.where(kind < 2, LOG2E, SCALE)
 
     for pair in range(4):
         even, odd = stat(2 * pair), stat(2 * pair + 1)
@@ -149,8 +170,10 @@
     def one_block(j, carry):
         kv = jnp.concatenate([table[slot_ref[j, s]] for s in range(SLOTS)], axis=0)
         turned = pltpu.roll(kv, LANES // 2, 1)
+        scaled = turned * SCALE
+        kept = kv * SCALE
         k2 = jnp.concatenate([jnp.where(low, kv, 0.0), jnp.where(low, 0.0, turned)], axis=0).astype(BF16)
-        v2 = jnp.concatenate([jnp.where(low, turned, 0.0), jnp.where(low, 0.0, kv)], axis=0).astype(BF16)
+        v2 = jnp.concatenate([jnp.where(low, scaled, 0.0), jnp.where(low, 0.0, kept)], axis=0).astype(BF16)
         at = pl.multiple_of(j * BLOCK, BLOCK)
         q = jnp.concatenate(
             [r[pl.ds(at, BLOCK), :] for r in near]
@@ -174,9 +197,9 @@
         for h in range(2):
             s = scores[h * LANES : (h + 1) * LANES]
             d = dprobs[h * LANES : (h + 1) * LANES]
-            p = jnp.where(seen, jnp.exp(s * SCALE - stat_j[h : h + 1, :]), 0.0)
+            p = jnp.where(seen, jnp.exp2(s * (SCALE * LOG2E) - stat_j[h : h + 1, :]), 0.0)
             probs.append(p.astype(BF16))
-            dscores.append((p * (d - stat_j[2 + h : 3 + h, :]) * SCALE).astype(BF16))
+            dscores.append((p * (d - stat_j[2 + h : 3 + h, :])).astype(BF16))
         probs = jnp.concatenate(probs, axis=0)
         dscores = jnp.concatenate(dscores, axis=0)
         plain = (((1,), (0,)), ((), ()))
@@ -193,7 +216,12 @@
             acc[home_ref[j, s]] += both[s * ROWS : (s + 1) * ROWS]
         return carry
 
-    lax.fori_loop(0, BLOCKS, one_block, 0)
+    def some_blocks(i, carry):
+        for n in range(2):
+            one_block(i * 2 + n, carry)
+        return carry
+
+    lax.fori_loop(0, BLOCKS // 2, some_blocks, 0)
     away_ref[:, :ROWS] = acc[:PEERS].astype(BF16)
     for s in range(PEERS):
         want = jnp.broadcast_to(want_ref[s : s + 1, :], (ROWS, LANES))
@@ -356,9 +384,26 @@
         gq = gq + x_back(gq4[k].astype(BF16), k).astype(F32)
     grad_queries = gq.astype(BF16)
     part = lax.dot_general(
-        normed, grad_queries, (((0,), (0,)), ((), ())), preferred_element_type=F32
+        grad_queries, normed, (((0,), (0,)), ((), ())), preferred_element_type=F32
     ).astype(BF16)
-    parts = exchange(part.reshape(PEERS, BLOCK, LANES))
+    turned = call(
+        turn_kernel,
+        [SMEM, VMEM],
+        held((PEERS, BLOCK, LANES), BF16),
+        (tp.reshape(1), near_core(part)),
+        1 << 20,
+        name="turn",
+    )
+    parts = along(turned.reshape(SIDE, SIDE, BLOCK, LANES), True)
+    half = call(
+        fold_kernel,
+        [VMEM],
+        held((SIDE, BLOCK, LANES), BF16),
+        (near_core(parts),),
+        1 << 20,
+        name="fold",
+    )
+    parts = along(half, False)
     weight_grad = jnp.sum(parts.astype(F32), axis=0)
 
     total = call(

time: 145 us -> 147 us (1.014)
  starting transfers between devices: 57.9 us -> 60.1 us
    all_to_all x1 -> x3, waiting for transfers between devices: 8.98 us -> 22.9 us  [along(): lax.all_to_all(arr, ALL, split_axis=0, concat_axis=0, tiled=True, axis_in...]
    all_to_all x2 -> x1, waiting for transfers between devices: 22.6 us -> 10.2 us  [exchange(): return lax.all_to_all(arr, KV, split_axis=0, concat_axis=0, tiled=True)]
    all_to_all x1 -> x3, starting transfers between devices: 7.1 us -> 14 us  [along(): lax.all_to_all(arr, ALL, split_axis=0, concat_axis=0, tiled=True, axis_in...]
    all_to_all x2 -> x1, starting transfers between devices: 9.27 us -> 4.62 us  [exchange(): return lax.all_to_all(arr, KV, split_axis=0, concat_axis=0, tiled=True)]
    ppermute x6, waiting for transfers between devices: 9.24 us -> 6.89 us  [x_from(): return lax.ppermute(arr, 'x', [(i, (i + k) % 4) for i in range(4)])]
    pallas_call x6 -> x8, Pallas kernels: 12.4 us -> 13.3 us  [call(): pl.pallas_call(kernel, in_specs=ins, out_specs=[VMEM] * len(out_shape) if...]
  transfers between devices with their start and end apart: 16 -> 17, of which waited for: 9 -> 9; matrix products, arithmetic and copies ran while one was open for 3% -> 2% of each run, Pallas kernels for 3% -> 4%
where the time goes in v7:
time: 147 us; the launch traced here: 146 us
  starting transfers between devices  60.1 us (41%)
  waiting for transfers between devices  44.4 us (30%)
  blocking collectives  19.6 us (13%)
  Pallas kernels  13.3 us (9%)
  other arithmetic  3.03 us (2%)
  matrix products  2.98 us (2%)
  local copies, waits for them, and re-layouts  1.52 us (1%)
    all_to_all x3, waiting for transfers between devices, along(): lax.all_to_all(arr, ALL, split_axis=0, concat_axis=0, tiled=True, axis_in...  22.9 us
    ppermute x6, starting transfers between devices, x_from(): return lax.ppermute(arr, 'x', [(i, (i + k) % 4) for i in range(4)])  22.6 us
    all_to_all x1, blocking collectives, along(): lax.all_to_all(arr, ALL, split_axis=0, concat_axis=0, tiled=True, axis_in...  19.6 us
    all_to_all x3, starting transfers between devices, along(): lax.all_to_all(arr, ALL, split_axis=0, concat_axis=0, tiled=True, axis_in...  14 us
    pallas_call x8, Pallas kernels, call(): pl.pallas_call(kernel, in_specs=ins, out_specs=[VMEM] * len(out_shape) if...  13.3 us
    ppermute x3, starting transfers between devices, x_back(): return lax.ppermute(arr, 'x', [((i + k) % 4, i) for i in range(4)])  11.1 us
    all_to_all x1, waiting for transfers between devices, exchange(): return lax.all_to_all(arr, KV, split_axis=0, concat_axis=0, tiled=True)  10.2 us
    ppermute x4, starting transfers between devices, swap(): return lax.ppermute(arr, 'c', [(0, 1), (1, 0)])  7.78 us
  transfers between devices with their start and end apart: 17, of which 9 were waited for; matrix products, arithmetic and copies ran while one was open for 2% of the time, Pallas kernels for 4%

profile of v7, /device:TPU:2, one launch (start us, length us, event | category | flops | bytes accessed | tf_op | source)
XLA Modules:
  0.0 145.8 jit_solution(7360474276840673545)
XLA Ops:
  0.6 1.9 %pack.1.q0 = bf16[1072,128]{1,0:T(8,128)(2,1)} custom-call(bf16[512,128]{1,0:T(8,128)(2,1)} %q_ref.1, bf16[512,128]{1,0:T(8,128)(2,1)} %g_ref.1, bf16[512,128]{1,0:T(8,128)(2,1)} %o_ref.1, f32[2,512]{1,0:T(2,128)} %bitcast.48), custom_call_target="tpu_custom_call" | custom-call | flops 262144 | bytes 1048576 | tf_op jit(solution)/shard_map/pack/pallas_call | solution.py:248
  2.5 7.8 %collective-permute-start.3 = (bf16[1072,128]{1,0:T(8,128)(2,1)}, bf16[1072,128]{1,0:T(8,128)(2,1)S(1)}, u32[]{:S(2)}, u32[]{:S(2)}) collective-permute-start(bf16[1072,128]{1,0:T(8,128)(2,1)} %pack.1.q0), channel_id=1, source_target_pairs={{0,6},{2,0},{4,2},{6,4},{1,7},{3,1},{5,3},{7,5},{8,14},{10,8},{12,... | collective-permute-start | bytes 823304 | tf_op jit(solution)/shard_map/ppermute | solution.py:268
  10.3 1.9 %collective-permute-start.2 = (bf16[1072,128]{1,0:T(8,128)(2,1)}, bf16[1072,128]{1,0:T(8,128)(2,1)S(1)}, u32[]{:S(2)}, u32[]{:S(2)}) collective-permute-start(bf16[1072,128]{1,0:T(8,128)(2,1)} %pack.1.q0), channel_id=1, source_target_pairs={{0,4},{2,6},{4,0},{6,2},{1,5},{3,7},{5,1},{7,3},{8,12},{10,14},{12... | collective-permute-start | bytes 823304 | tf_op jit(solution)/shard_map/ppermute | solution.py:268
  12.2 3.4 %collective-permute-start.1 = (bf16[1072,128]{1,0:T(8,128)(2,1)}, bf16[1072,128]{1,0:T(8,128)(2,1)S(1)}, u32[]{:S(2)}, u32[]{:S(2)}) collective-permute-start(bf16[1072,128]{1,0:T(8,128)(2,1)} %pack.1.q0), channel_id=1, source_target_pairs={{0,2},{2,4},{4,6},{6,0},{1,3},{3,5},{5,7},{7,1},{8,10},{10,12},{12... | collective-permute-start | bytes 823304 | tf_op jit(solution)/shard_map/ppermute | solution.py:268
  15.6 4.8 %collective-permute-done.2.q2 = bf16[1072,128]{1,0:T(8,128)(2,1)S(1)} collective-permute-done((bf16[1072,128]{1,0:T(8,128)(2,1)}, bf16[1072,128]{1,0:T(8,128)(2,1)S(1)}, u32[]{:S(2)}, u32[]{:S(2)}) %collective-permute-start.2) | collective-permute-done | bytes 274464 | tf_op jit(solution)/shard_map/ppermute | solution.py:268
  20.4 2.1 %collective-permute-done.1.q1 = bf16[1072,128]{1,0:T(8,128)(2,1)S(1)} collective-permute-done((bf16[1072,128]{1,0:T(8,128)(2,1)}, bf16[1072,128]{1,0:T(8,128)(2,1)S(1)}, u32[]{:S(2)}, u32[]{:S(2)}) %collective-permute-start.1) | collective-permute-done | bytes 274464 | tf_op jit(solution)/shard_map/ppermute | solution.py:268
  22.5 2.1 %pad_maximum_fusion = bf16[4,1072,128]{2,1,0:T(8,128)(2,1)} fusion(bf16[1,1072,128]{2,1,0:T(8,128)(2,1)S(1)} %bitcast.38, bf16[1,1072,128]{2,1,0:T(8,128)(2,1)S(1)} %bitcast.39, bf16[1,1072,128]{2,1,0:T(8,128)(2,1)S(1)} %bitcast.40, bf16[1,1072,128]{2,1,0:T(8,128)(2,1)} %bitcast.37), kind=kLoop, calls=%fused_computation.1 | loop fusion | flops 1646592 | bytes 2195456 | tf_op jit(solution)/shard_map/stack | solution.py:350
  24.6 2.0 %collective-permute-start.4 = (bf16[4,1072,128]{2,1,0:T(8,128)(2,1)}, bf16[4,1072,128]{2,1,0:T(8,128)(2,1)S(1)}, u32[]{:S(2)}, u32[]{:S(2)}) collective-permute-start(bf16[4,1072,128]{2,1,0:T(8,128)(2,1)} %pad_maximum_fusion), channel_id=1, source_target_pairs={{0,1},{1,0},{2,3},{3,2},{4,5},{5,4},{6,7},{7,6},{8,9},{9,8},{10,11... | collective-permute-start | bytes 3293192 | tf_op jit(solution)/shard_map/ppermute | solution.py:276
  26.7 1.8 %offer.1 = (bf16[8,9,8,128]{3,2,1,0:T(8,128)(2,1)}, bf16[8,8,128]{2,1,0:T(8,128)(2,1)}, f32[64,128]{1,0:T(8,128)}) custom-call(s32[1]{0:T(128)} %bitcast.rank_ref, s32[1]{0:T(128)} %bitcast.1.tp_ref, bf16[64,512]{1,0:T(8,128)(2,1)} %bitcast.43, bf16[64,512]{1,0:T(8,128)(2,1)} %bitcast.44, s32[8,16]{1,0:T(8,128)} %chosen_ref.1), custom_call_target="tpu_custom_call" | custom-call | flops 262144 | bytes 1048576 | tf_op jit(solution)/shard_map/offer/pallas_call | solution.py:248
  28.5 19.6 %all_to_all.25.pushed_ref = bf16[8,9,8,128]{3,2,1,0:T(8,128)(2,1)S(1)} all-to-all(bf16[8,9,8,128]{3,2,1,0:T(8,128)(2,1)} %get-tuple-element.13), channel_id=1, replica_groups={{0,64,128,192,256,320,384,448},{8,72,136,200,264,328,392,456},{16,80,14..., dimensions={0} | all-to-all | bytes 294912 | tf_op jit(solution)/shard_map/all_to_all | solution.py:296
  48.0 1.9 %collective-permute-start = (bf16[8,8,128]{2,1,0:T(8,128)(2,1)S(1)}, bf16[8,8,128]{2,1,0:T(8,128)(2,1)S(1)}, u32[]{:S(2)}, u32[]{:S(2)}) collective-permute-start(bf16[8,8,128]{2,1,0:T(8,128)(2,1)S(1)} %slice_bitcast_fusion.4), channel_id=1, source_target_pairs={{0,1},{1,0},{2,3},{3,2},{4,5},{5,4},{6,7},{7,6},{8,9},{9,8},{10,11... | collective-permute-start | bytes 49160 | tf_op jit(solution)/shard_map/ppermute | solution.py:276
  51.9 7.1 %all-to-all-start.1 = ((bf16[8,8,8,128]{3,2,1,0:T(8,128)(2,1)}), bf16[8,8,8,128]{3,2,1,0:T(8,128)(2,1)S(1)}, u32[]{:S(2)}, u32[]{:S(2)}) async-start(bf16[8,8,8,128]{3,2,1,0:T(8,128)(2,1)} %pick.1), calls=%async_computation.1 | async-start | bytes 262144 | tf_op jit(solution)/shard_map/all_to_all | solution.py:296
  59.1 9.0 %all-to-all-done.1 = bf16[8,8,8,128]{3,2,1,0:T(8,128)(2,1)S(1)} async-done(((bf16[8,8,8,128]{3,2,1,0:T(8,128)(2,1)}), bf16[8,8,8,128]{3,2,1,0:T(8,128)(2,1)S(1)}, u32[]{:S(2)}, u32[]{:S(2)}) %all-to-all-start.1) | async-done | bytes 131104 | tf_op jit(solution)/shard_map/all_to_all | solution.py:296
  69.6 5.6 %attend.1 = (bf16[64,16,128]{2,1,0:T(8,128)(2,1)}, f32[8,8,128]{2,1,0:T(8,128)S(1)}, f32[4,512,128]{2,1,0:T(8,128)S(1)}, bf16[4,512,128]{2,1,0:T(8,128)(2,1)S(1)}) custom-call(s32[8,16]{1,0:T(8,128)S(1)} %get-tuple-element.28.slot_ref, s32[8,16]{1,0:T(8,128)S(1)} %get-tuple-element.29.home_ref, s32[8,16]{1,0:T(8,128)S(1)} %get-tuple-element.27.rel_ref, ...), custom_call_target="tpu_custom_call" | custom-call | flops 1073741824 | bytes 1048576 | tf_op jit(solution)/shard_map/attend/pallas_call | solution.py:248
  75.2 1.9 %collective-permute-start.5 = (bf16[4,512,128]{2,1,0:T(8,128)(2,1)S(1)}, bf16[4,512,128]{2,1,0:T(8,128)(2,1)S(1)}, u32[]{:S(2)}, u32[]{:S(2)}) collective-permute-start(bf16[4,512,128]{2,1,0:T(8,128)(2,1)S(1)} %get-tuple-element.17), channel_id=1, source_target_pairs={{0,1},{1,0},{2,3},{3,2},{4,5},{5,4},{6,7},{7,6},{8,9},{9,8},{10,11... | collective-permute-start | bytes 1572872 | tf_op jit(solution)/shard_map/ppermute | solution.py:276
  77.1 1.9 %collective-permute-done.5 = bf16[4,512,128]{2,1,0:T(8,128)(2,1)S(1)} collective-permute-done((bf16[4,512,128]{2,1,0:T(8,128)(2,1)S(1)}, bf16[4,512,128]{2,1,0:T(8,128)(2,1)S(1)}, u32[]{:S(2)}, u32[]{:S(2)}) %collective-permute-start.5) | collective-permute-done | bytes 524320 | tf_op jit(solution)/shard_map/ppermute | solution.py:276
  79.2 4.6 %collective-permute-start.6 = (bf16[512,128]{1,0:T(8,128)(2,1)S(1)}, bf16[512,128]{1,0:T(8,128)(2,1)S(1)}, u32[]{:S(2)}, u32[]{:S(2)}) collective-permute-start(bf16[512,128]{1,0:T(8,128)(2,1)S(1)} %get-tuple-element.24), channel_id=1, source_target_pairs={{2,0},{4,2},{6,4},{0,6},{3,1},{5,3},{7,5},{1,7},{10,8},{12,10},{14... | collective-permute-start | bytes 393224 | tf_op jit(solution)/shard_map/ppermute | solution.py:272
  83.8 1.9 %collective-permute-start.8 = (bf16[512,128]{1,0:T(8,128)(2,1)S(1)}, bf16[512,128]{1,0:T(8,128)(2,1)S(1)}, u32[]{:S(2)}, u32[]{:S(2)}) collective-permute-start(bf16[512,128]{1,0:T(8,128)(2,1)S(1)} %get-tuple-element.25), channel_id=1, source_target_pairs={{6,0},{0,2},{2,4},{4,6},{7,1},{1,3},{3,5},{5,7},{14,8},{8,10},{10,... | collective-permute-start | bytes 393224 | tf_op jit(solution)/shard_map/ppermute | solution.py:272
  85.7 4.6 %collective-permute-start.7 = (bf16[512,128]{1,0:T(8,128)(2,1)S(1)}, bf16[512,128]{1,0:T(8,128)(2,1)S(1)}, u32[]{:S(2)}, u32[]{:S(2)}) collective-permute-start(bf16[512,128]{1,0:T(8,128)(2,1)S(1)} %get-tuple-element.26), channel_id=1, source_target_pairs={{4,0},{6,2},{0,4},{2,6},{5,1},{7,3},{1,5},{3,7},{12,8},{14,10},{8,... | collective-permute-start | bytes 393224 | tf_op jit(solution)/shard_map/ppermute | solution.py:272
  90.3 4.6 %all-to-all-start.2 = ((bf16[64,16,128]{2,1,0:T(8,128)(2,1)}), bf16[64,16,128]{2,1,0:T(8,128)(2,1)S(1)}, u32[]{:S(2)}, u32[]{:S(2)}) async-start(bf16[64,16,128]{2,1,0:T(8,128)(2,1)} %get-tuple-element.19), calls=%async_computation.2 | async-start | bytes 524288 | tf_op jit(solution)/shard_map/all_to_all | solution.py:302
  95.0 3.0 %convolution_convert_fusion.part_ref = bf16[128,4096]{1,0:T(8,128)(2,1)S(1)} fusion(bf16[512,128]{1,0:T(8,128)(2,1)S(1)} %fusion.3, bf16[512,4096]{1,0:T(8,128)(2,1)} %param.8), kind=kOutput, calls=%fused_computation | convolution fusion | flops 537395200 | bytes 5373952 | tf_op jit(solution)/shard_map/dot_general | solution.py:386
  98.0 1.3 turn.1
  99.4 10.2 %all-to-all-done.2.given_ref = bf16[64,16,128]{2,1,0:T(8,128)(2,1)S(1)} async-done(((bf16[64,16,128]{2,1,0:T(8,128)(2,1)}), bf16[64,16,128]{2,1,0:T(8,128)(2,1)S(1)}, u32[]{:S(2)}, u32[]{:S(2)}) %all-to-all-start.2) | async-done | bytes 262176 | tf_op jit(solution)/shard_map/all_to_all | solution.py:302
  109.6 3.6 %all-to-all-start.3 = ((bf16[8,8,64,128]{3,2,1,0:T(8,128)(2,1)}), bf16[8,8,64,128]{3,2,1,0:T(8,128)(2,1)S(1)}, u32[]{:S(2)}, u32[]{:S(2)}) async-start(bf16[8,8,64,128]{3,2,1,0:T(8,128)(2,1)} %bitcast.21), calls=%async_computation.3 | async-start | bytes 2097152 | tf_op jit(solution)/shard_map/all_to_all | solution.py:296
  113.4 2.1 %collective-permute-start.11 = (f32[8,8,128]{2,1,0:T(8,128)S(1)}, f32[8,8,128]{2,1,0:T(8,128)S(1)}, u32[]{:S(2)}, u32[]{:S(2)}) collective-permute-start(f32[8,8,128]{2,1,0:T(8,128)S(1)} %settle.1), channel_id=1, source_target_pairs={{0,6},{2,0},{4,2},{6,4},{1,7},{3,1},{5,3},{7,5},{8,14},{10,8},{12,... | collective-permute-start | bytes 98312 | tf_op jit(solution)/shard_map/ppermute | solution.py:268
  115.5 4.0 %collective-permute-start.10 = (f32[8,8,128]{2,1,0:T(8,128)S(1)}, f32[8,8,128]{2,1,0:T(8,128)S(1)}, u32[]{:S(2)}, u32[]{:S(2)}) collective-permute-start(f32[8,8,128]{2,1,0:T(8,128)S(1)} %settle.1), channel_id=1, source_target_pairs={{0,4},{2,6},{4,0},{6,2},{1,5},{3,7},{5,1},{7,3},{8,12},{10,14},{12... | collective-permute-start | bytes 98312 | tf_op jit(solution)/shard_map/ppermute | solution.py:268
  119.5 3.4 %collective-permute-start.9 = (f32[8,8,128]{2,1,0:T(8,128)S(1)}, f32[8,8,128]{2,1,0:T(8,128)S(1)}, u32[]{:S(2)}, u32[]{:S(2)}) collective-permute-start(f32[8,8,128]{2,1,0:T(8,128)S(1)} %settle.1), channel_id=1, source_target_pairs={{0,2},{2,4},{4,6},{6,0},{1,3},{3,5},{5,7},{7,1},{8,10},{10,12},{12... | collective-permute-start | bytes 98312 | tf_op jit(solution)/shard_map/ppermute | solution.py:268
  123.0 9.1 %all-to-all-done.3.parts_ref = bf16[8,8,64,128]{3,2,1,0:T(8,128)(2,1)S(1)} async-done(((bf16[8,8,64,128]{3,2,1,0:T(8,128)(2,1)}), bf16[8,8,64,128]{3,2,1,0:T(8,128)(2,1)S(1)}, u32[]{:S(2)}, u32[]{:S(2)}) %all-to-all-start.3) | async-done | bytes 1048608 | tf_op jit(solution)/shard_map/all_to_all | solution.py:296
  132.8 3.4 %all-to-all-start.4 = ((bf16[8,64,128]{2,1,0:T(8,128)(2,1)}), bf16[8,64,128]{2,1,0:T(8,128)(2,1)S(1)}, u32[]{:S(2)}, u32[]{:S(2)}) async-start(bf16[8,64,128]{2,1,0:T(8,128)(2,1)} %fold.1), calls=%async_computation.4 | async-start | bytes 262144 | tf_op jit(solution)/shard_map/all_to_all | solution.py:296
  136.2 1.9 %collective-permute-start.12 = (f32[4,8,8,128]{3,2,1,0:T(8,128)S(1)}, f32[4,8,8,128]{3,2,1,0:T(8,128)S(1)}, u32[]{:S(2)}, u32[]{:S(2)}) collective-permute-start(f32[4,8,8,128]{3,2,1,0:T(8,128)S(1)} %pad_maximum_fusion.1.near_ref), channel_id=1, source_target_pairs={{0,1},{1,0},{2,3},{3,2},{4,5},{5,4},{6,7},{7,6},{8,9},{9,8},{10,11... | collective-permute-start | bytes 393224 | tf_op jit(solution)/shard_map/ppermute | solution.py:276
  138.2 1.3 collective-permute-done.12.far_ref
  140.3 4.9 %all-to-all-done.4 = bf16[8,64,128]{2,1,0:T(8,128)(2,1)S(1)} async-done(((bf16[8,64,128]{2,1,0:T(8,128)(2,1)}), bf16[8,64,128]{2,1,0:T(8,128)(2,1)S(1)}, u32[]{:S(2)}, u32[]{:S(2)}) %all-to-all-start.4) | async-done | bytes 131104 | tf_op jit(solution)/shard_map/all_to_all | solution.py:296
  (31 shorter events, 6.3 us)
Async XLA Ops:
  2.5 13.1 %collective-permute-start.3 = (bf16[1072,128]{1,0:T(8,128)(2,1)}, bf16[1072,128]{1,0:T(8,128)(2,1)S(1)}, u32[]{:S(2)}, u32[]{:S(2)}) collective-permute-start(bf16[1072,128]{1,0:T(8,128)(2,1)} %pack.1.q0), channel_id=1, source_target_pairs={{0,6},{2,0},{4,2},{6,4},{1,7},{3,1},{5,3},{7,5},{8,14},{10,8},{12,... | collective-permute-start | bytes 823304 | tf_op jit(solution)/shard_map/ppermute | solution.py:268
  10.3 10.1 %collective-permute-start.2 = (bf16[1072,128]{1,0:T(8,128)(2,1)}, bf16[1072,128]{1,0:T(8,128)(2,1)S(1)}, u32[]{:S(2)}, u32[]{:S(2)}) collective-permute-start(bf16[1072,128]{1,0:T(8,128)(2,1)} %pack.1.q0), channel_id=1, source_target_pairs={{0,4},{2,6},{4,0},{6,2},{1,5},{3,7},{5,1},{7,3},{8,12},{10,14},{12... | collective-permute-start | bytes 823304 | tf_op jit(solution)/shard_map/ppermute | solution.py:268
  12.2 10.3 %collective-permute-start.1 = (bf16[1072,128]{1,0:T(8,128)(2,1)}, bf16[1072,128]{1,0:T(8,128)(2,1)S(1)}, u32[]{:S(2)}, u32[]{:S(2)}) collective-permute-start(bf16[1072,128]{1,0:T(8,128)(2,1)} %pack.1.q0), channel_id=1, source_target_pairs={{0,2},{2,4},{4,6},{6,0},{1,3},{3,5},{5,7},{7,1},{8,10},{10,12},{12... | collective-permute-start | bytes 823304 | tf_op jit(solution)/shard_map/ppermute | solution.py:268
  22.5 36.5 %copy-start.4 = (s32[8,16]{1,0:T(8,128)S(1)}, s32[8,16]{1,0:T(8,128)}, u32[]{:S(2)}) copy-start(s32[8,16]{1,0:T(8,128)} %chosen_ref.1) | copy-start | bytes 1540
  24.6 43.5 %copy-start = (bf16[1072,128]{1,0:T(8,128)(2,1)S(1)}, bf16[1072,128]{1,0:T(8,128)(2,1)}, u32[]{:S(2)}) copy-start(bf16[1072,128]{1,0:T(8,128)(2,1)} %pack.1.q0) | copy-start | bytes 823300
  24.6 43.5 %collective-permute-start.4 = (bf16[4,1072,128]{2,1,0:T(8,128)(2,1)}, bf16[4,1072,128]{2,1,0:T(8,128)(2,1)S(1)}, u32[]{:S(2)}, u32[]{:S(2)}) collective-permute-start(bf16[4,1072,128]{2,1,0:T(8,128)(2,1)} %pad_maximum_fusion), channel_id=1, source_target_pairs={{0,1},{1,0},{2,3},{3,2},{4,5},{5,4},{6,7},{7,6},{8,9},{9,8},{10,11... | collective-permute-start | bytes 3293192 | tf_op jit(solution)/shard_map/ppermute | solution.py:276
  48.0 3.1 %collective-permute-start = (bf16[8,8,128]{2,1,0:T(8,128)(2,1)S(1)}, bf16[8,8,128]{2,1,0:T(8,128)(2,1)S(1)}, u32[]{:S(2)}, u32[]{:S(2)}) collective-permute-start(bf16[8,8,128]{2,1,0:T(8,128)(2,1)S(1)} %slice_bitcast_fusion.4), channel_id=1, source_target_pairs={{0,1},{1,0},{2,3},{3,2},{4,5},{5,4},{6,7},{7,6},{8,9},{9,8},{10,11... | collective-permute-start | bytes 49160 | tf_op jit(solution)/shard_map/ppermute | solution.py:276
  51.9 16.2 %all-to-all-start.1 = ((bf16[8,8,8,128]{3,2,1,0:T(8,128)(2,1)}), bf16[8,8,8,128]{3,2,1,0:T(8,128)(2,1)S(1)}, u32[]{:S(2)}, u32[]{:S(2)}) async-start(bf16[8,8,8,128]{3,2,1,0:T(8,128)(2,1)} %pick.1), calls=%async_computation.1 | async-start | bytes 262144 | tf_op jit(solution)/shard_map/all_to_all | solution.py:296
  68.1 0.8 copy-start.1
  68.9 0.7 copy-start.2
  75.2 3.8 %collective-permute-start.5 = (bf16[4,512,128]{2,1,0:T(8,128)(2,1)S(1)}, bf16[4,512,128]{2,1,0:T(8,128)(2,1)S(1)}, u32[]{:S(2)}, u32[]{:S(2)}) collective-permute-start(bf16[4,512,128]{2,1,0:T(8,128)(2,1)S(1)} %get-tuple-element.17), channel_id=1, source_target_pairs={{0,1},{1,0},{2,3},{3,2},{4,5},{5,4},{6,7},{7,6},{8,9},{9,8},{10,11... | collective-permute-start | bytes 1572872 | tf_op jit(solution)/shard_map/ppermute | solution.py:276
  79.2 15.8 %collective-permute-start.6 = (bf16[512,128]{1,0:T(8,128)(2,1)S(1)}, bf16[512,128]{1,0:T(8,128)(2,1)S(1)}, u32[]{:S(2)}, u32[]{:S(2)}) collective-permute-start(bf16[512,128]{1,0:T(8,128)(2,1)S(1)} %get-tuple-element.24), channel_id=1, source_target_pairs={{2,0},{4,2},{6,4},{0,6},{3,1},{5,3},{7,5},{1,7},{10,8},{12,10},{14... | collective-permute-start | bytes 393224 | tf_op jit(solution)/shard_map/ppermute | solution.py:272
  83.8 11.1 %collective-permute-start.8 = (bf16[512,128]{1,0:T(8,128)(2,1)S(1)}, bf16[512,128]{1,0:T(8,128)(2,1)S(1)}, u32[]{:S(2)}, u32[]{:S(2)}) collective-permute-start(bf16[512,128]{1,0:T(8,128)(2,1)S(1)} %get-tuple-element.25), channel_id=1, source_target_pairs={{6,0},{0,2},{2,4},{4,6},{7,1},{1,3},{3,5},{5,7},{14,8},{8,10},{10,... | collective-permute-start | bytes 393224 | tf_op jit(solution)/shard_map/ppermute | solution.py:272
  85.7 9.2 %collective-permute-start.7 = (bf16[512,128]{1,0:T(8,128)(2,1)S(1)}, bf16[512,128]{1,0:T(8,128)(2,1)S(1)}, u32[]{:S(2)}, u32[]{:S(2)}) collective-permute-start(bf16[512,128]{1,0:T(8,128)(2,1)S(1)} %get-tuple-element.26), channel_id=1, source_target_pairs={{4,0},{6,2},{0,4},{2,6},{5,1},{7,3},{1,5},{3,7},{12,8},{14,10},{8,... | collective-permute-start | bytes 393224 | tf_op jit(solution)/shard_map/ppermute | solution.py:272
  90.3 19.3 %all-to-all-start.2 = ((bf16[64,16,128]{2,1,0:T(8,128)(2,1)}), bf16[64,16,128]{2,1,0:T(8,128)(2,1)S(1)}, u32[]{:S(2)}, u32[]{:S(2)}) async-start(bf16[64,16,128]{2,1,0:T(8,128)(2,1)} %get-tuple-element.19), calls=%async_computation.2 | async-start | bytes 524288 | tf_op jit(solution)/shard_map/all_to_all | solution.py:302
  95.0 3.0 %copy-start.3 = (bf16[512,128]{1,0:T(8,128)(2,1)}, bf16[512,128]{1,0:T(8,128)(2,1)S(1)}, u32[]{:S(2)}) copy-start(bf16[512,128]{1,0:T(8,128)(2,1)S(1)} %fusion.3) | copy-start | bytes 393220
  109.6 22.4 %all-to-all-start.3 = ((bf16[8,8,64,128]{3,2,1,0:T(8,128)(2,1)}), bf16[8,8,64,128]{3,2,1,0:T(8,128)(2,1)S(1)}, u32[]{:S(2)}, u32[]{:S(2)}) async-start(bf16[8,8,64,128]{3,2,1,0:T(8,128)(2,1)} %bitcast.21), calls=%async_computation.3 | async-start | bytes 2097152 | tf_op jit(solution)/shard_map/all_to_all | solution.py:296
  113.4 22.8 %collective-permute-start.11 = (f32[8,8,128]{2,1,0:T(8,128)S(1)}, f32[8,8,128]{2,1,0:T(8,128)S(1)}, u32[]{:S(2)}, u32[]{:S(2)}) collective-permute-start(f32[8,8,128]{2,1,0:T(8,128)S(1)} %settle.1), channel_id=1, source_target_pairs={{0,6},{2,0},{4,2},{6,4},{1,7},{3,1},{5,3},{7,5},{8,14},{10,8},{12,... | collective-permute-start | bytes 98312 | tf_op jit(solution)/shard_map/ppermute | solution.py:268
  115.5 20.7 %collective-permute-start.10 = (f32[8,8,128]{2,1,0:T(8,128)S(1)}, f32[8,8,128]{2,1,0:T(8,128)S(1)}, u32[]{:S(2)}, u32[]{:S(2)}) collective-permute-start(f32[8,8,128]{2,1,0:T(8,128)S(1)} %settle.1), channel_id=1, source_target_pairs={{0,4},{2,6},{4,0},{6,2},{1,5},{3,7},{5,1},{7,3},{8,12},{10,14},{12... | collective-permute-start | bytes 98312 | tf_op jit(solution)/shard_map/ppermute | solution.py:268
  119.5 16.7 %collective-permute-start.9 = (f32[8,8,128]{2,1,0:T(8,128)S(1)}, f32[8,8,128]{2,1,0:T(8,128)S(1)}, u32[]{:S(2)}, u32[]{:S(2)}) collective-permute-start(f32[8,8,128]{2,1,0:T(8,128)S(1)} %settle.1), channel_id=1, source_target_pairs={{0,2},{2,4},{4,6},{6,0},{1,3},{3,5},{5,7},{7,1},{8,10},{10,12},{12... | collective-permute-start | bytes 98312 | tf_op jit(solution)/shard_map/ppermute | solution.py:268
  132.8 12.4 %all-to-all-start.4 = ((bf16[8,64,128]{2,1,0:T(8,128)(2,1)}), bf16[8,64,128]{2,1,0:T(8,128)(2,1)S(1)}, u32[]{:S(2)}, u32[]{:S(2)}) async-start(bf16[8,64,128]{2,1,0:T(8,128)(2,1)} %fold.1), calls=%async_computation.4 | async-start | bytes 262144 | tf_op jit(solution)/shard_map/all_to_all | solution.py:296
  136.2 3.2 %collective-permute-start.12 = (f32[4,8,8,128]{3,2,1,0:T(8,128)S(1)}, f32[4,8,8,128]{3,2,1,0:T(8,128)S(1)}, u32[]{:S(2)}, u32[]{:S(2)}) collective-permute-start(f32[4,8,8,128]{3,2,1,0:T(8,128)S(1)} %pad_maximum_fusion.1.near_ref), channel_id=1, source_target_pairs={{0,1},{1,0},{2,3},{3,2},{4,5},{5,4},{6,7},{7,6},{8,9},{9,8},{10,11... | collective-permute-start | bytes 393224 | tf_op jit(solution)/shard_map/ppermute | solution.py:276

commit v8 on v5

--- a/solution.py
+++ b/solution.py
@@ -16,6 +16,7 @@
 TOK = 512
 LANES = 128
 SCALE = 0.125
+LOG2E = 1.4426950408889634
 KV = ("z", "y")
 ALL = ("z", "y", "x", "c")
 FAR = 1 << 20
@@ -134,7 +135,9 @@
         for n in range(3):
             at = 2 * TOK + 16 * n
             parts.append((near[p][at : at + 16, :] if p < 4 else qp_ref[p - 4, at : at + 16, :]).astype(F32))
-        return parts[0] + parts[1] + parts[2]
+        total = parts[0] + parts[1] + parts[2]
+        kind = lax.broadcasted_iota(jnp.int32, total.shape, 0) & 3
+        return total * jnp.where(kind < 2, LOG2E, SCALE)
 
     for pair in range(4):
         even, odd = stat(2 * pair), stat(2 * pair + 1)
@@ -149,8 +152,10 @@
     def one_block(j, carry):
         kv = jnp.concatenate([table[slot_ref[j, s]] for s in range(SLOTS)], axis=0)
         turned = pltpu.roll(kv, LANES // 2, 1)
+        scaled = turned * SCALE
+        kept = kv * SCALE
         k2 = jnp.concatenate([jnp.where(low, kv, 0.0), jnp.where(low, 0.0, turned)], axis=0).astype(BF16)
-        v2 = jnp.concatenate([jnp.where(low, turned, 0.0), jnp.where(low, 0.0, kv)], axis=0).astype(BF16)
+        v2 = jnp.concatenate([jnp.where(low, scaled, 0.0), jnp.where(low, 0.0, kept)], axis=0).astype(BF16)
         at = pl.multiple_of(j * BLOCK, BLOCK)
         q = jnp.concatenate(
             [r[pl.ds(at, BLOCK), :] for r in near]
@@ -174,9 +179,9 @@
         for h in range(2):
             s = scores[h * LANES : (h + 1) * LANES]
             d = dprobs[h * LANES : (h + 1) * LANES]
-            p = jnp.where(seen, jnp.exp(s * SCALE - stat_j[h : h + 1, :]), 0.0)
+            p = jnp.where(seen, jnp.exp2(s * (SCALE * LOG2E) - stat_j[h : h + 1, :]), 0.0)
             probs.append(p.astype(BF16))
-            dscores.append((p * (d - stat_j[2 + h : 3 + h, :]) * SCALE).astype(BF16))
+            dscores.append((p * (d - stat_j[2 + h : 3 + h, :])).astype(BF16))
         probs = jnp.concatenate(probs, axis=0)
         dscores = jnp.concatenate(dscores, axis=0)
         plain = (((1,), (0,)), ((), ()))
@@ -193,7 +198,12 @@
             acc[home_ref[j, s]] += both[s * ROWS : (s + 1) * ROWS]
         return carry
 
-    lax.fori_loop(0, BLOCKS, one_block, 0)
+    def some_blocks(i, carry):
+        for n in range(4):
+            one_block(i * 4 + n, carry)
+        return carry
+
+    lax.fori_loop(0, BLOCKS // 4, some_blocks, 0)
     away_ref[:, :ROWS] = acc[:PEERS].astype(BF16)
     for s in range(PEERS):
         want = jnp.broadcast_to(want_ref[s : s + 1, :], (ROWS, LANES))

time: 145 us -> 143 us (0.986)
  Pallas kernels: 12.4 us -> 10.7 us
    pallas_call x6, Pallas kernels: 12.4 us -> 10.7 us  [call(): pl.pallas_call(kernel, in_specs=ins, out_specs=[VMEM] * len(out_shape) if...]
where the time goes in v8:
time: 143 us; the launch traced here: 142 us
  starting transfers between devices  57.9 us (40%)
  waiting for transfers between devices  45.1 us (32%)
  blocking collectives  19.6 us (14%)
  Pallas kernels  10.7 us (7%)
  matrix products  2.98 us (2%)
  local copies, waits for them, and re-layouts  2.84 us (2%)
  other arithmetic  2.18 us (2%)
    ppermute x6, starting transfers between devices, x_from(): return lax.ppermute(arr, 'x', [(i, (i + k) % 4) for i in range(4)])  22.6 us
    all_to_all x2, waiting for transfers between devices, exchange(): return lax.all_to_all(arr, KV, split_axis=0, concat_axis=0, tiled=True)  22.6 us
    all_to_all x1, blocking collectives, along(): lax.all_to_all(arr, ALL, split_axis=0, concat_axis=0, tiled=True, axis_in...  19.6 us
    ppermute x3, starting transfers between devices, x_back(): return lax.ppermute(arr, 'x', [((i + k) % 4, i) for i in range(4)])  11.1 us
    pallas_call x6, Pallas kernels, call(): pl.pallas_call(kernel, in_specs=ins, out_specs=[VMEM] * len(out_shape) if...  10.7 us
    all_to_all x2, starting transfers between devices, exchange(): return lax.all_to_all(arr, KV, split_axis=0, concat_axis=0, tiled=True)  9.27 us
    ppermute x6, waiting for transfers between devices, x_from(): return lax.ppermute(arr, 'x', [(i, (i + k) % 4) for i in range(4)])  9.24 us
    all_to_all x1, waiting for transfers between devices, along(): lax.all_to_all(arr, ALL, split_axis=0, concat_axis=0, tiled=True, axis_in...  8.98 us
  transfers between devices with their start and end apart: 16, of which 9 were waited for; matrix products, arithmetic and copies ran while one was open for 3% of the time, Pallas kernels for 3%

profile of v8, /device:TPU:2, one launch (start us, length us, event | category | flops | bytes accessed | tf_op | source)
XLA Modules:
  0.0 142.2 jit_solution(3404314634682919781)
XLA Ops:
  0.6 1.9 %pack.1.q0 = bf16[1072,128]{1,0:T(8,128)(2,1)} custom-call(bf16[512,128]{1,0:T(8,128)(2,1)} %q_ref.1, bf16[512,128]{1,0:T(8,128)(2,1)} %g_ref.1, bf16[512,128]{1,0:T(8,128)(2,1)} %o_ref.1, f32[2,512]{1,0:T(2,128)} %bitcast.50), custom_call_target="tpu_custom_call" | custom-call | flops 262144 | bytes 1048576 | tf_op jit(solution)/shard_map/pack/pallas_call | solution.py:230
  2.5 7.8 %collective-permute-start.3 = (bf16[1072,128]{1,0:T(8,128)(2,1)}, bf16[1072,128]{1,0:T(8,128)(2,1)S(1)}, u32[]{:S(2)}, u32[]{:S(2)}) collective-permute-start(bf16[1072,128]{1,0:T(8,128)(2,1)} %pack.1.q0), channel_id=1, source_target_pairs={{0,6},{2,0},{4,2},{6,4},{1,7},{3,1},{5,3},{7,5},{8,14},{10,8},{12,... | collective-permute-start | bytes 823304 | tf_op jit(solution)/shard_map/ppermute | solution.py:250
  10.3 1.9 %collective-permute-start.2 = (bf16[1072,128]{1,0:T(8,128)(2,1)}, bf16[1072,128]{1,0:T(8,128)(2,1)S(1)}, u32[]{:S(2)}, u32[]{:S(2)}) collective-permute-start(bf16[1072,128]{1,0:T(8,128)(2,1)} %pack.1.q0), channel_id=1, source_target_pairs={{0,4},{2,6},{4,0},{6,2},{1,5},{3,7},{5,1},{7,3},{8,12},{10,14},{12... | collective-permute-start | bytes 823304 | tf_op jit(solution)/shard_map/ppermute | solution.py:250
  12.2 3.4 %collective-permute-start.1 = (bf16[1072,128]{1,0:T(8,128)(2,1)}, bf16[1072,128]{1,0:T(8,128)(2,1)S(1)}, u32[]{:S(2)}, u32[]{:S(2)}) collective-permute-start(bf16[1072,128]{1,0:T(8,128)(2,1)} %pack.1.q0), channel_id=1, source_target_pairs={{0,2},{2,4},{4,6},{6,0},{1,3},{3,5},{5,7},{7,1},{8,10},{10,12},{12... | collective-permute-start | bytes 823304 | tf_op jit(solution)/shard_map/ppermute | solution.py:250
  15.6 4.8 %collective-permute-done.2.q2 = bf16[1072,128]{1,0:T(8,128)(2,1)S(1)} collective-permute-done((bf16[1072,128]{1,0:T(8,128)(2,1)}, bf16[1072,128]{1,0:T(8,128)(2,1)S(1)}, u32[]{:S(2)}, u32[]{:S(2)}) %collective-permute-start.2) | collective-permute-done | bytes 274464 | tf_op jit(solution)/shard_map/ppermute | solution.py:250
  20.4 2.1 %collective-permute-done.1.q1 = bf16[1072,128]{1,0:T(8,128)(2,1)S(1)} collective-permute-done((bf16[1072,128]{1,0:T(8,128)(2,1)}, bf16[1072,128]{1,0:T(8,128)(2,1)S(1)}, u32[]{:S(2)}, u32[]{:S(2)}) %collective-permute-start.1) | collective-permute-done | bytes 274464 | tf_op jit(solution)/shard_map/ppermute | solution.py:250
  22.5 1.1 pad_maximum_fusion
  23.6 2.1 %collective-permute-start.4 = (bf16[4,1072,128]{2,1,0:T(8,128)(2,1)S(1)}, bf16[4,1072,128]{2,1,0:T(8,128)(2,1)S(1)}, u32[]{:S(2)}, u32[]{:S(2)}) collective-permute-start(bf16[4,1072,128]{2,1,0:T(8,128)(2,1)S(1)} %pad_maximum_fusion), channel_id=1, source_target_pairs={{0,1},{1,0},{2,3},{3,2},{4,5},{5,4},{6,7},{7,6},{8,9},{9,8},{10,11... | collective-permute-start | bytes 3293192 | tf_op jit(solution)/shard_map/ppermute | solution.py:258
  25.7 1.8 %offer.1 = (bf16[8,9,8,128]{3,2,1,0:T(8,128)(2,1)}, bf16[8,8,128]{2,1,0:T(8,128)(2,1)}, f32[64,128]{1,0:T(8,128)}) custom-call(s32[1]{0:T(128)} %bitcast.rank_ref, s32[1]{0:T(128)} %bitcast.1.tp_ref, bf16[64,512]{1,0:T(8,128)(2,1)} %bitcast.45, bf16[64,512]{1,0:T(8,128)(2,1)} %bitcast.46, s32[8,16]{1,0:T(8,128)} %chosen_ref.1), custom_call_target="tpu_custom_call" | custom-call | flops 262144 | bytes 1048576 | tf_op jit(solution)/shard_map/offer/pallas_call | solution.py:230
  27.5 19.6 %all_to_all.20.pushed_ref = bf16[8,9,8,128]{3,2,1,0:T(8,128)(2,1)S(1)} all-to-all(bf16[8,9,8,128]{3,2,1,0:T(8,128)(2,1)} %get-tuple-element.13), channel_id=1, replica_groups={{0,64,128,192,256,320,384,448},{8,72,136,200,264,328,392,456},{16,80,14..., dimensions={0} | all-to-all | bytes 294912 | tf_op jit(solution)/shard_map/all_to_all | solution.py:278
  47.1 1.9 %collective-permute-start = (bf16[8,8,128]{2,1,0:T(8,128)(2,1)S(1)}, bf16[8,8,128]{2,1,0:T(8,128)(2,1)S(1)}, u32[]{:S(2)}, u32[]{:S(2)}) collective-permute-start(bf16[8,8,128]{2,1,0:T(8,128)(2,1)S(1)} %slice_bitcast_fusion.4), channel_id=1, source_target_pairs={{0,1},{1,0},{2,3},{3,2},{4,5},{5,4},{6,7},{7,6},{8,9},{9,8},{10,11... | collective-permute-start | bytes 49160 | tf_op jit(solution)/shard_map/ppermute | solution.py:258
  49.0 1.1 collective-permute-done.wants_ref
  51.0 7.1 %all-to-all-start.1 = ((bf16[8,8,8,128]{3,2,1,0:T(8,128)(2,1)}), bf16[8,8,8,128]{3,2,1,0:T(8,128)(2,1)S(1)}, u32[]{:S(2)}, u32[]{:S(2)}) async-start(bf16[8,8,8,128]{3,2,1,0:T(8,128)(2,1)} %pick.1), calls=%async_computation.1 | async-start | bytes 262144 | tf_op jit(solution)/shard_map/all_to_all | solution.py:278
  58.2 9.0 %all-to-all-done.1 = bf16[8,8,8,128]{3,2,1,0:T(8,128)(2,1)S(1)} async-done(((bf16[8,8,8,128]{3,2,1,0:T(8,128)(2,1)}), bf16[8,8,8,128]{3,2,1,0:T(8,128)(2,1)S(1)}, u32[]{:S(2)}, u32[]{:S(2)}) %all-to-all-start.1) | async-done | bytes 131104 | tf_op jit(solution)/shard_map/all_to_all | solution.py:278
  68.6 5.1 %attend.1 = (bf16[64,16,128]{2,1,0:T(8,128)(2,1)}, f32[8,8,128]{2,1,0:T(8,128)S(1)}, f32[4,512,128]{2,1,0:T(8,128)S(1)}, bf16[4,512,128]{2,1,0:T(8,128)(2,1)S(1)}) custom-call(s32[8,16]{1,0:T(8,128)S(1)} %get-tuple-element.28.slot_ref, s32[8,16]{1,0:T(8,128)S(1)} %get-tuple-element.29.home_ref, s32[8,16]{1,0:T(8,128)S(1)} %get-tuple-element.27.rel_ref, ...), custom_call_target="tpu_custom_call" | custom-call | flops 1073741824 | bytes 1048576 | tf_op jit(solution)/shard_map/attend/pallas_call | solution.py:230
  73.7 1.9 %collective-permute-start.5 = (bf16[4,512,128]{2,1,0:T(8,128)(2,1)S(1)}, bf16[4,512,128]{2,1,0:T(8,128)(2,1)S(1)}, u32[]{:S(2)}, u32[]{:S(2)}) collective-permute-start(bf16[4,512,128]{2,1,0:T(8,128)(2,1)S(1)} %get-tuple-element.17), channel_id=1, source_target_pairs={{0,1},{1,0},{2,3},{3,2},{4,5},{5,4},{6,7},{7,6},{8,9},{9,8},{10,11... | collective-permute-start | bytes 1572872 | tf_op jit(solution)/shard_map/ppermute | solution.py:258
  75.7 1.9 %collective-permute-done.5 = bf16[4,512,128]{2,1,0:T(8,128)(2,1)S(1)} collective-permute-done((bf16[4,512,128]{2,1,0:T(8,128)(2,1)S(1)}, bf16[4,512,128]{2,1,0:T(8,128)(2,1)S(1)}, u32[]{:S(2)}, u32[]{:S(2)}) %collective-permute-start.5) | collective-permute-done | bytes 524320 | tf_op jit(solution)/shard_map/ppermute | solution.py:258
  77.7 4.6 %collective-permute-start.6 = (bf16[512,128]{1,0:T(8,128)(2,1)S(1)}, bf16[512,128]{1,0:T(8,128)(2,1)S(1)}, u32[]{:S(2)}, u32[]{:S(2)}) collective-permute-start(bf16[512,128]{1,0:T(8,128)(2,1)S(1)} %get-tuple-element.24), channel_id=1, source_target_pairs={{2,0},{4,2},{6,4},{0,6},{3,1},{5,3},{7,5},{1,7},{10,8},{12,10},{14... | collective-permute-start | bytes 393224 | tf_op jit(solution)/shard_map/ppermute | solution.py:254
  82.3 1.9 %collective-permute-start.8 = (bf16[512,128]{1,0:T(8,128)(2,1)S(1)}, bf16[512,128]{1,0:T(8,128)(2,1)S(1)}, u32[]{:S(2)}, u32[]{:S(2)}) collective-permute-start(bf16[512,128]{1,0:T(8,128)(2,1)S(1)} %get-tuple-element.25), channel_id=1, source_target_pairs={{6,0},{0,2},{2,4},{4,6},{7,1},{1,3},{3,5},{5,7},{14,8},{8,10},{10,... | collective-permute-start | bytes 393224 | tf_op jit(solution)/shard_map/ppermute | solution.py:254
  84.3 4.6 %collective-permute-start.7 = (bf16[512,128]{1,0:T(8,128)(2,1)S(1)}, bf16[512,128]{1,0:T(8,128)(2,1)S(1)}, u32[]{:S(2)}, u32[]{:S(2)}) collective-permute-start(bf16[512,128]{1,0:T(8,128)(2,1)S(1)} %get-tuple-element.26), channel_id=1, source_target_pairs={{4,0},{6,2},{0,4},{2,6},{5,1},{7,3},{1,5},{3,7},{12,8},{14,10},{8,... | collective-permute-start | bytes 393224 | tf_op jit(solution)/shard_map/ppermute | solution.py:254
  88.8 4.6 %all-to-all-start.2 = ((bf16[64,16,128]{2,1,0:T(8,128)(2,1)}), bf16[64,16,128]{2,1,0:T(8,128)(2,1)S(1)}, u32[]{:S(2)}, u32[]{:S(2)}) async-start(bf16[64,16,128]{2,1,0:T(8,128)(2,1)} %get-tuple-element.19), calls=%async_computation.2 | async-start | bytes 524288 | tf_op jit(solution)/shard_map/all_to_all | solution.py:284
  93.6 3.0 %fusion = bf16[4096,128]{0,1:T(8,128)(2,1)S(1)} fusion(bf16[512,128]{1,0:T(8,128)(2,1)S(1)} %fusion.4, bf16[512,4096]{1,0:T(8,128)(2,1)} %param.8), kind=kOutput, calls=%fused_computation.1 | convolution fusion | flops 537395200 | bytes 5373952 | tf_op jit(solution)/shard_map/dot_general | solution.py:368
  96.6 1.3 copy.12
  97.9 10.2 %all-to-all-done.2.given_ref = bf16[64,16,128]{2,1,0:T(8,128)(2,1)S(1)} async-done(((bf16[64,16,128]{2,1,0:T(8,128)(2,1)}), bf16[64,16,128]{2,1,0:T(8,128)(2,1)S(1)}, u32[]{:S(2)}, u32[]{:S(2)}) %all-to-all-start.2) | async-done | bytes 262176 | tf_op jit(solution)/shard_map/all_to_all | solution.py:284
  108.1 4.7 %all-to-all-start.3 = ((bf16[64,64,128]{2,1,0:T(8,128)(2,1)}), bf16[64,64,128]{2,1,0:T(8,128)(2,1)S(1)}, u32[]{:S(2)}, u32[]{:S(2)}) async-start(bf16[64,64,128]{2,1,0:T(8,128)(2,1)} %bitcast.22), calls=%async_computation.3 | async-start | bytes 2097152 | tf_op jit(solution)/shard_map/all_to_all | solution.py:284
  113.1 2.1 %collective-permute-start.11 = (f32[8,8,128]{2,1,0:T(8,128)S(1)}, f32[8,8,128]{2,1,0:T(8,128)S(1)}, u32[]{:S(2)}, u32[]{:S(2)}) collective-permute-start(f32[8,8,128]{2,1,0:T(8,128)S(1)} %settle.1), channel_id=1, source_target_pairs={{0,6},{2,0},{4,2},{6,4},{1,7},{3,1},{5,3},{7,5},{8,14},{10,8},{12,... | collective-permute-start | bytes 98312 | tf_op jit(solution)/shard_map/ppermute | solution.py:250
  115.1 4.0 %collective-permute-start.10 = (f32[8,8,128]{2,1,0:T(8,128)S(1)}, f32[8,8,128]{2,1,0:T(8,128)S(1)}, u32[]{:S(2)}, u32[]{:S(2)}) collective-permute-start(f32[8,8,128]{2,1,0:T(8,128)S(1)} %settle.1), channel_id=1, source_target_pairs={{0,4},{2,6},{4,0},{6,2},{1,5},{3,7},{5,1},{7,3},{8,12},{10,14},{12... | collective-permute-start | bytes 98312 | tf_op jit(solution)/shard_map/ppermute | solution.py:250
  119.2 3.4 %collective-permute-start.9 = (f32[8,8,128]{2,1,0:T(8,128)S(1)}, f32[8,8,128]{2,1,0:T(8,128)S(1)}, u32[]{:S(2)}, u32[]{:S(2)}) collective-permute-start(f32[8,8,128]{2,1,0:T(8,128)S(1)} %settle.1), channel_id=1, source_target_pairs={{0,2},{2,4},{4,6},{6,0},{1,3},{3,5},{5,7},{7,1},{8,10},{10,12},{12... | collective-permute-start | bytes 98312 | tf_op jit(solution)/shard_map/ppermute | solution.py:250
  122.6 2.3 %collective-permute-done.9 = f32[8,8,128]{2,1,0:T(8,128)S(1)} collective-permute-done((f32[8,8,128]{2,1,0:T(8,128)S(1)}, f32[8,8,128]{2,1,0:T(8,128)S(1)}, u32[]{:S(2)}, u32[]{:S(2)}) %collective-permute-start.9) | collective-permute-done | bytes 32800 | tf_op jit(solution)/shard_map/ppermute | solution.py:250
  125.0 1.9 %collective-permute-start.12 = (f32[4,8,8,128]{3,2,1,0:T(8,128)S(1)}, f32[4,8,8,128]{3,2,1,0:T(8,128)S(1)}, u32[]{:S(2)}, u32[]{:S(2)}) collective-permute-start(f32[4,8,8,128]{3,2,1,0:T(8,128)S(1)} %pad_maximum_fusion.1.near_ref), channel_id=1, source_target_pairs={{0,1},{1,0},{2,3},{3,2},{4,5},{5,4},{6,7},{7,6},{8,9},{9,8},{10,11... | collective-permute-start | bytes 393224 | tf_op jit(solution)/shard_map/ppermute | solution.py:258
  126.9 1.3 collective-permute-done.12.far_ref
  129.0 12.3 %all-to-all-done.3 = bf16[64,64,128]{2,1,0:T(8,128)(2,1)S(1)} async-done(((bf16[64,64,128]{2,1,0:T(8,128)(2,1)}), bf16[64,64,128]{2,1,0:T(8,128)(2,1)S(1)}, u32[]{:S(2)}, u32[]{:S(2)}) %all-to-all-start.3) | async-done | bytes 1048608 | tf_op jit(solution)/shard_map/all_to_all | solution.py:284
  (28 shorter events, 4.5 us)
Async XLA Ops:
  2.5 13.1 %collective-permute-start.3 = (bf16[1072,128]{1,0:T(8,128)(2,1)}, bf16[1072,128]{1,0:T(8,128)(2,1)S(1)}, u32[]{:S(2)}, u32[]{:S(2)}) collective-permute-start(bf16[1072,128]{1,0:T(8,128)(2,1)} %pack.1.q0), channel_id=1, source_target_pairs={{0,6},{2,0},{4,2},{6,4},{1,7},{3,1},{5,3},{7,5},{8,14},{10,8},{12,... | collective-permute-start | bytes 823304 | tf_op jit(solution)/shard_map/ppermute | solution.py:250
  10.3 10.1 %collective-permute-start.2 = (bf16[1072,128]{1,0:T(8,128)(2,1)}, bf16[1072,128]{1,0:T(8,128)(2,1)S(1)}, u32[]{:S(2)}, u32[]{:S(2)}) collective-permute-start(bf16[1072,128]{1,0:T(8,128)(2,1)} %pack.1.q0), channel_id=1, source_target_pairs={{0,4},{2,6},{4,0},{6,2},{1,5},{3,7},{5,1},{7,3},{8,12},{10,14},{12... | collective-permute-start | bytes 823304 | tf_op jit(solution)/shard_map/ppermute | solution.py:250
  12.2 10.3 %collective-permute-start.1 = (bf16[1072,128]{1,0:T(8,128)(2,1)}, bf16[1072,128]{1,0:T(8,128)(2,1)S(1)}, u32[]{:S(2)}, u32[]{:S(2)}) collective-permute-start(bf16[1072,128]{1,0:T(8,128)(2,1)} %pack.1.q0), channel_id=1, source_target_pairs={{0,2},{2,4},{4,6},{6,0},{1,3},{3,5},{5,7},{7,1},{8,10},{10,12},{12... | collective-permute-start | bytes 823304 | tf_op jit(solution)/shard_map/ppermute | solution.py:250
  22.5 35.6 %copy-start.4 = (s32[8,16]{1,0:T(8,128)S(1)}, s32[8,16]{1,0:T(8,128)}, u32[]{:S(2)}) copy-start(s32[8,16]{1,0:T(8,128)} %chosen_ref.1) | copy-start | bytes 1540
  23.6 43.5 %copy-start = (bf16[1072,128]{1,0:T(8,128)(2,1)S(1)}, bf16[1072,128]{1,0:T(8,128)(2,1)}, u32[]{:S(2)}) copy-start(bf16[1072,128]{1,0:T(8,128)(2,1)} %pack.1.q0) | copy-start | bytes 823300
  23.6 43.5 %collective-permute-start.4 = (bf16[4,1072,128]{2,1,0:T(8,128)(2,1)S(1)}, bf16[4,1072,128]{2,1,0:T(8,128)(2,1)S(1)}, u32[]{:S(2)}, u32[]{:S(2)}) collective-permute-start(bf16[4,1072,128]{2,1,0:T(8,128)(2,1)S(1)} %pad_maximum_fusion), channel_id=1, source_target_pairs={{0,1},{1,0},{2,3},{3,2},{4,5},{5,4},{6,7},{7,6},{8,9},{9,8},{10,11... | collective-permute-start | bytes 3293192 | tf_op jit(solution)/shard_map/ppermute | solution.py:258
  47.1 3.1 %collective-permute-start = (bf16[8,8,128]{2,1,0:T(8,128)(2,1)S(1)}, bf16[8,8,128]{2,1,0:T(8,128)(2,1)S(1)}, u32[]{:S(2)}, u32[]{:S(2)}) collective-permute-start(bf16[8,8,128]{2,1,0:T(8,128)(2,1)S(1)} %slice_bitcast_fusion.4), channel_id=1, source_target_pairs={{0,1},{1,0},{2,3},{3,2},{4,5},{5,4},{6,7},{7,6},{8,9},{9,8},{10,11... | collective-permute-start | bytes 49160 | tf_op jit(solution)/shard_map/ppermute | solution.py:258
  51.0 16.2 %all-to-all-start.1 = ((bf16[8,8,8,128]{3,2,1,0:T(8,128)(2,1)}), bf16[8,8,8,128]{3,2,1,0:T(8,128)(2,1)S(1)}, u32[]{:S(2)}, u32[]{:S(2)}) async-start(bf16[8,8,8,128]{3,2,1,0:T(8,128)(2,1)} %pick.1), calls=%async_computation.1 | async-start | bytes 262144 | tf_op jit(solution)/shard_map/all_to_all | solution.py:278
  67.1 0.8 copy-start.1
  67.9 0.7 copy-start.2
  73.7 3.8 %collective-permute-start.5 = (bf16[4,512,128]{2,1,0:T(8,128)(2,1)S(1)}, bf16[4,512,128]{2,1,0:T(8,128)(2,1)S(1)}, u32[]{:S(2)}, u32[]{:S(2)}) collective-permute-start(bf16[4,512,128]{2,1,0:T(8,128)(2,1)S(1)} %get-tuple-element.17), channel_id=1, source_target_pairs={{0,1},{1,0},{2,3},{3,2},{4,5},{5,4},{6,7},{7,6},{8,9},{9,8},{10,11... | collective-permute-start | bytes 1572872 | tf_op jit(solution)/shard_map/ppermute | solution.py:258
  77.7 15.8 %collective-permute-start.6 = (bf16[512,128]{1,0:T(8,128)(2,1)S(1)}, bf16[512,128]{1,0:T(8,128)(2,1)S(1)}, u32[]{:S(2)}, u32[]{:S(2)}) collective-permute-start(bf16[512,128]{1,0:T(8,128)(2,1)S(1)} %get-tuple-element.24), channel_id=1, source_target_pairs={{2,0},{4,2},{6,4},{0,6},{3,1},{5,3},{7,5},{1,7},{10,8},{12,10},{14... | collective-permute-start | bytes 393224 | tf_op jit(solution)/shard_map/ppermute | solution.py:254
  82.3 11.1 %collective-permute-start.8 = (bf16[512,128]{1,0:T(8,128)(2,1)S(1)}, bf16[512,128]{1,0:T(8,128)(2,1)S(1)}, u32[]{:S(2)}, u32[]{:S(2)}) collective-permute-start(bf16[512,128]{1,0:T(8,128)(2,1)S(1)} %get-tuple-element.25), channel_id=1, source_target_pairs={{6,0},{0,2},{2,4},{4,6},{7,1},{1,3},{3,5},{5,7},{14,8},{8,10},{10,... | collective-permute-start | bytes 393224 | tf_op jit(solution)/shard_map/ppermute | solution.py:254
  84.3 9.2 %collective-permute-start.7 = (bf16[512,128]{1,0:T(8,128)(2,1)S(1)}, bf16[512,128]{1,0:T(8,128)(2,1)S(1)}, u32[]{:S(2)}, u32[]{:S(2)}) collective-permute-start(bf16[512,128]{1,0:T(8,128)(2,1)S(1)} %get-tuple-element.26), channel_id=1, source_target_pairs={{4,0},{6,2},{0,4},{2,6},{5,1},{7,3},{1,5},{3,7},{12,8},{14,10},{8,... | collective-permute-start | bytes 393224 | tf_op jit(solution)/shard_map/ppermute | solution.py:254
  88.8 19.3 %all-to-all-start.2 = ((bf16[64,16,128]{2,1,0:T(8,128)(2,1)}), bf16[64,16,128]{2,1,0:T(8,128)(2,1)S(1)}, u32[]{:S(2)}, u32[]{:S(2)}) async-start(bf16[64,16,128]{2,1,0:T(8,128)(2,1)} %get-tuple-element.19), calls=%async_computation.2 | async-start | bytes 524288 | tf_op jit(solution)/shard_map/all_to_all | solution.py:284
  93.6 3.0 %copy-start.3 = (bf16[512,128]{1,0:T(8,128)(2,1)}, bf16[512,128]{1,0:T(8,128)(2,1)S(1)}, u32[]{:S(2)}) copy-start(bf16[512,128]{1,0:T(8,128)(2,1)S(1)} %fusion.4) | copy-start | bytes 393220
  108.1 33.3 %all-to-all-start.3 = ((bf16[64,64,128]{2,1,0:T(8,128)(2,1)}), bf16[64,64,128]{2,1,0:T(8,128)(2,1)S(1)}, u32[]{:S(2)}, u32[]{:S(2)}) async-start(bf16[64,64,128]{2,1,0:T(8,128)(2,1)} %bitcast.22), calls=%async_computation.3 | async-start | bytes 2097152 | tf_op jit(solution)/shard_map/all_to_all | solution.py:284
  113.1 9.6 %collective-permute-start.11 = (f32[8,8,128]{2,1,0:T(8,128)S(1)}, f32[8,8,128]{2,1,0:T(8,128)S(1)}, u32[]{:S(2)}, u32[]{:S(2)}) collective-permute-start(f32[8,8,128]{2,1,0:T(8,128)S(1)} %settle.1), channel_id=1, source_target_pairs={{0,6},{2,0},{4,2},{6,4},{1,7},{3,1},{5,3},{7,5},{8,14},{10,8},{12,... | collective-permute-start | bytes 98312 | tf_op jit(solution)/shard_map/ppermute | solution.py:250
  115.1 7.5 %collective-permute-start.10 = (f32[8,8,128]{2,1,0:T(8,128)S(1)}, f32[8,8,128]{2,1,0:T(8,128)S(1)}, u32[]{:S(2)}, u32[]{:S(2)}) collective-permute-start(f32[8,8,128]{2,1,0:T(8,128)S(1)} %settle.1), channel_id=1, source_target_pairs={{0,4},{2,6},{4,0},{6,2},{1,5},{3,7},{5,1},{7,3},{8,12},{10,14},{12... | collective-permute-start | bytes 98312 | tf_op jit(solution)/shard_map/ppermute | solution.py:250
  119.2 5.8 %collective-permute-start.9 = (f32[8,8,128]{2,1,0:T(8,128)S(1)}, f32[8,8,128]{2,1,0:T(8,128)S(1)}, u32[]{:S(2)}, u32[]{:S(2)}) collective-permute-start(f32[8,8,128]{2,1,0:T(8,128)S(1)} %settle.1), channel_id=1, source_target_pairs={{0,2},{2,4},{4,6},{6,0},{1,3},{3,5},{5,7},{7,1},{8,10},{10,12},{12... | collective-permute-start | bytes 98312 | tf_op jit(solution)/shard_map/ppermute | solution.py:250
  125.0 3.2 %collective-permute-start.12 = (f32[4,8,8,128]{3,2,1,0:T(8,128)S(1)}, f32[4,8,8,128]{3,2,1,0:T(8,128)S(1)}, u32[]{:S(2)}, u32[]{:S(2)}) collective-permute-start(f32[4,8,8,128]{3,2,1,0:T(8,128)S(1)} %pad_maximum_fusion.1.near_ref), channel_id=1, source_target_pairs={{0,1},{1,0},{2,3},{3,2},{4,5},{5,4},{6,7},{7,6},{8,9},{9,8},{10,11... | collective-permute-start | bytes 393224 | tf_op jit(solution)/shard_map/ppermute | solution.py:258

commit v9 on v8

--- a/solution.py
+++ b/solution.py
@@ -18,6 +18,7 @@
 SCALE = 0.125
 LOG2E = 1.4426950408889634
 KV = ("z", "y")
+TP = ("x", "c")
 ALL = ("z", "y", "x", "c")
 FAR = 1 << 20
 F32 = jnp.float32
@@ -30,7 +31,7 @@
     return lax.broadcasted_iota(jnp.int32, shape, len(shape) - 1) < LANES // 2
 
 
-def offer_kernel(rank_ref, tp_ref, keys_ref, vals_ref, chosen_ref, out_ref, piece_ref, want_ref, pairs):
+def offer_kernel(rank_ref, tp_ref, keys_ref, vals_ref, chosen_ref, out_ref, piece_ref, pairs):
     rank = rank_ref[0]
     tp = tp_ref[0]
     flip = tp & 1
@@ -48,7 +49,6 @@
         return jnp.broadcast_to(best, (PEERS, LANES)).astype(F32)
 
     best = wanted(jnp.where(jnp.full(at.shape, flip, jnp.int32) == 0, at, (at & 7) * 8 + (at >> 3)))
-    want_ref[...] = wanted(at)
     for b in range(BLOCKS):
         at = pl.multiple_of(b * BLOCK + tp * ROWS, ROWS)
         piece = pairs[pl.ds(at, ROWS), :].astype(BF16)
@@ -70,15 +70,47 @@
             out_ref[i, r] = got.astype(BF16)
 
 
-def settle_kernel(own_ref, given_ref, out_ref):
-    totals = [own_ref[b] for b in range(BLOCKS)]
-    for s in range(PEERS):
-        got = given_ref[s, :ROWS].astype(F32)
-        want = given_ref[s, ROWS:].astype(F32)
+def turn_kernel(tp_ref, part_ref, away_ref, out_ref):
+    flip = tp_ref[0] & 1
+    for m in range(PEERS // 2):
+        two = part_ref[:, m * LANES : (m + 1) * LANES].astype(F32).T.astype(BF16)
+        for n in range(2):
+            hi, lo = (2 * m + n) // SIDE, (2 * m + n) % SIDE
+            out_ref[jnp.where(flip == 0, lo, hi), jnp.where(flip == 0, hi, lo)] = two[
+                n * BLOCK : (n + 1) * BLOCK
+            ]
+    for i in range(SIDE):
+        for r in range(SIDE):
+            out_ref[i, SIDE, r * ROWS : (r + 1) * ROWS] = away_ref[i * SIDE + r]
+
+
+def fold_kernel(wants_ref, parts_ref, out_ref):
+    for r in range(SIDE):
+        total = parts_ref[0, r].astype(F32)
+        for i in range(1, SIDE):
+            total = total + parts_ref[i, r].astype(F32)
+        out_ref[r, 0] = total.astype(BF16)
+        sums = [jnp.zeros((ROWS, LANES), F32) for _ in range(BLOCKS)]
+        for i in range(SIDE):
+            want = jnp.broadcast_to(wants_ref[i].astype(F32)[r : r + 1], (ROWS, LANES))
+            got = parts_ref[i, SIDE, r * ROWS : (r + 1) * ROWS].astype(F32)
+            for b in range(BLOCKS):
+                sums[b] = sums[b] + jnp.where(want == b + 1.0, got, 0.0)
         for b in range(BLOCKS):
-            totals[b] = totals[b] + jnp.where(want == b + 1.0, got, 0.0)
+            out_ref[r, 1, b * ROWS : (b + 1) * ROWS] = sums[b].astype(BF16)
+
+
+def settle_kernel(own_ref, back_ref, out_ref, weight_ref):
+    weight = back_ref[0, 0].astype(F32)
+    for i in range(1, SIDE):
+        weight = weight + back_ref[i, 0].astype(F32)
+    weight_ref[...] = weight
     for b in range(BLOCKS):
-        out_ref[b] = totals[b]
+        total = own_ref[b]
+        for i in range(SIDE):
+            total = total + back_ref[i, 1, b * ROWS : (b + 1) * ROWS].astype(F32)
+        for i in range(SIDE):
+            out_ref[i, b] = total
 
 
 def pack_kernel(q_ref, g_ref, o_ref, log_ref, out_ref):
@@ -103,11 +135,10 @@
 
 def attend_kernel(
     slot_ref,
-    home_ref,
+    tp_ref,
     rel_ref,
     fetched_ref,
     piece_ref,
-    want_ref,
     q0,
     q1,
     q2,
@@ -189,13 +220,14 @@
         dk = lax.dot_general(dscores, q, plain, preferred_element_type=F32)
         gq = lax.dot_general(dscores, k2, (((0,), (0,)), ((), ())), preferred_element_type=F32)
         for k in range(4):
-            gq_own_ref[k, pl.ds(at, BLOCK), :] = gq[k * BLOCK : (k + 1) * BLOCK]
-            gq_far_ref[k, pl.ds(at, BLOCK), :] = gq[(4 + k) * BLOCK : (5 + k) * BLOCK].astype(BF16)
+            to = ((tp_ref[0] >> 1) + 4 - k) & 3
+            gq_own_ref[to, pl.ds(at, BLOCK), :] = gq[k * BLOCK : (k + 1) * BLOCK]
+            gq_far_ref[to, pl.ds(at, BLOCK), :] = gq[(4 + k) * BLOCK : (5 + k) * BLOCK].astype(BF16)
         both = jnp.where(low, dk[:LANES], dv[LANES:]) + pltpu.roll(
             jnp.where(low, dv[:LANES], dk[LANES:]), LANES // 2, 1
         )
         for s in range(SLOTS):
-            acc[home_ref[j, s]] += both[s * ROWS : (s + 1) * ROWS]
+            acc[slot_ref[j, s]] += both[s * ROWS : (s + 1) * ROWS]
         return carry
 
     def some_blocks(i, carry):
@@ -204,22 +236,15 @@
         return carry
 
     lax.fori_loop(0, BLOCKS // 4, some_blocks, 0)
-    away_ref[:, :ROWS] = acc[:PEERS].astype(BF16)
-    for s in range(PEERS):
-        want = jnp.broadcast_to(want_ref[s : s + 1, :], (ROWS, LANES))
-        away_ref[s, ROWS:] = want.astype(BF16)
+    away_ref[...] = acc[:PEERS].astype(BF16)
     own_ref[...] = acc[PEERS:]
 
 
-def place_kernel(tp_ref, near_ref, far_ref, keys_ref, vals_ref, rows):
-    x = tp_ref[0] >> 1
-    mine = jnp.full((ROWS, LANES), tp_ref[0] & 1, jnp.int32)
-    for xa in range(4):
-        k = (x + 4 - xa) & 3
-        for ca in range(2):
-            for b in range(BLOCKS):
-                at = b * BLOCK + (xa * 2 + ca) * ROWS
-                rows[at : at + ROWS, :] = jnp.where(mine == ca, near_ref[k, b], far_ref[k, b])
+def place_kernel(pieces_ref, keys_ref, vals_ref, rows):
+    for i in range(SIDE):
+        for b in range(BLOCKS):
+            at = b * BLOCK + i * ROWS
+            rows[at : at + ROWS, :] = pieces_ref[i, b]
     turned = rows[...].T
     keys_ref[...] = turned[: LANES // 2]
     vals_ref[...] = turned[LANES // 2 :]
@@ -250,10 +275,6 @@
     return lax.ppermute(arr, "x", [(i, (i + k) % 4) for i in range(4)])
 
 
-def x_back(arr, k):
-    return lax.ppermute(arr, "x", [((i + k) % 4, i) for i in range(4)])
-
-
 def swap(arr):
     return lax.ppermute(arr, "c", [(0, 1), (1, 0)])
 
@@ -280,10 +301,6 @@
     )
 
 
-def exchange(arr):
-    return lax.all_to_all(arr, KV, split_axis=0, concat_axis=0, tiled=True)
-
-
 def near_core(arr):
     return pltpu.with_memory_space_constraint(arr, pltpu.VMEM)
 
@@ -293,13 +310,12 @@
     x = lax.axis_index("x").astype(jnp.int32)
     c = lax.axis_index("c").astype(jnp.int32)
     tp = x * 2 + c
-    offer, piece, want = call(
+    offer, piece = call(
         offer_kernel,
         [SMEM] * 2 + [VMEM] * 3,
         [
             sds((SIDE, BLOCKS + 1, ROWS, LANES), BF16),
             sds((BLOCKS, ROWS, LANES), BF16),
-            sds((PEERS, LANES), F32),
         ],
         (rank.reshape(1), tp.reshape(1), keys.T, values.T, chosen),
         1 << 18,
@@ -337,19 +353,18 @@
     peer = jnp.where(c == 0, (owner & 7) * 8 + (owner >> 3), owner)
     slot = jnp.where(listed, jnp.where(owner == rank, PEERS + inner, peer), 0)
     starts = rank * TOK + lax.broadcasted_iota(jnp.int32, chosen.shape, 0) * BLOCK
-    home = jnp.where(listed, jnp.where(owner == rank, PEERS + inner, owner), 0)
     rel = jnp.where(listed, chosen * BLOCK + ROWS * tp - starts, FAR)
 
     away, own, gq_own, gq_far = call(
         attend_kernel,
-        [SMEM] * 3 + [VMEM] * 8,
+        [SMEM] * 3 + [VMEM] * 7,
         [
-            held((PEERS, 2 * ROWS, LANES), BF16),
+            held((PEERS, ROWS, LANES), BF16),
             held((BLOCKS, ROWS, LANES), F32),
             held((4, TOK, LANES), F32),
             held((4, TOK, LANES), BF16),
         ],
-        (slot, home, rel, near_core(fetched), near_core(piece), near_core(want), *map(near_core, qds), near_core(qd_far)),
+        (slot, tp.reshape(1), rel, near_core(fetched), near_core(piece), *map(near_core, qds), near_core(qd_far)),
         1 << 30,
         limit=16 << 20,
         scratch_shapes=[
@@ -359,33 +374,44 @@
         ],
         name="attend",
     )
-    gq4 = gq_own + swap(gq_far).astype(F32)
-    returned = exchange(away)
-    gq = gq4[0]
-    for k in (1, 2, 3):
-        gq = gq + x_back(gq4[k].astype(BF16), k).astype(F32)
-    grad_queries = gq.astype(BF16)
+    gq4 = (gq_own + swap(gq_far).astype(F32)).astype(BF16)
+    got = lax.all_to_all(gq4, "x", split_axis=0, concat_axis=0, tiled=True).astype(F32)
+    grad_queries = (got[0] + got[1] + (got[2] + got[3])).astype(BF16)
     part = lax.dot_general(
-        normed, grad_queries, (((0,), (0,)), ((), ())), preferred_element_type=F32
+        grad_queries, normed, (((0,), (0,)), ((), ())), preferred_element_type=F32
     ).astype(BF16)
-    parts = exchange(part.reshape(PEERS, BLOCK, LANES))
-    weight_grad = jnp.sum(parts.astype(F32), axis=0)
-
-    total = call(
+    turned = call(
+        turn_kernel,
+        [SMEM, VMEM, VMEM],
+        held((SIDE, SIDE + 1, BLOCK, LANES), BF16),
+        (tp.reshape(1), near_core(part), near_core(away)),
+        1 << 20,
+        name="turn",
+    )
+    parts = along(turned, False)
+    folded = call(
+        fold_kernel,
+        [VMEM] * 2,
+        held((SIDE, 2, BLOCK, LANES), BF16),
+        (near_core(wants), near_core(parts)),
+        1 << 20,
+        name="fold",
+    )
+    back = along(folded, True)
+    total, weight_grad = call(
         settle_kernel,
         [VMEM] * 2,
-        held((BLOCKS, ROWS, LANES), F32),
-        (near_core(own), near_core(returned)),
+        [sds((SIDE, BLOCKS, ROWS, LANES), F32), sds((BLOCK, LANES), F32)],
+        (near_core(own), near_core(back)),
         1 << 20,
         name="settle",
     )
-    near = jnp.stack([total] + [x_from(total, k) for k in (1, 2, 3)])
-    far = swap(near)
+    pieces = lax.all_to_all(total, TP, split_axis=0, concat_axis=0, tiled=True)
     grad_keys, grad_values = call(
         place_kernel,
-        [SMEM, VMEM, VMEM],
+        [VMEM],
         [sds((64, TOK), F32), sds((64, TOK), F32)],
-        (tp.reshape(1), near_core(near), near_core(far)),
+        (near_core(pieces),),
         1 << 20,
         scratch_shapes=[pltpu.VMEM((TOK, LANES), F32)],
         name="place",

time: 143 us -> 141 us (0.986)
  the two profiles are of different devices: /device:TPU:2 before, /device:TPU:1 now
where the time goes in v9:
time: 141 us; the launch traced here: 140 us
  blocking collectives  72.5 us (51%)
  starting transfers between devices  32.1 us (23%)
  waiting for transfers between devices  20.7 us (15%)
  Pallas kernels  10.9 us (8%)
  other arithmetic  1.47 us (1%)
    all_to_all x3, blocking collectives, along(): lax.all_to_all(arr, ALL, split_axis=0, concat_axis=0, tiled=True, axis_in...  48.4 us
    ppermute x3, starting transfers between devices, swap(): return lax.ppermute(arr, 'c', [(0, 1), (1, 0)])  16.3 us
    all_to_all x1, blocking collectives, step(): pieces = lax.all_to_all(total, TP, split_axis=0, concat_axis=0, tiled=True)  12.2 us
    all_to_all x1, blocking collectives, step(): lax.all_to_all(gq4, 'x', split_axis=0, concat_axis=0, tiled=True)  11.9 us
    pallas_call x8, Pallas kernels, call(): pl.pallas_call(kernel, in_specs=ins, out_specs=[VMEM] * len(out_shape) if...  10.9 us
    ppermute x3, waiting for transfers between devices, x_from(): return lax.ppermute(arr, 'x', [(i, (i + k) % 4) for i in range(4)])  10.5 us
    ppermute x3, starting transfers between devices, x_from(): return lax.ppermute(arr, 'x', [(i, (i + k) % 4) for i in range(4)])  10.1 us
    all_to_all x1, waiting for transfers between devices, along(): lax.all_to_all(arr, ALL, split_axis=0, concat_axis=0, tiled=True, axis_in...  7.83 us
  transfers between devices with their start and end apart: 7, of which 5 were waited for; matrix products, arithmetic and copies ran while one was open for 0% of the time, Pallas kernels for 2%

profile of v9, /device:TPU:1, one launch (start us, length us, event | category | flops | bytes accessed | tf_op | source)
XLA Modules:
  0.0 139.9 jit_solution(5998569133373900724)
XLA Ops:
  0.6 1.9 %pack.1.q0 = bf16[1072,128]{1,0:T(8,128)(2,1)} custom-call(bf16[512,128]{1,0:T(8,128)(2,1)} %q_ref.1, bf16[512,128]{1,0:T(8,128)(2,1)} %g_ref.1, bf16[512,128]{1,0:T(8,128)(2,1)} %o_ref.1, f32[2,512]{1,0:T(2,128)} %bitcast.27), custom_call_target="tpu_custom_call" | custom-call | flops 262144 | bytes 1048576 | tf_op jit(solution)/shard_map/pack/pallas_call | solution.py:255
  2.5 5.2 %collective-permute-start.3 = (bf16[1072,128]{1,0:T(8,128)(2,1)}, bf16[1072,128]{1,0:T(8,128)(2,1)S(1)}, u32[]{:S(2)}, u32[]{:S(2)}) collective-permute-start(bf16[1072,128]{1,0:T(8,128)(2,1)} %pack.1.q0), channel_id=1, source_target_pairs={{0,6},{2,0},{4,2},{6,4},{1,7},{3,1},{5,3},{7,5},{8,14},{10,8},{12,... | collective-permute-start | bytes 823304 | tf_op jit(solution)/shard_map/ppermute | solution.py:275
  7.7 2.4 %collective-permute-start.2 = (bf16[1072,128]{1,0:T(8,128)(2,1)}, bf16[1072,128]{1,0:T(8,128)(2,1)S(1)}, u32[]{:S(2)}, u32[]{:S(2)}) collective-permute-start(bf16[1072,128]{1,0:T(8,128)(2,1)} %pack.1.q0), channel_id=1, source_target_pairs={{0,4},{2,6},{4,0},{6,2},{1,5},{3,7},{5,1},{7,3},{8,12},{10,14},{12... | collective-permute-start | bytes 823304 | tf_op jit(solution)/shard_map/ppermute | solution.py:275
  10.2 2.5 %collective-permute-start.1 = (bf16[1072,128]{1,0:T(8,128)(2,1)}, bf16[1072,128]{1,0:T(8,128)(2,1)S(1)}, u32[]{:S(2)}, u32[]{:S(2)}) collective-permute-start(bf16[1072,128]{1,0:T(8,128)(2,1)} %pack.1.q0), channel_id=1, source_target_pairs={{0,2},{2,4},{4,6},{6,0},{1,3},{3,5},{5,7},{7,1},{8,10},{10,12},{12... | collective-permute-start | bytes 823304 | tf_op jit(solution)/shard_map/ppermute | solution.py:275
  12.7 4.1 %collective-permute-done.2.q2 = bf16[1072,128]{1,0:T(8,128)(2,1)S(1)} collective-permute-done((bf16[1072,128]{1,0:T(8,128)(2,1)}, bf16[1072,128]{1,0:T(8,128)(2,1)S(1)}, u32[]{:S(2)}, u32[]{:S(2)}) %collective-permute-start.2) | collective-permute-done | bytes 274464 | tf_op jit(solution)/shard_map/ppermute | solution.py:275
  16.8 6.4 %collective-permute-done.1.q1 = bf16[1072,128]{1,0:T(8,128)(2,1)S(1)} collective-permute-done((bf16[1072,128]{1,0:T(8,128)(2,1)}, bf16[1072,128]{1,0:T(8,128)(2,1)S(1)}, u32[]{:S(2)}, u32[]{:S(2)}) %collective-permute-start.1) | collective-permute-done | bytes 274464 | tf_op jit(solution)/shard_map/ppermute | solution.py:275
  23.2 1.2 pad_maximum_fusion
  24.4 4.9 %collective-permute-start.4 = (bf16[4,1072,128]{2,1,0:T(8,128)(2,1)S(1)}, bf16[4,1072,128]{2,1,0:T(8,128)(2,1)S(1)}, u32[]{:S(2)}, u32[]{:S(2)}) collective-permute-start(bf16[4,1072,128]{2,1,0:T(8,128)(2,1)S(1)} %pad_maximum_fusion), channel_id=1, source_target_pairs={{0,1},{1,0},{2,3},{3,2},{4,5},{5,4},{6,7},{7,6},{8,9},{9,8},{10,11... | collective-permute-start | bytes 3293192 | tf_op jit(solution)/shard_map/ppermute | solution.py:279
  29.3 1.8 %offer.1 = (bf16[8,9,8,128]{3,2,1,0:T(8,128)(2,1)}, bf16[8,8,128]{2,1,0:T(8,128)(2,1)}) custom-call(s32[1]{0:T(128)} %bitcast.1.rank_ref, s32[1]{0:T(128)} %bitcast.tp_ref, bf16[64,512]{1,0:T(8,128)(2,1)} %bitcast.25, bf16[64,512]{1,0:T(8,128)(2,1)} %bitcast.26, s32[8,16]{1,0:T(8,128)} %chosen_ref.1), custom_call_target="tpu_custom_call" | custom-call | flops 262144 | bytes 1048576 | tf_op jit(solution)/shard_map/offer/pallas_call | solution.py:255
  31.1 14.9 %all_to_all.30.pushed_ref = bf16[8,9,8,128]{3,2,1,0:T(8,128)(2,1)S(1)} all-to-all(bf16[8,9,8,128]{3,2,1,0:T(8,128)(2,1)} %get-tuple-element.14), channel_id=1, replica_groups={{0,64,128,192,256,320,384,448},{8,72,136,200,264,328,392,456},{16,80,14..., dimensions={0} | all-to-all | bytes 294912 | tf_op jit(solution)/shard_map/all_to_all | solution.py:299
  46.0 6.6 %collective-permute-start = (bf16[8,8,128]{2,1,0:T(8,128)(2,1)S(1)}, bf16[8,8,128]{2,1,0:T(8,128)(2,1)S(1)}, u32[]{:S(2)}, u32[]{:S(2)}) collective-permute-start(bf16[8,8,128]{2,1,0:T(8,128)(2,1)S(1)} %slice_bitcast_fusion), channel_id=1, source_target_pairs={{0,1},{1,0},{2,3},{3,2},{4,5},{5,4},{6,7},{7,6},{8,9},{9,8},{10,11... | collective-permute-start | bytes 49160 | tf_op jit(solution)/shard_map/ppermute | solution.py:279
  52.5 0.8 collective-permute-done.wants_ref
  53.4 0.8 pick.1
  54.2 5.7 %all-to-all-start.1 = ((bf16[8,8,8,128]{3,2,1,0:T(8,128)(2,1)}), bf16[8,8,8,128]{3,2,1,0:T(8,128)(2,1)S(1)}, u32[]{:S(2)}, u32[]{:S(2)}) async-start(bf16[8,8,8,128]{3,2,1,0:T(8,128)(2,1)} %pick.1), calls=%async_computation.1 | async-start | bytes 262144 | tf_op jit(solution)/shard_map/all_to_all | solution.py:299
  59.9 0.1 subtract_select_fusion
  60.0 7.8 %all-to-all-done.1 = bf16[8,8,8,128]{3,2,1,0:T(8,128)(2,1)S(1)} async-done(((bf16[8,8,8,128]{3,2,1,0:T(8,128)(2,1)}), bf16[8,8,8,128]{3,2,1,0:T(8,128)(2,1)S(1)}, u32[]{:S(2)}, u32[]{:S(2)}) %all-to-all-start.1) | async-done | bytes 131104 | tf_op jit(solution)/shard_map/all_to_all | solution.py:299
  67.8 0.7 copy-done.1
  68.6 4.3 %attend.1 = (bf16[64,8,128]{2,1,0:T(8,128)(2,1)S(1)}, f32[8,8,128]{2,1,0:T(8,128)S(1)}, f32[4,512,128]{2,1,0:T(8,128)S(1)}, bf16[4,512,128]{2,1,0:T(8,128)(2,1)S(1)}) custom-call(s32[8,16]{1,0:T(8,128)S(1)} %get-tuple-element.25.slot_ref, s32[1]{0:T(128)} %bitcast.tp_ref, s32[8,16]{1,0:T(8,128)S(1)} %get-tuple-element.24.rel_ref, ...), custom_call_target="tpu_custom_call" | custom-call | flops 1073741824 | bytes 1048576 | tf_op jit(solution)/shard_map/attend/pallas_call | solution.py:255
  72.9 4.8 %collective-permute-start.5 = (bf16[4,512,128]{2,1,0:T(8,128)(2,1)S(1)}, bf16[4,512,128]{2,1,0:T(8,128)(2,1)S(1)}, u32[]{:S(2)}, u32[]{:S(2)}) collective-permute-start(bf16[4,512,128]{2,1,0:T(8,128)(2,1)S(1)} %get-tuple-element.17), channel_id=1, source_target_pairs={{0,1},{1,0},{2,3},{3,2},{4,5},{5,4},{6,7},{7,6},{8,9},{9,8},{10,11... | collective-permute-start | bytes 1572872 | tf_op jit(solution)/shard_map/ppermute | solution.py:279
  77.7 1.5 %collective-permute-done.5 = bf16[4,512,128]{2,1,0:T(8,128)(2,1)S(1)} collective-permute-done((bf16[4,512,128]{2,1,0:T(8,128)(2,1)S(1)}, bf16[4,512,128]{2,1,0:T(8,128)(2,1)S(1)}, u32[]{:S(2)}, u32[]{:S(2)}) %collective-permute-start.5) | collective-permute-done | bytes 524320 | tf_op jit(solution)/shard_map/ppermute | solution.py:279
  79.2 0.1 add_convert_fusion
  79.3 11.9 %all_to_all.31 = bf16[4,512,128]{2,1,0:T(8,128)(2,1)S(1)} all-to-all(bf16[4,512,128]{2,1,0:T(8,128)(2,1)S(1)} %add_convert_fusion), channel_id=1, replica_groups=mesh['z'=8,'y'=8,'x'=4,'c'=2] {'x'}, dimensions={0} | all-to-all | bytes 1048576 | tf_op jit(solution)/shard_map/all_to_all | solution.py:378
  91.2 0.1 convert_element_type.20
  91.3 0.1 fusion.2
  91.3 0.8 convolution_convert_fusion.part_ref
  92.1 0.3 turn.1
  92.5 21.8 %all_to_all.32.parts_ref = bf16[8,9,64,128]{3,2,1,0:T(8,128)(2,1)S(1)} all-to-all(bf16[8,9,64,128]{3,2,1,0:T(8,128)(2,1)S(1)} %turn.1), channel_id=1, replica_groups={{0,8,16,24,32,40,48,56},{64,72,80,88,96,104,112,120},{128,136,144,152,1..., dimensions={0} | all-to-all | bytes 2359296 | tf_op jit(solution)/shard_map/all_to_all | solution.py:299
  114.2 0.4 fold.1
  114.6 11.7 %all_to_all.33.back_ref = bf16[8,2,64,128]{3,2,1,0:T(8,128)(2,1)S(1)} all-to-all(bf16[8,2,64,128]{3,2,1,0:T(8,128)(2,1)S(1)} %fold.1), channel_id=1, replica_groups={{0,64,128,192,256,320,384,448},{8,72,136,200,264,328,392,456},{16,80,14..., dimensions={0} | all-to-all | bytes 524288 | tf_op jit(solution)/shard_map/all_to_all | solution.py:299
  126.3 0.6 settle.1
  127.0 12.2 %all_to_all.34.pieces_ref = f32[8,8,8,128]{3,2,1,0:T(8,128)S(1)} all-to-all(f32[8,8,8,128]{3,2,1,0:T(8,128)S(1)} %get-tuple-element.20), channel_id=1, replica_groups=mesh['z'=8,'y'=8,'x'=4,'c'=2] {'x','c'}, dimensions={0} | all-to-all | bytes 524288 | tf_op jit(solution)/shard_map/all_to_all | solution.py:409
  139.1 0.8 place.1
  (13 shorter events, 0.0 us)
Async XLA Ops:
  2.5 10.2 %collective-permute-start.3 = (bf16[1072,128]{1,0:T(8,128)(2,1)}, bf16[1072,128]{1,0:T(8,128)(2,1)S(1)}, u32[]{:S(2)}, u32[]{:S(2)}) collective-permute-start(bf16[1072,128]{1,0:T(8,128)(2,1)} %pack.1.q0), channel_id=1, source_target_pairs={{0,6},{2,0},{4,2},{6,4},{1,7},{3,1},{5,3},{7,5},{8,14},{10,8},{12,... | collective-permute-start | bytes 823304 | tf_op jit(solution)/shard_map/ppermute | solution.py:275
  7.7 9.0 %collective-permute-start.2 = (bf16[1072,128]{1,0:T(8,128)(2,1)}, bf16[1072,128]{1,0:T(8,128)(2,1)S(1)}, u32[]{:S(2)}, u32[]{:S(2)}) collective-permute-start(bf16[1072,128]{1,0:T(8,128)(2,1)} %pack.1.q0), channel_id=1, source_target_pairs={{0,4},{2,6},{4,0},{6,2},{1,5},{3,7},{5,1},{7,3},{8,12},{10,14},{12... | collective-permute-start | bytes 823304 | tf_op jit(solution)/shard_map/ppermute | solution.py:275
  10.2 13.0 %collective-permute-start.1 = (bf16[1072,128]{1,0:T(8,128)(2,1)}, bf16[1072,128]{1,0:T(8,128)(2,1)S(1)}, u32[]{:S(2)}, u32[]{:S(2)}) collective-permute-start(bf16[1072,128]{1,0:T(8,128)(2,1)} %pack.1.q0), channel_id=1, source_target_pairs={{0,2},{2,4},{4,6},{6,0},{1,3},{3,5},{5,7},{7,1},{8,10},{10,12},{12... | collective-permute-start | bytes 823304 | tf_op jit(solution)/shard_map/ppermute | solution.py:275
  23.2 36.7 %copy-start.4 = (s32[8,16]{1,0:T(8,128)S(1)}, s32[8,16]{1,0:T(8,128)}, u32[]{:S(2)}) copy-start(s32[8,16]{1,0:T(8,128)} %chosen_ref.1) | copy-start | bytes 1540
  23.2 44.7 %copy-start = (bf16[1072,128]{1,0:T(8,128)(2,1)S(1)}, bf16[1072,128]{1,0:T(8,128)(2,1)}, u32[]{:S(2)}) copy-start(bf16[1072,128]{1,0:T(8,128)(2,1)} %pack.1.q0) | copy-start | bytes 823300
  24.4 43.5 %collective-permute-start.4 = (bf16[4,1072,128]{2,1,0:T(8,128)(2,1)S(1)}, bf16[4,1072,128]{2,1,0:T(8,128)(2,1)S(1)}, u32[]{:S(2)}, u32[]{:S(2)}) collective-permute-start(bf16[4,1072,128]{2,1,0:T(8,128)(2,1)S(1)} %pad_maximum_fusion), channel_id=1, source_target_pairs={{0,1},{1,0},{2,3},{3,2},{4,5},{5,4},{6,7},{7,6},{8,9},{9,8},{10,11... | collective-permute-start | bytes 3293192 | tf_op jit(solution)/shard_map/ppermute | solution.py:279
  46.0 7.4 %collective-permute-start = (bf16[8,8,128]{2,1,0:T(8,128)(2,1)S(1)}, bf16[8,8,128]{2,1,0:T(8,128)(2,1)S(1)}, u32[]{:S(2)}, u32[]{:S(2)}) collective-permute-start(bf16[8,8,128]{2,1,0:T(8,128)(2,1)S(1)} %slice_bitcast_fusion), channel_id=1, source_target_pairs={{0,1},{1,0},{2,3},{3,2},{4,5},{5,4},{6,7},{7,6},{8,9},{9,8},{10,11... | collective-permute-start | bytes 49160 | tf_op jit(solution)/shard_map/ppermute | solution.py:279
  54.2 13.6 %all-to-all-start.1 = ((bf16[8,8,8,128]{3,2,1,0:T(8,128)(2,1)}), bf16[8,8,8,128]{3,2,1,0:T(8,128)(2,1)S(1)}, u32[]{:S(2)}, u32[]{:S(2)}) async-start(bf16[8,8,8,128]{3,2,1,0:T(8,128)(2,1)} %pick.1), calls=%async_computation.1 | async-start | bytes 262144 | tf_op jit(solution)/shard_map/all_to_all | solution.py:299
  67.8 0.7 copy-start.1
  72.9 6.3 %collective-permute-start.5 = (bf16[4,512,128]{2,1,0:T(8,128)(2,1)S(1)}, bf16[4,512,128]{2,1,0:T(8,128)(2,1)S(1)}, u32[]{:S(2)}, u32[]{:S(2)}) collective-permute-start(bf16[4,512,128]{2,1,0:T(8,128)(2,1)S(1)} %get-tuple-element.17), channel_id=1, source_target_pairs={{0,1},{1,0},{2,3},{3,2},{4,5},{5,4},{6,7},{7,6},{8,9},{9,8},{10,11... | collective-permute-start | bytes 1572872 | tf_op jit(solution)/shard_map/ppermute | solution.py:279
  79.2 12.1 %copy-start.2 = (bf16[512,4096]{1,0:T(8,128)(2,1)S(1)}, bf16[512,4096]{1,0:T(8,128)(2,1)}, u32[]{:S(2)}) copy-start(bf16[512,4096]{1,0:T(8,128)(2,1)} %param.8) | copy-start | bytes 12582916
  91.3 0.8 copy-start.3

commit v10 on v9

--- a/solution.py
+++ b/solution.py
@@ -25,6 +25,7 @@
 BF16 = jnp.bfloat16
 VMEM = pl.BlockSpec(memory_space=pltpu.VMEM)
 SMEM = pl.BlockSpec(memory_space=pltpu.SMEM)
+ANY = pl.BlockSpec(memory_space=pltpu.HBM)
 
 
 def low_lanes(shape):
@@ -110,17 +111,25 @@
         for i in range(SIDE):
             total = total + back_ref[i, 1, b * ROWS : (b + 1) * ROWS].astype(F32)
         for i in range(SIDE):
-            out_ref[i, b] = total
-
-
-def pack_kernel(q_ref, g_ref, o_ref, log_ref, out_ref):
-    out_ref[0:TOK] = q_ref[...]
-    out_ref[TOK : 2 * TOK] = g_ref[...]
-    prod = (g_ref[...].astype(F32) * o_ref[...].astype(F32)).T
+            out_ref[i, b] = total.astype(BF16)
+
+
+def pack_kernel(q_ref, g_ref, o_ref, log_ref, out_ref, o_here, log_here, sems):
+    moves = [
+        pltpu.make_async_copy(q_ref, out_ref.at[pl.ds(0, TOK)], sems.at[0]),
+        pltpu.make_async_copy(g_ref, out_ref.at[pl.ds(TOK, TOK)], sems.at[1]),
+        pltpu.make_async_copy(o_ref, o_here, sems.at[2]),
+        pltpu.make_async_copy(log_ref, log_here, sems.at[3]),
+    ]
+    for move in moves:
+        move.start()
+    for move in moves:
+        move.wait()
+    prod = (out_ref[TOK : 2 * TOK].astype(F32) * o_here[...].astype(F32)).T
     half = LANES // 2
     stats = jnp.concatenate(
         [
-            log_ref[...],
+            log_here[...],
             jnp.sum(prod[:half], axis=0, keepdims=True),
             jnp.sum(prod[half:], axis=0, keepdims=True),
         ],
@@ -244,7 +253,7 @@
     for i in range(SIDE):
         for b in range(BLOCKS):
             at = b * BLOCK + i * ROWS
-            rows[at : at + ROWS, :] = pieces_ref[i, b]
+            rows[at : at + ROWS, :] = pieces_ref[i, b].astype(F32)
     turned = rows[...].T
     keys_ref[...] = turned[: LANES // 2]
     vals_ref[...] = turned[LANES // 2 :]
@@ -303,6 +312,10 @@
 
 def near_core(arr):
     return pltpu.with_memory_space_constraint(arr, pltpu.VMEM)
+
+
+def stay(arr):
+    return pltpu.with_memory_space_constraint(arr, pltpu.HBM)
 
 
 def step(normed, queries, keys, values, attended, cotangent, log_sum, chosen):
@@ -337,14 +350,19 @@
 
     qd = call(
         pack_kernel,
-        [VMEM] * 4,
-        sds((2 * TOK + 48, LANES), BF16),
-        (queries, cotangent, attended, log_sum.T),
+        [ANY] * 4,
+        held((2 * TOK + 48, LANES), BF16),
+        tuple(map(stay, (queries, cotangent, attended, log_sum.T))),
         1 << 18,
-        limit=58 << 20,
+        scratch_shapes=[
+            pltpu.VMEM((TOK, LANES), BF16),
+            pltpu.VMEM((2, TOK), F32),
+            pltpu.SemaphoreType.DMA((4,)),
+        ],
         name="pack",
     )
-    qds = [qd] + [x_from(qd, k) for k in (1, 2, 3)]
+    first = x_from(qd, 1)
+    qds = [qd, first] + [x_from(qd, k) for k in (2, 3)]
     qd_far = swap(jnp.stack(qds))
 
     owner = chosen >> 3
@@ -401,7 +419,7 @@
     total, weight_grad = call(
         settle_kernel,
         [VMEM] * 2,
-        [sds((SIDE, BLOCKS, ROWS, LANES), F32), sds((BLOCK, LANES), F32)],
+        [held((SIDE, BLOCKS, ROWS, LANES), BF16), sds((BLOCK, LANES), F32)],
         (near_core(own), near_core(back)),
         1 << 20,
         name="settle",

time: 141 us -> 138 us (0.979)
  no operation moved by 1% of the time
where the time goes in v10:
time: 138 us
  blocking collectives  71.2 us (52%)
  starting transfers between devices  32.1 us (23%)
  waiting for transfers between devices  20.4 us (15%)
  Pallas kernels  10.3 us (7%)
  other arithmetic  1.43 us (1%)
    all_to_all x3, blocking collectives, along(): lax.all_to_all(arr, ALL, split_axis=0, concat_axis=0, tiled=True, axis_in...  48.4 us
    ppermute x3, starting transfers between devices, swap(): return lax.ppermute(arr, 'c', [(0, 1), (1, 0)])  16.3 us
    all_to_all x1, blocking collectives, step(): lax.all_to_all(gq4, 'x', split_axis=0, concat_axis=0, tiled=True)  11.9 us
    all_to_all x1, blocking collectives, step(): pieces = lax.all_to_all(total, TP, split_axis=0, concat_axis=0, tiled=True)  10.9 us
    ppermute x3, waiting for transfers between devices, x_from(): return lax.ppermute(arr, 'x', [(i, (i + k) % 4) for i in range(4)])  10.3 us
    pallas_call x8, Pallas kernels, call(): pl.pallas_call(kernel, in_specs=ins, out_specs=[VMEM] * len(out_shape) if...  10.3 us
    ppermute x3, starting transfers between devices, x_from(): return lax.ppermute(arr, 'x', [(i, (i + k) % 4) for i in range(4)])  10.1 us
    all_to_all x1, waiting for transfers between devices, along(): lax.all_to_all(arr, ALL, split_axis=0, concat_axis=0, tiled=True, axis_in...  7.83 us
  transfers between devices with their start and end apart: 7, of which 5 were waited for; matrix products, arithmetic and copies ran while one was open for 0% of the time, Pallas kernels for 2%

profile of v10, /device:TPU:1, one launch (start us, length us, event | category | flops | bytes accessed | tf_op | source)
XLA Modules:
  0.0 137.8 jit_solution(10829850279333170819)
XLA Ops:
  0.6 1.2 pack.1.q0
  1.9 5.2 %collective-permute-start.3 = (bf16[1072,128]{1,0:T(8,128)(2,1)S(1)}, bf16[1072,128]{1,0:T(8,128)(2,1)S(1)}, u32[]{:S(2)}, u32[]{:S(2)}) collective-permute-start(bf16[1072,128]{1,0:T(8,128)(2,1)S(1)} %pack.1.q0), channel_id=1, source_target_pairs={{0,6},{2,0},{4,2},{6,4},{1,7},{3,1},{5,3},{7,5},{8,14},{10,8},{12,... | collective-permute-start | bytes 823304 | tf_op jit(solution)/shard_map/ppermute | solution.py:284
  7.1 2.4 %collective-permute-start.2 = (bf16[1072,128]{1,0:T(8,128)(2,1)S(1)}, bf16[1072,128]{1,0:T(8,128)(2,1)S(1)}, u32[]{:S(2)}, u32[]{:S(2)}) collective-permute-start(bf16[1072,128]{1,0:T(8,128)(2,1)S(1)} %pack.1.q0), channel_id=1, source_target_pairs={{0,4},{2,6},{4,0},{6,2},{1,5},{3,7},{5,1},{7,3},{8,12},{10,14},{12... | collective-permute-start | bytes 823304 | tf_op jit(solution)/shard_map/ppermute | solution.py:284
  9.5 2.5 %collective-permute-start.1 = (bf16[1072,128]{1,0:T(8,128)(2,1)S(1)}, bf16[1072,128]{1,0:T(8,128)(2,1)S(1)}, u32[]{:S(2)}, u32[]{:S(2)}) collective-permute-start(bf16[1072,128]{1,0:T(8,128)(2,1)S(1)} %pack.1.q0), channel_id=1, source_target_pairs={{0,2},{2,4},{4,6},{6,0},{1,3},{3,5},{5,7},{7,1},{8,10},{10,12},{12... | collective-permute-start | bytes 823304 | tf_op jit(solution)/shard_map/ppermute | solution.py:284
  12.0 3.9 %collective-permute-done.2.q2 = bf16[1072,128]{1,0:T(8,128)(2,1)S(1)} collective-permute-done((bf16[1072,128]{1,0:T(8,128)(2,1)S(1)}, bf16[1072,128]{1,0:T(8,128)(2,1)S(1)}, u32[]{:S(2)}, u32[]{:S(2)}) %collective-permute-start.2) | collective-permute-done | bytes 274464 | tf_op jit(solution)/shard_map/ppermute | solution.py:284
  15.9 6.4 %collective-permute-done.1.q1 = bf16[1072,128]{1,0:T(8,128)(2,1)S(1)} collective-permute-done((bf16[1072,128]{1,0:T(8,128)(2,1)S(1)}, bf16[1072,128]{1,0:T(8,128)(2,1)S(1)}, u32[]{:S(2)}, u32[]{:S(2)}) %collective-permute-start.1) | collective-permute-done | bytes 274464 | tf_op jit(solution)/shard_map/ppermute | solution.py:284
  22.3 1.1 pad_maximum_fusion
  23.5 4.9 %collective-permute-start.4 = (bf16[4,1072,128]{2,1,0:T(8,128)(2,1)}, bf16[4,1072,128]{2,1,0:T(8,128)(2,1)S(1)}, u32[]{:S(2)}, u32[]{:S(2)}) collective-permute-start(bf16[4,1072,128]{2,1,0:T(8,128)(2,1)} %pad_maximum_fusion), channel_id=1, source_target_pairs={{0,1},{1,0},{2,3},{3,2},{4,5},{5,4},{6,7},{7,6},{8,9},{9,8},{10,11... | collective-permute-start | bytes 3293192 | tf_op jit(solution)/shard_map/ppermute | solution.py:288
  28.4 1.8 %offer.1 = (bf16[8,9,8,128]{3,2,1,0:T(8,128)(2,1)}, bf16[8,8,128]{2,1,0:T(8,128)(2,1)}) custom-call(s32[1]{0:T(128)} %bitcast.1.rank_ref, s32[1]{0:T(128)} %bitcast.tp_ref, bf16[64,512]{1,0:T(8,128)(2,1)} %bitcast.25, bf16[64,512]{1,0:T(8,128)(2,1)} %bitcast.26, s32[8,16]{1,0:T(8,128)} %chosen_ref.1), custom_call_target="tpu_custom_call" | custom-call | flops 262144 | bytes 1048576 | tf_op jit(solution)/shard_map/offer/pallas_call | solution.py:264
  30.2 14.9 %all_to_all.30.pushed_ref = bf16[8,9,8,128]{3,2,1,0:T(8,128)(2,1)S(1)} all-to-all(bf16[8,9,8,128]{3,2,1,0:T(8,128)(2,1)} %get-tuple-element.14), channel_id=1, replica_groups={{0,64,128,192,256,320,384,448},{8,72,136,200,264,328,392,456},{16,80,14..., dimensions={0} | all-to-all | bytes 294912 | tf_op jit(solution)/shard_map/all_to_all | solution.py:308
  45.1 6.6 %collective-permute-start = (bf16[8,8,128]{2,1,0:T(8,128)(2,1)S(1)}, bf16[8,8,128]{2,1,0:T(8,128)(2,1)S(1)}, u32[]{:S(2)}, u32[]{:S(2)}) collective-permute-start(bf16[8,8,128]{2,1,0:T(8,128)(2,1)S(1)} %slice_bitcast_fusion), channel_id=1, source_target_pairs={{0,1},{1,0},{2,3},{3,2},{4,5},{5,4},{6,7},{7,6},{8,9},{9,8},{10,11... | collective-permute-start | bytes 49160 | tf_op jit(solution)/shard_map/ppermute | solution.py:288
  51.7 0.8 collective-permute-done.wants_ref
  52.5 0.8 pick.1
  53.3 5.7 %all-to-all-start.1 = ((bf16[8,8,8,128]{3,2,1,0:T(8,128)(2,1)}), bf16[8,8,8,128]{3,2,1,0:T(8,128)(2,1)S(1)}, u32[]{:S(2)}, u32[]{:S(2)}) async-start(bf16[8,8,8,128]{3,2,1,0:T(8,128)(2,1)} %pick.1), calls=%async_computation.1 | async-start | bytes 262144 | tf_op jit(solution)/shard_map/all_to_all | solution.py:308
  59.0 0.1 subtract_select_fusion
  59.1 7.8 %all-to-all-done.1 = bf16[8,8,8,128]{3,2,1,0:T(8,128)(2,1)S(1)} async-done(((bf16[8,8,8,128]{3,2,1,0:T(8,128)(2,1)}), bf16[8,8,8,128]{3,2,1,0:T(8,128)(2,1)S(1)}, u32[]{:S(2)}, u32[]{:S(2)}) %all-to-all-start.1) | async-done | bytes 131104 | tf_op jit(solution)/shard_map/all_to_all | solution.py:308
  67.0 0.7 copy-done
  67.7 4.3 %attend.1 = (bf16[64,8,128]{2,1,0:T(8,128)(2,1)S(1)}, f32[8,8,128]{2,1,0:T(8,128)S(1)}, f32[4,512,128]{2,1,0:T(8,128)S(1)}, bf16[4,512,128]{2,1,0:T(8,128)(2,1)S(1)}) custom-call(s32[8,16]{1,0:T(8,128)S(1)} %get-tuple-element.25.slot_ref, s32[1]{0:T(128)} %bitcast.tp_ref, s32[8,16]{1,0:T(8,128)S(1)} %get-tuple-element.24.rel_ref, ...), custom_call_target="tpu_custom_call" | custom-call | flops 1073741824 | bytes 1048576 | tf_op jit(solution)/shard_map/attend/pallas_call | solution.py:264
  72.0 4.8 %collective-permute-start.5 = (bf16[4,512,128]{2,1,0:T(8,128)(2,1)S(1)}, bf16[4,512,128]{2,1,0:T(8,128)(2,1)S(1)}, u32[]{:S(2)}, u32[]{:S(2)}) collective-permute-start(bf16[4,512,128]{2,1,0:T(8,128)(2,1)S(1)} %get-tuple-element.17), channel_id=1, source_target_pairs={{0,1},{1,0},{2,3},{3,2},{4,5},{5,4},{6,7},{7,6},{8,9},{9,8},{10,11... | collective-permute-start | bytes 1572872 | tf_op jit(solution)/shard_map/ppermute | solution.py:288
  76.8 1.5 %collective-permute-done.5 = bf16[4,512,128]{2,1,0:T(8,128)(2,1)S(1)} collective-permute-done((bf16[4,512,128]{2,1,0:T(8,128)(2,1)S(1)}, bf16[4,512,128]{2,1,0:T(8,128)(2,1)S(1)}, u32[]{:S(2)}, u32[]{:S(2)}) %collective-permute-start.5) | collective-permute-done | bytes 524320 | tf_op jit(solution)/shard_map/ppermute | solution.py:288
  78.3 0.1 add_convert_fusion
  78.4 11.9 %all_to_all.31 = bf16[4,512,128]{2,1,0:T(8,128)(2,1)S(1)} all-to-all(bf16[4,512,128]{2,1,0:T(8,128)(2,1)S(1)} %add_convert_fusion), channel_id=1, replica_groups=mesh['z'=8,'y'=8,'x'=4,'c'=2] {'x'}, dimensions={0} | all-to-all | bytes 1048576 | tf_op jit(solution)/shard_map/all_to_all | solution.py:396
  90.3 0.1 convert_element_type.20
  90.4 0.1 fusion.2
  90.4 0.7 convolution_convert_fusion.part_ref
  91.2 0.3 turn.1
  91.6 21.8 %all_to_all.32.parts_ref = bf16[8,9,64,128]{3,2,1,0:T(8,128)(2,1)S(1)} all-to-all(bf16[8,9,64,128]{3,2,1,0:T(8,128)(2,1)S(1)} %turn.1), channel_id=1, replica_groups={{0,8,16,24,32,40,48,56},{64,72,80,88,96,104,112,120},{128,136,144,152,1..., dimensions={0} | all-to-all | bytes 2359296 | tf_op jit(solution)/shard_map/all_to_all | solution.py:308
  113.3 0.4 fold.1
  113.7 11.7 %all_to_all.33.back_ref = bf16[8,2,64,128]{3,2,1,0:T(8,128)(2,1)S(1)} all-to-all(bf16[8,2,64,128]{3,2,1,0:T(8,128)(2,1)S(1)} %fold.1), channel_id=1, replica_groups={{0,64,128,192,256,320,384,448},{8,72,136,200,264,328,392,456},{16,80,14..., dimensions={0} | all-to-all | bytes 524288 | tf_op jit(solution)/shard_map/all_to_all | solution.py:308
  125.4 0.6 settle.1
  126.1 10.9 %all_to_all.34.pieces_ref = bf16[8,8,8,128]{3,2,1,0:T(8,128)(2,1)S(1)} all-to-all(bf16[8,8,8,128]{3,2,1,0:T(8,128)(2,1)S(1)} %get-tuple-element.20), channel_id=1, replica_groups=mesh['z'=8,'y'=8,'x'=4,'c'=2] {'x','c'}, dimensions={0} | all-to-all | bytes 262144 | tf_op jit(solution)/shard_map/all_to_all | solution.py:427
  137.0 0.8 place.1
  (11 shorter events, 0.0 us)
Async XLA Ops:
  1.9 10.2 %collective-permute-start.3 = (bf16[1072,128]{1,0:T(8,128)(2,1)S(1)}, bf16[1072,128]{1,0:T(8,128)(2,1)S(1)}, u32[]{:S(2)}, u32[]{:S(2)}) collective-permute-start(bf16[1072,128]{1,0:T(8,128)(2,1)S(1)} %pack.1.q0), channel_id=1, source_target_pairs={{0,6},{2,0},{4,2},{6,4},{1,7},{3,1},{5,3},{7,5},{8,14},{10,8},{12,... | collective-permute-start | bytes 823304 | tf_op jit(solution)/shard_map/ppermute | solution.py:284
  7.1 8.8 %collective-permute-start.2 = (bf16[1072,128]{1,0:T(8,128)(2,1)S(1)}, bf16[1072,128]{1,0:T(8,128)(2,1)S(1)}, u32[]{:S(2)}, u32[]{:S(2)}) collective-permute-start(bf16[1072,128]{1,0:T(8,128)(2,1)S(1)} %pack.1.q0), channel_id=1, source_target_pairs={{0,4},{2,6},{4,0},{6,2},{1,5},{3,7},{5,1},{7,3},{8,12},{10,14},{12... | collective-permute-start | bytes 823304 | tf_op jit(solution)/shard_map/ppermute | solution.py:284
  9.5 12.8 %collective-permute-start.1 = (bf16[1072,128]{1,0:T(8,128)(2,1)S(1)}, bf16[1072,128]{1,0:T(8,128)(2,1)S(1)}, u32[]{:S(2)}, u32[]{:S(2)}) collective-permute-start(bf16[1072,128]{1,0:T(8,128)(2,1)S(1)} %pack.1.q0), channel_id=1, source_target_pairs={{0,2},{2,4},{4,6},{6,0},{1,3},{3,5},{5,7},{7,1},{8,10},{10,12},{12... | collective-permute-start | bytes 823304 | tf_op jit(solution)/shard_map/ppermute | solution.py:284
  22.3 36.7 %copy-start.3 = (s32[8,16]{1,0:T(8,128)S(1)}, s32[8,16]{1,0:T(8,128)}, u32[]{:S(2)}) copy-start(s32[8,16]{1,0:T(8,128)} %chosen_ref.1) | copy-start | bytes 1540
  23.5 43.5 %collective-permute-start.4 = (bf16[4,1072,128]{2,1,0:T(8,128)(2,1)}, bf16[4,1072,128]{2,1,0:T(8,128)(2,1)S(1)}, u32[]{:S(2)}, u32[]{:S(2)}) collective-permute-start(bf16[4,1072,128]{2,1,0:T(8,128)(2,1)} %pad_maximum_fusion), channel_id=1, source_target_pairs={{0,1},{1,0},{2,3},{3,2},{4,5},{5,4},{6,7},{7,6},{8,9},{9,8},{10,11... | collective-permute-start | bytes 3293192 | tf_op jit(solution)/shard_map/ppermute | solution.py:288
  45.1 7.4 %collective-permute-start = (bf16[8,8,128]{2,1,0:T(8,128)(2,1)S(1)}, bf16[8,8,128]{2,1,0:T(8,128)(2,1)S(1)}, u32[]{:S(2)}, u32[]{:S(2)}) collective-permute-start(bf16[8,8,128]{2,1,0:T(8,128)(2,1)S(1)} %slice_bitcast_fusion), channel_id=1, source_target_pairs={{0,1},{1,0},{2,3},{3,2},{4,5},{5,4},{6,7},{7,6},{8,9},{9,8},{10,11... | collective-permute-start | bytes 49160 | tf_op jit(solution)/shard_map/ppermute | solution.py:288
  53.3 13.6 %all-to-all-start.1 = ((bf16[8,8,8,128]{3,2,1,0:T(8,128)(2,1)}), bf16[8,8,8,128]{3,2,1,0:T(8,128)(2,1)S(1)}, u32[]{:S(2)}, u32[]{:S(2)}) async-start(bf16[8,8,8,128]{3,2,1,0:T(8,128)(2,1)} %pick.1), calls=%async_computation.1 | async-start | bytes 262144 | tf_op jit(solution)/shard_map/all_to_all | solution.py:308
  67.0 0.7 copy-start
  72.0 6.3 %collective-permute-start.5 = (bf16[4,512,128]{2,1,0:T(8,128)(2,1)S(1)}, bf16[4,512,128]{2,1,0:T(8,128)(2,1)S(1)}, u32[]{:S(2)}, u32[]{:S(2)}) collective-permute-start(bf16[4,512,128]{2,1,0:T(8,128)(2,1)S(1)} %get-tuple-element.17), channel_id=1, source_target_pairs={{0,1},{1,0},{2,3},{3,2},{4,5},{5,4},{6,7},{7,6},{8,9},{9,8},{10,11... | collective-permute-start | bytes 1572872 | tf_op jit(solution)/shard_map/ppermute | solution.py:288
  78.3 12.1 %copy-start.1 = (bf16[512,4096]{1,0:T(8,128)(2,1)S(1)}, bf16[512,4096]{1,0:T(8,128)(2,1)}, u32[]{:S(2)}) copy-start(bf16[512,4096]{1,0:T(8,128)(2,1)} %param.8) | copy-start | bytes 12582916
  90.4 0.8 copy-start.2
